TPU v7x, 512 devices: a whole 4x4x16 slice. The times are simulated.
512 devices in a mesh: sp: 16 (over z), fs: 4 (over y), tp: 8 (over x, core).
Axes of the slice: x: 4, y: 4, z: 16, core: 2. Of those that a mesh axis runs over, the one named last changes fastest.
Arguments:
- activations: bfloat16 [4, 4096, 4096], P('fs', 'sp'), may hold values from -60 to 60
- input_norm_gain: float32 [4096], replicated, may hold values from 0.1 to 1.9
- pooling_channel_weight: bfloat16 [4096, 1024], P(('sp', 'fs'), 'tp'), may hold values from -0.09375 to 0.09375
- query_projection_weight: bfloat16 [4096, 1024], P(('sp', 'fs'), 'tp'), may hold values from -0.09375 to 0.09375
- key_projection_weight: bfloat16 [4096, 1024], P(('sp', 'fs'), 'tp'), may hold values from -0.09375 to 0.09375
- value_projection_weight: bfloat16 [4096, 1024], P(('sp', 'fs'), 'tp'), may hold values from -0.09375 to 0.09375
- output_gate_weight: bfloat16 [4096, 1024], P(('sp', 'fs'), 'tp'), may hold values from -0.09375 to 0.09375
- decay_first_factor: bfloat16 [4096, 64], P(('sp', 'fs')), may hold values from -0.09375 to 0.09375
- decay_second_factor: bfloat16 [64, 1024], P(None, 'tp'), may hold values from -0.75 to 0.75
- decay_gate_bias: float32 [1024], P('tp')
- decay_extra_log: float32 [16, 4096], P('tp', 'sp'), may hold values from -1.5 to 0
- head_norm_gain: float32 [1024], P('tp'), may hold values from 0.1 to 1.9
- starting_state: float32 [4, 16, 64, 64], P('fs', 'tp'), may hold values from -384 to 384
- pooling_group_weight: bfloat16 [8, 128, 128], P('tp'), may hold values from -0.5 to 0.5
- pooling_channel_scale: float32 [1024], P('tp'), may hold values from 0.1 to 1.9
- pooling_output_rows: bfloat16 [1024, 4096], P('sp', 'tp'), may hold values from -0.125 to 0.125
- attention_output_rows: bfloat16 [1024, 4096], P('sp', 'tp'), may hold values from -0.125 to 0.125
Outputs:
- mixed: bfloat16 [4, 4096, 4096], P('fs', 'sp', 'tp')
All inputs are finite; a program needn't handle non-finite values.
Results may differ from a plain program's by a relative error of at most 0.012.
Values may be sent and summed in bfloat16 or wider, within the bound.
No kernel may reach another device: no remote copies, remote signals or barrier semaphores. Data moves between devices by JAX's collectives and lax.ppermute only.
A program may use at most 64 MiB of HBM per device.

v0:
```python
import math

import jax
import jax.numpy as jnp
from jax import lax
from jax.sharding import PartitionSpec as P

POOL_GROUP_WIDTH = 128
HEAD_WIDTH = 64
BLOCK = 64
REACH = 15


norm_eps = 1e-06
decay_temper = 16.0
highest = lax.Precision.HIGHEST


def in_one_piece(arrays, axis, dim, along):
    both = jnp.concatenate(arrays, axis=along)
    result, at, done = (lax.all_gather(both, axis, axis=dim, tiled=True), 0, [])
    for a in arrays:
        done.append(lax.slice_in_dim(result, at, at + a.shape[along], axis=along))
        at += a.shape[along]
    return tuple(done)


def shifted(shard, axis, by):
    peers = lax.axis_size(axis)
    pairs = [(i, i + by) for i in range(peers) if 0 <= i + by < peers]
    return lax.ppermute(shard, axis, pairs)


def side_by_side(arrays, axis, dim, along):
    widths = [math.prod(a.shape[along:]) for a in arrays]
    both = jnp.concatenate(
        [a.reshape(*a.shape[:along], w) for a, w in zip(arrays, widths)], axis=along
    )
    result = lax.all_gather(both, axis, axis=dim, tiled=True)
    parts = jnp.split(result, [sum(widths[:k]) for k in range(1, len(widths))], axis=along)
    return tuple(
        (b.reshape(*result.shape[:along], *a.shape[along:]) for a, b in zip(arrays, parts))
    )


def window_levels(extended, total_row_count):
    width_two = extended[:, 1:] + extended[:, :-1]
    width_four = width_two[:, 2:] + width_two[:, :-2]
    width_eight = width_four[:, 4:] + width_four[:, :-4]
    width_sixteen = width_eight[:, 8:] + width_eight[:, :-8]
    return (
        width_two[:, -total_row_count:],
        width_four[:, -total_row_count:],
        width_eight[:, -total_row_count:],
        width_sixteen,
    )


def pool_branch(
    pool_input, previous, pooling_group_weight, pooling_channel_scale, channel_first, position_first
):
    batch_groups, total_row_count, channels = pool_input.shape
    current = pool_input.astype(jnp.float32)
    extended = jnp.concatenate([previous.astype(jnp.float32), current], axis=1)
    window_sums = window_levels(extended, total_row_count)
    level_ids = (channel_first + jnp.arange(channels)) // POOL_GROUP_WIDTH % 4
    window = jnp.where(
        level_ids == 0, 2.0, jnp.where(level_ids == 1, 4.0, jnp.where(level_ids == 2, 8.0, 16.0))
    ).astype(jnp.float32)
    chosen = jnp.where(
        level_ids == 0,
        window_sums[0],
        jnp.where(
            level_ids == 1,
            window_sums[1],
            jnp.where(level_ids == 2, window_sums[2], window_sums[3]),
        ),
    )
    positions = (position_first + jnp.arange(total_row_count)).astype(jnp.float32)
    counts = jnp.minimum(positions[:, None] + 1.0, window[None, :])
    deviation = (chosen / counts - current).astype(jnp.bfloat16)
    grouped = deviation.reshape(
        batch_groups, total_row_count, channels // POOL_GROUP_WIDTH, POOL_GROUP_WIDTH
    )
    mixture = jnp.einsum(
        "btgc,gcd->btgd", grouped, pooling_group_weight, preferred_element_type=jnp.float32
    )
    return (
        mixture.reshape(batch_groups, total_row_count, channels) * pooling_channel_scale
    ).astype(jnp.bfloat16)


def decay_log_values(decay_lower_bound, decay_second_factor, decay_gate_bias, decay_extra_log):
    batch_groups, total_row_count, rank_width = decay_lower_bound.shape
    gate_input = (
        jnp.dot(
            decay_lower_bound.reshape(batch_groups * total_row_count, rank_width),
            decay_second_factor,
            preferred_element_type=jnp.float32,
        )
        + decay_gate_bias
    )
    logarithm_rates = jax.nn.log_sigmoid(gate_input) / decay_temper
    local_head_count = decay_extra_log.shape[0]
    logarithm_rates = (
        logarithm_rates.reshape(batch_groups, total_row_count, local_head_count, HEAD_WIDTH)
        + decay_extra_log.T[None, :, :, None]
    )
    return logarithm_rates.reshape(batch_groups, total_row_count, local_head_count * HEAD_WIDTH)


def to_blocks(source, local_head_count):
    batch_groups, total_row_count, _ = source.shape
    shaped = source.astype(jnp.float32).reshape(
        batch_groups, total_row_count // BLOCK, BLOCK, local_head_count, HEAD_WIDTH
    )
    return shaped.transpose(0, 3, 1, 2, 4)


def block_terms(queries, keys, values, decay_logarithm, local_head_count):
    scaled_query = to_blocks(queries, local_head_count) * HEAD_WIDTH ** (-0.5)
    key_blocks = to_blocks(keys, local_head_count)
    value_blocks = to_blocks(values, local_head_count)
    decay_sum = jnp.cumsum(to_blocks(decay_logarithm, local_head_count), axis=3)
    final_log = decay_sum[:, :, :, -1:, :]
    middle = decay_sum[:, :, :, BLOCK // 2 - 1 : BLOCK // 2, :]
    scores = jnp.einsum(
        "bhncd,bhnsd->bhncs",
        scaled_query * jnp.exp(decay_sum - middle),
        key_blocks * jnp.exp(middle - decay_sum),
        precision=highest,
    )
    causal = jnp.tril(jnp.ones((BLOCK, BLOCK), dtype=bool))
    scores = jnp.where(causal, scores, 0.0)
    within = jnp.einsum("bhncs,bhnse->bhnce", scores, value_blocks, precision=highest)
    block_states = jnp.einsum(
        "bhncd,bhnce->bhnde",
        key_blocks * jnp.exp(final_log - decay_sum),
        value_blocks,
        precision=highest,
    )
    return (scaled_query, decay_sum, within, block_states)


def finish(scaled_query, decay_sum, within, prior_states, outgate, head_norm_gain):
    carried = jnp.einsum(
        "bhncd,bhnde->bhnce", scaled_query * jnp.exp(decay_sum), prior_states, precision=highest
    )
    merged = within + carried
    merged = merged * lax.rsqrt(jnp.mean(merged * merged, axis=-1, keepdims=True) + norm_eps)
    batch_groups, local_head_count, blocks, _, _ = merged.shape
    merged = (
        merged.transpose(0, 2, 3, 1, 4).reshape(
            batch_groups, blocks * BLOCK, local_head_count * HEAD_WIDTH
        )
        * head_norm_gain
    )
    return (merged * jax.nn.silu(outgate.astype(jnp.float32))).astype(jnp.bfloat16)


def combine_states(earlier, later):
    return (earlier[0] * later[0], later[0][..., None] * earlier[1] + later[1])


def body(
    activations,
    input_norm_gain,
    pooling_channel_weight,
    query_projection_weight,
    key_projection_weight,
    value_projection_weight,
    output_gate_weight,
    decay_first_factor,
    decay_second_factor,
    decay_gate_bias,
    decay_extra_log,
    head_norm_gain,
    starting_state,
    pooling_group_weight,
    pooling_channel_scale,
    pooling_output_rows,
    attention_output_rows,
):
    batch_groups, total_row_count, model_width = activations.shape
    flat_rows = activations.reshape(batch_groups * total_row_count, model_width).astype(jnp.float32)
    inverse = lax.rsqrt(jnp.mean(flat_rows * flat_rows, axis=1, keepdims=True) + norm_eps)
    scaled = (flat_rows * input_norm_gain).astype(jnp.bfloat16)
    column_sizes = [
        pooling_channel_weight.shape[1],
        query_projection_weight.shape[1],
        key_projection_weight.shape[1],
        value_projection_weight.shape[1],
        output_gate_weight.shape[1],
        decay_first_factor.shape[1],
    ]
    pool_group, query_group, key_group, value_group, outgate_group, down_group = in_one_piece(
        (
            pooling_channel_weight,
            query_projection_weight,
            key_projection_weight,
            value_projection_weight,
            output_gate_weight,
            decay_first_factor,
        ),
        "fs",
        0,
        1,
    )
    projected = jnp.dot(
        scaled,
        jnp.concatenate(
            in_one_piece(
                (pool_group, query_group, key_group, value_group, outgate_group, down_group),
                "sp",
                0,
                1,
            ),
            axis=1,
        ),
        preferred_element_type=jnp.float32,
    )
    projected = (projected * inverse).astype(jnp.bfloat16)
    split_parts = []
    column_first = 0
    for size_here in column_sizes:
        split_parts.append(
            projected[:, column_first : column_first + size_here].reshape(
                batch_groups, total_row_count, size_here
            )
        )
        column_first += size_here
    pool_input, queries, keys, values, outgate, decay_lower_bound = split_parts
    previous = shifted(pool_input[:, total_row_count - REACH :, :], "sp", 1)
    channels_here = pool_input.shape[2]
    pool_out = pool_branch(
        pool_input,
        previous,
        pooling_group_weight,
        pooling_channel_scale,
        lax.axis_index("tp") * channels_here,
        lax.axis_index("sp") * total_row_count,
    )
    decay_logarithm = decay_log_values(
        decay_lower_bound, decay_second_factor, decay_gate_bias, decay_extra_log
    )
    local_head_count = starting_state.shape[1]
    scaled_query, decay_sum, within, block_states = block_terms(
        queries, keys, values, decay_logarithm, local_head_count
    )
    block_log = decay_sum[:, :, :, -1, :]
    block_decay = jnp.exp(block_log)

    def advance(state_now, block_pair):
        return (block_pair[1][..., None] * state_now + block_pair[0], state_now)

    zero_state = jnp.zeros(starting_state.shape, jnp.float32)
    device_state, local_prior = lax.scan(
        advance,
        zero_state,
        (block_states.transpose(2, 0, 1, 3, 4), block_decay.transpose(2, 0, 1, 3)),
    )
    local_prior = local_prior.transpose(1, 2, 0, 3, 4)
    device_decay = jnp.exp(jnp.sum(block_log, axis=2))
    all_decay, all_state = side_by_side((device_decay[None], device_state[None]), "sp", 0, 4)
    own_index = lax.axis_index("sp")

    def absorb(position, running_pair):
        folded = combine_states(running_pair, (all_decay[position], all_state[position]))
        keep = position < own_index
        return (
            jnp.where(keep, folded[0], running_pair[0]),
            jnp.where(keep, folded[1], running_pair[1]),
        )

    before_decay, before_state = lax.fori_loop(
        0, all_decay.shape[0], absorb, (jnp.ones_like(device_decay), jnp.zeros_like(device_state))
    )
    incoming = before_decay[..., None] * starting_state + before_state
    opening = jnp.exp(jnp.cumsum(block_log, axis=2) - block_log)
    prior_states = local_prior + opening[..., None] * incoming[:, :, None]
    state_out = finish(scaled_query, decay_sum, within, prior_states, outgate, head_norm_gain)
    pool_rows_all, state_rows_all = in_one_piece(
        (pooling_output_rows, attention_output_rows), "sp", 0, 1
    )
    pieces = in_one_piece((pool_out, state_out), "tp", 2, 0)
    accumulated = jnp.einsum(
        "btc,cd->btd", pieces[0], pool_rows_all, preferred_element_type=jnp.float32
    )
    result = accumulated + jnp.einsum(
        "btc,cd->btd", pieces[1], state_rows_all, preferred_element_type=jnp.float32
    )
    return result.astype(jnp.bfloat16)


def solution(mesh):
    in_specs = (
        P("fs", "sp", None),
        P(),
        P(("sp", "fs"), "tp"),
        P(("sp", "fs"), "tp"),
        P(("sp", "fs"), "tp"),
        P(("sp", "fs"), "tp"),
        P(("sp", "fs"), "tp"),
        P(("sp", "fs"), None),
        P(None, "tp"),
        P("tp"),
        P("tp", "sp"),
        P("tp"),
        P("fs", "tp", None, None),
        P("tp", None, None),
        P("tp"),
        P("sp", "tp"),
        P("sp", "tp"),
    )
    out_specs = P("fs", "sp", "tp")
    return jax.shard_map(body, mesh=mesh, in_specs=in_specs, out_specs=out_specs, check_vma=False)
```

profile of v0, /device:TPU:1, one launch (start us, length us, event | category | flops | bytes accessed | tf_op | source)
XLA Modules:
  0.0 229.2 jit_solution(7451734811331020356)
XLA Ops:
  6.6 0.9 constant_dynamic-update-slice_fusion.5
  7.4 0.7 constant_dynamic-update-slice_fusion.4
  8.2 0.7 constant_dynamic-update-slice_fusion.3
  8.9 0.7 constant_dynamic-update-slice_fusion.2
  9.6 0.7 constant_dynamic-update-slice_fusion.1
  10.4 0.7 constant_dynamic-update-slice_fusion
  11.1 12.0 %all_gather.15 = bf16[256,704]{1,0:T(8,128)(2,1)} all-gather(bf16[64,704]{1,0:T(8,128)(2,1)S(1)} %constant_dynamic-update-slice_fusion), channel_id=1, replica_groups=mesh['sp'=16,'fs'=4,'tp'=8] {'fs'}, dimensions={0}, use_global_device_ids=true | all-gather | bytes 450560 | tf_op jit(solution)/shard_map/all_gather | solution.py:21
  23.2 1.5 pad_maximum_fusion.2
  24.9 2.1 fusion.2
  27.1 85.9 %all-gather.4.cloned.1.call-done = bf16[4096,704]{1,0:T(8,128)(2,1)} async-done(((bf16[256,704]{1,0:T(8,128)(2,1)}), bf16[4096,704]{1,0:T(8,128)(2,1)}) %all-gather.4.cloned.1.call-update) | async-done | bytes 5767184 | tf_op jit(solution)/shard_map/all_gather | solution.py:21
  113.0 5.3 %fusion.10 = bf16[256,704]{0,1:T(8,128)(2,1)S(1)} fusion(bf16[4096,704]{1,0:T(8,128)(2,1)} %all-gather.4.cloned.1.call-done, bf16[1,256,4096]{2,1,0:T(8,128)(2,1)S(1)} %copy-done.1, f32[4096]{0:T(1024)S(1)} %copy-done.9, f32[256]{0:T(256)S(1)} %add_rsqrt_fusion.1), kind=kOutput, calls=%fused_computation.15 | convolution fusion | flops 1479901184 | bytes 8242176 | tf_op jit(solution)/shard_map/dot_general | solution.py:209
  118.4 0.7 copy-done.2
  120.8 3.1 %while.29 = (s32[]{:T(128)}, f32[1,2,64,64]{3,2,1,0:T(8,128)S(1)}, f32[4,1,2,64,64]{4,3,2,1,0:T(8,128)}, f32[4,1,2,64]{3,0,2,1:T(4,128)S(1)}, f32[4,1,2,64,64]{4,3,0,2,1:T(8,128)S(1)}, /*index=5*/s32[]{:T(128)}, s32[]{:T(128)}) while((s32[]{:T(128)}, f32[1,2,64,64]{3,2,1,0:T(8,128)S(1)}, f32[4,1,2,64,64]{4,3,2,1,0:T(8,128)}, ...), condition=%wide.region_3.4_spmd.clone, body=%wide.region_2.3_spmd.clone.sunk | while | flops 32771 | bytes 198752 | solution.py:257
  120.8 0.6 bitcast_dynamic-update-slice_fusion.2
  124.1 34.3 %all_gather.17 = f32[16,1,2,64,65]{4,3,2,1,0:T(8,128)S(1)} all-gather(f32[1,1,2,64,65]{4,3,2,1,0:T(8,128)S(1)} %pad_maximum_fusion.3), channel_id=1, replica_groups=mesh['sp'=16,'fs'=4,'tp'=8] {'sp'}, dimensions={0}, use_global_device_ids=true | all-gather | bytes 565760 | tf_op jit(solution)/shard_map/all_gather | solution.py:39
  159.1 2.5 %while.30 = (s32[]{:T(128)}, f32[1,2,64]{2,1,0:T(2,128)S(1)}, f32[1,2,64,64]{3,2,1,0:T(8,128)S(1)}, s32[]{:T(128)}, f32[16,1,2,64]{3,0,2,1:T(8,128)S(1)}, /*inde...) while((s32[]{:T(128)}, f32[1,2,64]{2,1,0:T(2,128)S(1)}, f32[1,2,64,64]{3,2,1,0:T(8,128)S(1)}, ...), condition=%wide.region_7.8_spmd.clone, body=%wide.region_6.7_spmd.clone.sunk | while | flops 33156 | bytes 101491 | solution.py:275
  163.1 0.7 multiply_reduce_fusion
  164.3 2.2 collective-permute-start
  166.6 1.0 collective-permute-done
  168.5 0.7 pad_maximum_fusion.1
  169.2 11.2 %all-gather.8.cloned.1.call-done = bf16[1024,1024]{1,0:T(8,128)(2,1)} async-done(((bf16[64,1024]{1,0:T(8,128)(2,1)}), bf16[1024,1024]{1,0:T(8,128)(2,1)}) %all-gather.8.cloned.1.call-update) | async-done | bytes 2097168 | tf_op jit(solution)/shard_map/all_gather | solution.py:21
  180.4 38.1 %all-gather.6.cloned.1.call-done = bf16[2,256,1024]{1,2,0:T(8,128)(2,1)} async-done(((bf16[2,256,128]{1,2,0:T(8,128)(2,1)}), bf16[2,256,1024]{1,2,0:T(8,128)(2,1)}) %all-gather.6.cloned.1.call-update) | async-done | bytes 1048592 | tf_op jit(solution)/shard_map/all_gather | solution.py:21
  218.6 1.8 fusion.19
  220.4 2.2 fusion.14
  (136 shorter events, 9.9 us)
Async XLA Ops:
  6.5 161.6 %copy-start = (bf16[1,128,128]{2,1,0:T(8,128)(2,1)S(1)}, bf16[1,128,128]{2,1,0:T(8,128)(2,1)}, u32[]{:S(2)}) copy-start(bf16[1,128,128]{2,1,0:T(8,128)(2,1)} %param.34) | copy-start | bytes 98308
  6.5 106.5 %copy-start.1 = (bf16[1,256,4096]{2,1,0:T(8,128)(2,1)S(1)}, bf16[1,256,4096]{2,1,0:T(8,128)(2,1)}, u32[]{:S(2)}) copy-start(bf16[1,256,4096]{2,1,0:T(8,128)(2,1)} %param.21) | copy-start | bytes 6291460
  6.5 20.5 %copy-start.6 = (f32[2,256]{1,0:T(2,128)S(1)}, f32[2,256]{1,0:T(2,128)}, u32[]{:S(2)}) copy-start(f32[2,256]{1,0:T(2,128)} %param.31) | copy-start | bytes 6148
  6.5 106.5 %copy-start.9 = (f32[4096]{0:T(1024)S(1)}, f32[4096]{0:T(1024)}, u32[]{:S(2)}) copy-start(f32[4096]{0:T(1024)} %param.22) | copy-start | bytes 49156
  6.5 106.5 %all-gather.4.cloned.1.call-start = ((), (), s32[]{:S(2)}) async-start(), calls=%async_computation | async-start | bytes 6684672 | tf_op jit(solution)/shard_map/all_gather | solution.py:21
  23.1 157.3 %all-gather.8.cloned.1.call-start = ((), (), s32[]{:S(2)}) async-start(), calls=%async_computation.2 | async-start | bytes 2228224 | tf_op jit(solution)/shard_map/all_gather | solution.py:21
  24.8 193.8 %all-gather.6.cloned.1.call-start = ((), (), s32[]{:S(2)}) async-start(), calls=%async_computation.1 | async-start | bytes 1179648 | tf_op jit(solution)/shard_map/all_gather | solution.py:21
  27.1 91.9 %copy-start.10 = (bf16[64,128]{1,0:T(8,128)(2,1)S(1)}, bf16[64,128]{1,0:T(8,128)(2,1)}, u32[]{:S(2)}) copy-start(bf16[64,128]{1,0:T(8,128)(2,1)} %param.29) | copy-start | bytes 49156
  27.1 91.9 %copy-start.11 = (f32[128]{0:T(128)S(1)}, f32[128]{0:T(128)}, u32[]{:S(2)}) copy-start(f32[128]{0:T(128)} %param.30) | copy-start | bytes 1540
  118.3 0.7 copy-start.2
  158.4 3.3 %copy-start.3 = (bf16[256,704]{0,1:T(8,128)(2,1)S(1)}, bf16[256,704]{0,1:T(8,128)(2,1)}, u32[]{:S(2)}) copy-start(bf16[256,704]{0,1:T(8,128)(2,1)} %copy-done.2) | copy-start | bytes 1081348
  158.7 3.3 %copy-start.5 = (f32[1,2,64,64]{3,2,1,0:T(8,128)S(1)}, f32[1,2,64,64]{3,2,1,0:T(8,128)}, u32[]{:S(2)}) copy-start(f32[1,2,64,64]{3,2,1,0:T(8,128)} %param.33) | copy-start | bytes 98308
  159.1 4.0 %copy-start.4 = (f32[4,1,2,64,64]{4,3,2,1,0:T(8,128)S(1)}, f32[4,1,2,64,64]{4,3,2,1,0:T(8,128)}, u32[]{:S(2)}) copy-start(f32[4,1,2,64,64]{4,3,2,1,0:T(8,128)} %get-tuple-element.143) | copy-start | bytes 393220
  162.7 3.8 %copy-start.7 = (f32[128]{0:T(128)S(1)}, f32[128]{0:T(128)}, u32[]{:S(2)}) copy-start(f32[128]{0:T(128)} %param.32) | copy-start | bytes 1540
  163.0 5.1 %copy-start.12 = (f32[128]{0:T(128)S(1)}, f32[128]{0:T(128)}, u32[]{:S(2)}) copy-start(f32[128]{0:T(128)} %param.35) | copy-start | bytes 1540
  164.3 3.4 %collective-permute-start = (bf16[1,15,128]{1,2,0:T(8,128)(2,1)S(1)}, bf16[1,15,128]{1,2,0:T(8,128)(2,1)S(1)}, u32[]{:S(2)}, u32[]{:S(2)}) collective-permute-start(bf16[1,15,128]{1,2,0:T(8,128)(2,1)S(1)} %slice.109), channel_id=1, source_target_pairs={{0,32},{32,64},{64,96},{96,128},{128,160},{160,192},{192,224},{224... | collective-permute-start | bytes 11528 | tf_op jit(solution)/shard_map/ppermute | solution.py:31
  180.4 40.0 %copy-start.8 = (bf16[1024,1024]{1,0:T(8,128)(2,1)S(1)}, bf16[1024,1024]{1,0:T(8,128)(2,1)}, u32[]{:S(2)}) copy-start(bf16[1024,1024]{1,0:T(8,128)(2,1)} %all-gather.8.cloned.1.call-done) | copy-start | bytes 6291460
Sparse Core Ops, SparseCore 0:
  23.3 89.7 all-gather.3
  115.1 65.2 all-gather.7
  182.6 35.9 all-gather.5
where the time goes:
time: 230 us; the launch traced here: 229 us
  waiting for transfers between devices  136 us (59%)
  blocking collectives  46.3 us (20%)
  between operations  13.5 us (6%)
  matrix products  12.1 us (5%)
  other arithmetic  10.3 us (4%)
  local copies, waits for them, and re-layouts  7.63 us (3%)
  starting transfers between devices  2.34 us (1%)
    all_gather x3, waiting for transfers between devices, in_one_piece(): result, at, done = (lax.all_gather(both, axis, axis=dim, tiled=True), 0, [])  135 us
    all_gather x1, blocking collectives, side_by_side(): result = lax.all_gather(both, axis, axis=dim, tiled=True)  34.3 us
    all_gather x1, blocking collectives, in_one_piece(): result, at, done = (lax.all_gather(both, axis, axis=dim, tiled=True), 0, [])  12 us
    dot_general x1, matrix products, body(): jnp.dot(scaled, jnp.concatenate(in_one_piece((pool_group, query_group, ke...  5.27 us
    unnamed x32, local copies, waits for them, and re-layouts  4.87 us
  transfers between devices with their start and end apart: 4, of which 4 were waited for; matrix products, arithmetic and copies ran while one was open for 9% of the time, Pallas kernels for 0%

commit v1 on v0

v1 whole, which is shorter than its diff:
```python
import jax
import jax.numpy as jnp
from jax import lax
from jax.experimental import pallas as pl
from jax.experimental.pallas import tpu as pltpu
from jax.sharding import PartitionSpec as P

POOL_GROUP_WIDTH = 128
HEAD_WIDTH = 64
BLOCK = 64
REACH = 15

norm_eps = 1e-06
decay_temper = 16.0
highest = lax.Precision.HIGHEST


def shifted(x, axis, by, wrap):
    n = lax.axis_size(axis)
    if wrap:
        pairs = [(i, (i + by) % n) for i in range(n)]
    else:
        pairs = [(i, i + by) for i in range(n) if 0 <= i + by < n]
    return lax.ppermute(x, axis, pairs)


def prep_kernel(own, act, gain, x0, x1, x2, x3, inverse):
    f32 = jnp.float32
    rows, width = act.shape
    outs = (x0, x1, x2, x3)
    lane = lax.broadcasted_iota(jnp.int32, (rows, 128), 1)
    low = lane < 64
    squares = jnp.zeros((rows, 128), f32)
    me = own[0]
    for p in range(width // 512):
        tiles = []
        for q in range(4):
            at = p * 512 + q * 128
            t = act[:, at : at + 128].astype(f32)
            squares = squares + t * t
            tiles.append(t * gain[:, at : at + 128])
        blocks = []
        for a, b in ((tiles[0], tiles[2]), (tiles[1], tiles[3])):
            blocks.append(jnp.where(low, a, pltpu.roll(b, 64, 1)).astype(jnp.bfloat16))
            blocks.append(jnp.where(low, pltpu.roll(a, 64, 1), b).astype(jnp.bfloat16))
        for f in range(4):

            @pl.when(me == f)
            def _(f=f, blocks=blocks, p=p):
                for k in range(4):
                    outs[k][:, p * 128 : (p + 1) * 128] = blocks[(f + k) % 4]

    total = jnp.sum(squares, axis=1, keepdims=True)
    inverse[...] = jnp.broadcast_to(lax.rsqrt(total / width + norm_eps), (rows, 128))


def prepare(act, gain, own):
    tokens, width = act.shape
    rows = 64
    part = pl.BlockSpec((rows, width // 4), lambda i, own: (i, 0))
    return pl.pallas_call(
        prep_kernel,
        grid_spec=pltpu.PrefetchScalarGridSpec(
            num_scalar_prefetch=1,
            grid=(tokens // rows,),
            in_specs=[
                pl.BlockSpec((rows, width), lambda i, own: (i, 0)),
                pl.BlockSpec((1, width), lambda i, own: (0, 0)),
            ],
            out_specs=[part, part, part, part, pl.BlockSpec((rows, 128), lambda i, own: (i, 0))],
        ),
        out_shape=[jax.ShapeDtypeStruct((tokens, width // 4), jnp.bfloat16)] * 4
        + [jax.ShapeDtypeStruct((tokens, 128), jnp.float32)],
        name="prep",
    )(own, act, gain)


def pool_branch(pool_input, previous, group_weight, channel_scale, group, position_first):
    rows, channels = pool_input.shape
    current = pool_input.astype(jnp.float32)
    extended = jnp.concatenate([previous.astype(jnp.float32), current], axis=0)
    two = extended[1:] + extended[:-1]
    four = two[2:] + two[:-2]
    eight = four[4:] + four[:-4]
    sixteen = eight[8:] + eight[:-8]
    level = group % 4
    chosen = jnp.where(
        level == 0,
        two[-rows:],
        jnp.where(level == 1, four[-rows:], jnp.where(level == 2, eight[-rows:], sixteen)),
    )
    window = jnp.where(
        level == 0, 2.0, jnp.where(level == 1, 4.0, jnp.where(level == 2, 8.0, 16.0))
    ).astype(jnp.float32)
    positions = (position_first + jnp.arange(rows)).astype(jnp.float32)
    counts = jnp.minimum(positions[:, None] + 1.0, window)
    deviation = (chosen / counts - current).astype(jnp.bfloat16)
    mixture = jnp.dot(deviation, group_weight[0], preferred_element_type=jnp.float32)
    return (mixture * channel_scale).astype(jnp.bfloat16)


def to_blocks(source, heads):
    rows, _ = source.shape
    shaped = source.astype(jnp.float32).reshape(rows // BLOCK, BLOCK, heads, HEAD_WIDTH)
    return shaped.transpose(2, 0, 1, 3)


def project_back(parts):
    total = parts[0]
    for k in (1, 2, 3):
        total = total + shifted(parts[k].astype(jnp.bfloat16), "fs", -k, True).astype(jnp.float32)
    return total


def body(
    activations,
    input_norm_gain,
    pooling_channel_weight,
    query_projection_weight,
    key_projection_weight,
    value_projection_weight,
    output_gate_weight,
    decay_first_factor,
    decay_second_factor,
    decay_gate_bias,
    decay_extra_log,
    head_norm_gain,
    starting_state,
    pooling_group_weight,
    pooling_channel_scale,
    pooling_output_rows,
    attention_output_rows,
):
    f32 = jnp.float32
    bf16 = jnp.bfloat16
    _, tokens, width = activations.shape
    heads = starting_state.shape[1]
    own = lax.axis_index("fs").astype(jnp.int32).reshape(1)
    late = jnp.concatenate(
        [
            query_projection_weight,
            output_gate_weight,
            pooling_channel_weight,
            pooling_output_rows,
            attention_output_rows,
        ],
        axis=1,
    )
    late = lax.all_gather(late, "sp", axis=0, tiled=True)
    x0, x1, x2, x3, inverse = prepare(
        activations.reshape(tokens, width), input_norm_gain.reshape(1, width), own
    )
    early = jnp.concatenate(
        [key_projection_weight, value_projection_weight, decay_first_factor], axis=1
    )
    with jax.named_scope("early"):
        early = lax.all_gather(early, "sp", axis=0, tiled=True)
    with jax.named_scope("exchange"):
        x1 = shifted(x1, "fs", 1, True)
        x2 = shifted(x2, "fs", 2, True)
        x3 = shifted(x3, "fs", 3, True)
    xs = (x0, x1, x2, x3)
    inverse = inverse[:, :1]
    got = project_back([jnp.dot(x, early, preferred_element_type=f32) for x in xs])
    got = (got * inverse).astype(bf16)
    keys, values, low = got[:, :128], got[:, 128:256], got[:, 256:]

    gate_input = jnp.dot(low, decay_second_factor, preferred_element_type=f32) + decay_gate_bias
    rates = jax.nn.log_sigmoid(gate_input) / decay_temper
    rates = rates + jnp.repeat(decay_extra_log.T, HEAD_WIDTH, axis=1)
    key_blocks = to_blocks(keys, heads)
    value_blocks = to_blocks(values, heads)
    decay_sum = jnp.cumsum(to_blocks(rates, heads), axis=2)
    final_log = decay_sum[:, :, -1:, :]
    middle = decay_sum[:, :, BLOCK // 2 - 1 : BLOCK // 2, :]
    block_states = jnp.einsum(
        "hncd,hnce->hnde",
        key_blocks * jnp.exp(final_log - decay_sum),
        value_blocks,
        precision=highest,
    )
    block_log = decay_sum[:, :, -1, :]
    blocks = tokens // BLOCK
    state = jnp.zeros((heads, HEAD_WIDTH, HEAD_WIDTH), f32)
    local_prior = []
    opening = []
    log_before = jnp.zeros((heads, HEAD_WIDTH), f32)
    for n in range(blocks):
        local_prior.append(state)
        opening.append(jnp.exp(log_before))
        state = jnp.exp(block_log[:, n])[..., None] * state + block_states[:, n]
        log_before = log_before + block_log[:, n]

    run = jnp.concatenate(
        [
            state.transpose(2, 0, 1).reshape(HEAD_WIDTH, heads * HEAD_WIDTH),
            log_before.reshape(1, -1),
            jnp.zeros((7, heads * HEAD_WIDTH), f32),
        ],
        axis=0,
    )

    def join(earlier, later):
        log_later = later[HEAD_WIDTH : HEAD_WIDTH + 1]
        top = jnp.exp(log_later) * earlier[:HEAD_WIDTH] + later[:HEAD_WIDTH]
        return jnp.concatenate([top, earlier[HEAD_WIDTH:] + later[HEAD_WIDTH:]], axis=0)

    before = None
    for step in (1, 2, 4, 8):
        with jax.named_scope("scan"):
            came = shifted(run, "sp", step, False)
        before = came if before is None else join(came, before)
        run = join(came, run)
    start = starting_state[0].transpose(2, 0, 1).reshape(HEAD_WIDTH, heads * HEAD_WIDTH)
    incoming = jnp.exp(before[HEAD_WIDTH : HEAD_WIDTH + 1]) * start + before[:HEAD_WIDTH]
    incoming = incoming.reshape(HEAD_WIDTH, heads, HEAD_WIDTH).transpose(1, 2, 0)

    rest = late[:, :384]
    got = project_back([jnp.dot(x, rest, preferred_element_type=f32) for x in xs])
    got = (got * inverse).astype(bf16)
    queries, outgate, pool_input = got[:, :128], got[:, 128:256], got[:, 256:]
    previous = shifted(pool_input[tokens - REACH :], "sp", 1, False)

    scaled_query = to_blocks(queries, heads) * HEAD_WIDTH ** (-0.5)
    scores = jnp.einsum(
        "hncd,hnsd->hncs",
        scaled_query * jnp.exp(decay_sum - middle),
        key_blocks * jnp.exp(middle - decay_sum),
        precision=highest,
    )
    causal = jnp.tril(jnp.ones((BLOCK, BLOCK), dtype=bool))
    scores = jnp.where(causal, scores, 0.0)
    within = jnp.einsum("hncs,hnse->hnce", scores, value_blocks, precision=highest)
    prior = jnp.stack(
        [local_prior[n] + opening[n][..., None] * incoming for n in range(blocks)], axis=1
    )
    carried = jnp.einsum(
        "hncd,hnde->hnce", scaled_query * jnp.exp(decay_sum), prior, precision=highest
    )
    merged = within + carried
    merged = merged * lax.rsqrt(jnp.mean(merged * merged, axis=-1, keepdims=True) + norm_eps)
    merged = merged.transpose(1, 2, 0, 3).reshape(tokens, heads * HEAD_WIDTH) * head_norm_gain
    state_out = (merged * jax.nn.silu(outgate.astype(f32))).astype(bf16)

    pool_out = pool_branch(
        pool_input,
        previous,
        pooling_group_weight,
        pooling_channel_scale,
        lax.axis_index("tp"),
        lax.axis_index("sp") * tokens,
    )
    mine = jnp.concatenate([pool_out, state_out], axis=1)
    peers = lax.axis_size("tp")
    spread = lax.all_to_all(jnp.broadcast_to(mine[None], (peers,) + mine.shape), "tp", 0, 0)
    pool_rows = late[:, 384:896].reshape(peers, 128, -1)
    state_rows = late[:, 896:].reshape(peers, 128, -1)
    result = jnp.zeros((tokens, 512), f32)
    for t in range(peers):
        result = result + jnp.dot(spread[t, :, :128], pool_rows[t], preferred_element_type=f32)
        result = result + jnp.dot(spread[t, :, 128:], state_rows[t], preferred_element_type=f32)
    return result.astype(bf16)[None]


def solution(mesh):
    in_specs = (
        P("fs", "sp", None),
        P(),
        P(("sp", "fs"), "tp"),
        P(("sp", "fs"), "tp"),
        P(("sp", "fs"), "tp"),
        P(("sp", "fs"), "tp"),
        P(("sp", "fs"), "tp"),
        P(("sp", "fs"), None),
        P(None, "tp"),
        P("tp"),
        P("tp", "sp"),
        P("tp"),
        P("fs", "tp", None, None),
        P("tp", None, None),
        P("tp"),
        P("sp", "tp"),
        P("sp", "tp"),
    )
    out_specs = P("fs", "sp", "tp")
    return jax.shard_map(body, mesh=mesh, in_specs=in_specs, out_specs=out_specs, check_vma=False)
```

time: 230 us -> 188 us (0.82)
  waiting for transfers between devices: 136 us -> 13.9 us
  starting transfers between devices: 2.34 us -> 59 us
  blocking collectives: 46.3 us -> 69.8 us
  other arithmetic: 10.3 us -> 1.92 us
  Pallas kernels: 0 us -> 5.75 us
    all_gather x3 -> x1, waiting for transfers between devices: 135 us -> 0.02 us  [body(): late = lax.all_gather(late, 'sp', axis=0, tiled=True)]
    ppermute x1 -> x14, starting transfers between devices: 2.22 us -> 59 us  [shifted(): return lax.ppermute(x, axis, pairs)]
    all_to_all x0 -> x1, blocking collectives: none -> 29.5 us  [body(): lax.all_to_all(jnp.broadcast_to(mine[None], (peers,) + mine.shape), 'tp',...]
    ppermute x1 -> x14, waiting for transfers between devices: 1.04 us -> 13.9 us  [shifted(): return lax.ppermute(x, axis, pairs)]
    all_gather x2 -> x1, blocking collectives: 46.3 us -> 40.3 us  [body(): early = lax.all_gather(early, 'sp', axis=0, tiled=True)]
    pallas_call x0 -> x1, Pallas kernels: none -> 5.75 us  [prepare(): pl.pallas_call(prep_kernel, grid_spec=pltpu.PrefetchScalarGridSpec(num_sc...]
    dynamic_update_slice x4 -> x0, other arithmetic: 2.56 us -> none  [body(): lax.scan(advance, zero_state, (block_states.transpose(2, 0, 1, 3, 4), blo...]
    dot_general x9 -> x30, matrix products: 12.1 us -> 13.5 us  [the longest x4 4.16 us: body(): jnp.dot(x, rest, preferred_element_type=f32)]
  transfers between devices with their start and end apart: 4 -> 15, of which waited for: 4 -> 8; matrix products, arithmetic and copies ran while one was open for 9% -> 7% of each run, Pallas kernels for 0% -> 3%
where the time goes in v1:
time: 188 us; the launch traced here: 186 us
  blocking collectives  69.8 us (37%)
  starting transfers between devices  59 us (31%)
  between operations  14.2 us (8%)
  waiting for transfers between devices  13.9 us (7%)
  matrix products  13.5 us (7%)
  local copies, waits for them, and re-layouts  7.85 us (4%)
  Pallas kernels  5.75 us (3%)
  other arithmetic  1.92 us (1%)
    ppermute x14, starting transfers between devices, shifted(): return lax.ppermute(x, axis, pairs)  59 us
    all_gather x1, blocking collectives, body(): early = lax.all_gather(early, 'sp', axis=0, tiled=True)  40.3 us
    all_to_all x1, blocking collectives, body(): lax.all_to_all(jnp.broadcast_to(mine[None], (peers,) + mine.shape), 'tp',...  29.5 us
    ppermute x14, waiting for transfers between devices, shifted(): return lax.ppermute(x, axis, pairs)  13.9 us
    pallas_call x1, Pallas kernels, prepare(): pl.pallas_call(prep_kernel, grid_spec=pltpu.PrefetchScalarGridSpec(num_sc...  5.75 us
    dot_general x4, matrix products, body(): jnp.dot(x, rest, preferred_element_type=f32)  4.16 us
  transfers between devices with their start and end apart: 15, of which 8 were waited for; matrix products, arithmetic and copies ran while one was open for 7% of the time, Pallas kernels for 3%

profile of v1, /device:TPU:1, one launch (start us, length us, event | category | flops | bytes accessed | tf_op | source)
XLA Modules:
  0.0 186.0 jit_solution(11030274826034927387)
XLA Ops:
  11.1 5.7 %prep.1 = (bf16[256,1024]{1,0:T(8,128)(2,1)}, bf16[256,1024]{1,0:T(8,128)(2,1)}, bf16[256,1024]{1,0:T(8,128)(2,1)}, bf16[256,1024]{1,0:T(8,128)(2,1)}, f32[256,128]{1,0:T(8,128)}) custom-call(s32[1]{0:T(128)} %bitcast.own, bf16[256,4096]{1,0:T(8,128)(2,1)} %bitcast.173, f32[1,4096]{1,0:T(1,128)} %bitcast.184), custom_call_target="tpu_custom_call" | custom-call | tf_op jit(solution)/shard_map/prep/pallas_call | solution.py:61
  16.9 4.1 %collective-permute-start = (bf16[256,1024]{1,0:T(8,128)(2,1)}, bf16[256,1024]{1,0:T(8,128)(2,1)S(1)}, u32[]{:S(2)}, u32[]{:S(2)}) collective-permute-start(bf16[256,1024]{1,0:T(8,128)(2,1)} %get-tuple-element.11), channel_id=1, source_target_pairs={{0,8},{8,16},{16,24},{24,0},{1,9},{9,17},{17,25},{25,1},{2,10},{10... | collective-permute-start | bytes 1572872 | tf_op jit(solution)/shard_map/exchange/ppermute | solution.py:24
  21.0 4.6 %collective-permute-start.2 = (bf16[256,1024]{1,0:T(8,128)(2,1)}, bf16[256,1024]{1,0:T(8,128)(2,1)S(1)}, u32[]{:S(2)}, u32[]{:S(2)}) collective-permute-start(bf16[256,1024]{1,0:T(8,128)(2,1)} %get-tuple-element.12), channel_id=1, source_target_pairs={{0,16},{8,24},{16,0},{24,8},{1,17},{9,25},{17,1},{25,9},{2,18},{10... | collective-permute-start | bytes 1572872 | tf_op jit(solution)/shard_map/exchange/ppermute | solution.py:24
  25.6 2.9 %collective-permute-start.4 = (bf16[256,1024]{1,0:T(8,128)(2,1)}, bf16[256,1024]{1,0:T(8,128)(2,1)S(1)}, u32[]{:S(2)}, u32[]{:S(2)}) collective-permute-start(bf16[256,1024]{1,0:T(8,128)(2,1)} %get-tuple-element.13), channel_id=1, source_target_pairs={{0,24},{8,0},{16,8},{24,16},{1,25},{9,1},{17,9},{25,17},{2,26},{10... | collective-permute-start | bytes 1572872 | tf_op jit(solution)/shard_map/exchange/ppermute | solution.py:24
  29.2 40.3 %all_gather.7 = bf16[1024,320]{1,0:T(8,128)(2,1)S(1)} all-gather(bf16[64,320]{1,0:T(8,128)(2,1)S(1)} %pad_maximum_fusion.3), channel_id=1, replica_groups=mesh['sp'=16,'fs'=4,'tp'=8] {'sp'}, dimensions={0}, use_global_device_ids=true | all-gather | bytes 696320 | tf_op jit(solution)/shard_map/early/all_gather | solution.py:157
  69.5 1.5 fusion.73
  71.5 2.6 %collective-permute-start.7 = (bf16[256,320]{0,1:T(8,128)(2,1)S(1)}, bf16[256,320]{0,1:T(8,128)(2,1)S(1)}, u32[]{:S(2)}, u32[]{:S(2)}) collective-permute-start(bf16[256,320]{0,1:T(8,128)(2,1)S(1)} %convolution_convert_fusion.5), channel_id=1, source_target_pairs={{0,24},{8,0},{16,8},{24,16},{1,25},{9,1},{17,9},{25,17},{2,26},{10... | collective-permute-start | bytes 491528 | tf_op jit(solution)/shard_map/ppermute | solution.py:24
  74.6 3.2 %collective-permute-start.8 = (bf16[256,320]{0,1:T(8,128)(2,1)S(1)}, bf16[256,320]{0,1:T(8,128)(2,1)S(1)}, u32[]{:S(2)}, u32[]{:S(2)}) collective-permute-start(bf16[256,320]{0,1:T(8,128)(2,1)S(1)} %convolution_convert_fusion.4), channel_id=1, source_target_pairs={{0,16},{8,24},{16,0},{24,8},{1,17},{9,25},{17,1},{25,9},{2,18},{10... | collective-permute-start | bytes 491528 | tf_op jit(solution)/shard_map/ppermute | solution.py:24
  78.3 1.9 %collective-permute-start.9 = (bf16[256,320]{0,1:T(8,128)(2,1)S(1)}, bf16[256,320]{0,1:T(8,128)(2,1)S(1)}, u32[]{:S(2)}, u32[]{:S(2)}) collective-permute-start(bf16[256,320]{0,1:T(8,128)(2,1)S(1)} %convolution_convert_fusion.3), channel_id=1, source_target_pairs={{0,8},{8,16},{16,24},{24,0},{1,9},{9,17},{17,25},{25,1},{2,10},{10... | collective-permute-start | bytes 491528 | tf_op jit(solution)/shard_map/ppermute | solution.py:24
  80.6 1.6 collective-permute-done.8
  82.2 3.4 %collective-permute-done.9 = bf16[256,320]{0,1:T(8,128)(2,1)S(1)} collective-permute-done((bf16[256,320]{0,1:T(8,128)(2,1)S(1)}, bf16[256,320]{0,1:T(8,128)(2,1)S(1)}, u32[]{:S(2)}, u32[]{:S(2)}) %collective-permute-start.9) | collective-permute-done | bytes 163872 | tf_op jit(solution)/shard_map/ppermute | solution.py:24
  89.0 2.2 %collective-permute-start.10 = (f32[72,128]{1,0:T(8,128)S(1)}, f32[72,128]{1,0:T(8,128)S(1)}, u32[]{:S(2)}, u32[]{:S(2)}) collective-permute-start(f32[72,128]{1,0:T(8,128)S(1)} %maximum_maximum_fusion), channel_id=1, source_target_pairs={{0,32},{32,64},{64,96},{96,128},{128,160},{160,192},{192,224},{224... | collective-permute-start | bytes 110600 | tf_op jit(solution)/shard_map/scan/ppermute | solution.py:24
  92.2 5.0 %collective-permute-start.11 = (f32[72,128]{1,0:T(8,128)S(1)}, f32[72,128]{1,0:T(8,128)S(1)}, u32[]{:S(2)}, u32[]{:S(2)}) collective-permute-start(f32[72,128]{1,0:T(8,128)S(1)} %pad_maximum_fusion.4), channel_id=1, source_target_pairs={{0,64},{32,96},{64,128},{96,160},{128,192},{160,224},{192,256},{22... | collective-permute-start | bytes 110600 | tf_op jit(solution)/shard_map/scan/ppermute | solution.py:24
  98.3 9.4 %collective-permute-start.12 = (f32[72,128]{1,0:T(8,128)S(1)}, f32[72,128]{1,0:T(8,128)S(1)}, u32[]{:S(2)}, u32[]{:S(2)}) collective-permute-start(f32[72,128]{1,0:T(8,128)S(1)} %pad_maximum_fusion.5), channel_id=1, source_target_pairs={{0,128},{32,160},{64,192},{96,224},{128,256},{160,288},{192,320},{... | collective-permute-start | bytes 110600 | tf_op jit(solution)/shard_map/scan/ppermute | solution.py:24
  108.8 12.6 %collective-permute-start.13 = (f32[72,128]{1,0:T(8,128)S(1)}, f32[72,128]{1,0:T(8,128)S(1)}, u32[]{:S(2)}, u32[]{:S(2)}) collective-permute-start(f32[72,128]{1,0:T(8,128)S(1)} %pad_maximum_fusion.6), channel_id=1, source_target_pairs={{0,256},{32,288},{64,320},{96,352},{128,384},{160,416},{192,448},{... | collective-permute-start | bytes 110600 | tf_op jit(solution)/shard_map/scan/ppermute | solution.py:24
  122.8 1.7 convolution_convert_fusion.2
  124.5 2.0 %collective-permute-start.1 = (bf16[256,384]{1,0:T(8,128)(2,1)S(1)}, bf16[256,384]{1,0:T(8,128)(2,1)S(1)}, u32[]{:S(2)}, u32[]{:S(2)}) collective-permute-start(bf16[256,384]{1,0:T(8,128)(2,1)S(1)} %convolution_convert_fusion.2), channel_id=1, source_target_pairs={{0,24},{8,0},{16,8},{24,16},{1,25},{9,1},{17,9},{25,17},{2,26},{10... | collective-permute-start | bytes 589832 | tf_op jit(solution)/shard_map/ppermute | solution.py:24
  126.5 1.6 convolution_convert_fusion.1
  128.0 1.9 %collective-permute-start.3 = (bf16[256,384]{1,0:T(8,128)(2,1)S(1)}, bf16[256,384]{1,0:T(8,128)(2,1)S(1)}, u32[]{:S(2)}, u32[]{:S(2)}) collective-permute-start(bf16[256,384]{1,0:T(8,128)(2,1)S(1)} %convolution_convert_fusion.1), channel_id=1, source_target_pairs={{0,16},{8,24},{16,0},{24,8},{1,17},{9,25},{17,1},{25,9},{2,18},{10... | collective-permute-start | bytes 589832 | tf_op jit(solution)/shard_map/ppermute | solution.py:24
  130.4 3.3 %collective-permute-start.5 = (bf16[256,384]{1,0:T(8,128)(2,1)S(1)}, bf16[256,384]{1,0:T(8,128)(2,1)S(1)}, u32[]{:S(2)}, u32[]{:S(2)}) collective-permute-start(bf16[256,384]{1,0:T(8,128)(2,1)S(1)} %convolution_convert_fusion), channel_id=1, source_target_pairs={{0,8},{8,16},{16,24},{24,0},{1,9},{9,17},{17,25},{25,1},{2,10},{10... | collective-permute-start | bytes 589832 | tf_op jit(solution)/shard_map/ppermute | solution.py:24
  134.2 1.7 collective-permute-done.3
  136.0 3.2 %collective-permute-done.5 = bf16[256,384]{1,0:T(8,128)(2,1)S(1)} collective-permute-done((bf16[256,384]{1,0:T(8,128)(2,1)S(1)}, bf16[256,384]{1,0:T(8,128)(2,1)S(1)}, u32[]{:S(2)}, u32[]{:S(2)}) %collective-permute-start.5) | collective-permute-done | bytes 196640 | tf_op jit(solution)/shard_map/ppermute | solution.py:24
  139.4 3.3 %collective-permute-start.6 = (bf16[15,128]{1,0:T(8,128)(2,1)S(1)}, bf16[15,128]{1,0:T(8,128)(2,1)S(1)}, u32[]{:S(2)}, u32[]{:S(2)}) collective-permute-start(bf16[15,128]{1,0:T(8,128)(2,1)S(1)} %slice.350), channel_id=1, source_target_pairs={{0,32},{32,64},{64,96},{96,128},{128,160},{160,192},{192,224},{224... | collective-permute-start | bytes 11528 | tf_op jit(solution)/shard_map/ppermute | solution.py:24
  145.4 29.5 %all_to_all.5 = bf16[8,256,256]{2,1,0:T(8,128)(2,1)S(1)} all-to-all(bf16[8,256,256]{2,1,0:T(8,128)(2,1)S(1)} %broadcast_in_dim.25), channel_id=1, replica_groups=mesh['sp'=16,'fs'=4,'tp'=8] {'tp'}, dimensions={0} | all-to-all | bytes 2097152 | tf_op jit(solution)/shard_map/all_to_all | solution.py:255
  (131 shorter events, 22.5 us)
Async XLA Ops:
  6.5 138.5 %copy-start = (bf16[1,128,128]{2,1,0:T(8,128)(2,1)S(1)}, bf16[1,128,128]{2,1,0:T(8,128)(2,1)}, u32[]{:S(2)}) copy-start(bf16[1,128,128]{2,1,0:T(8,128)(2,1)} %param.30) | copy-start | bytes 98308
  6.5 116.2 %all-gather.2.cloned.1.call-start = ((), (), s32[]{:S(2)}) async-start(), calls=%async_computation.1 | async-start | bytes 3063808 | tf_op jit(solution)/shard_map/all_gather | solution.py:149
  16.9 54.2 %collective-permute-start = (bf16[256,1024]{1,0:T(8,128)(2,1)}, bf16[256,1024]{1,0:T(8,128)(2,1)S(1)}, u32[]{:S(2)}, u32[]{:S(2)}) collective-permute-start(bf16[256,1024]{1,0:T(8,128)(2,1)} %get-tuple-element.11), channel_id=1, source_target_pairs={{0,8},{8,16},{16,24},{24,0},{1,9},{9,17},{17,25},{25,1},{2,10},{10... | collective-permute-start | bytes 1572872 | tf_op jit(solution)/shard_map/exchange/ppermute | solution.py:24
  21.0 53.2 %collective-permute-start.2 = (bf16[256,1024]{1,0:T(8,128)(2,1)}, bf16[256,1024]{1,0:T(8,128)(2,1)S(1)}, u32[]{:S(2)}, u32[]{:S(2)}) collective-permute-start(bf16[256,1024]{1,0:T(8,128)(2,1)} %get-tuple-element.12), channel_id=1, source_target_pairs={{0,16},{8,24},{16,0},{24,8},{1,17},{9,25},{17,1},{25,9},{2,18},{10... | collective-permute-start | bytes 1572872 | tf_op jit(solution)/shard_map/exchange/ppermute | solution.py:24
  25.6 52.2 %collective-permute-start.4 = (bf16[256,1024]{1,0:T(8,128)(2,1)}, bf16[256,1024]{1,0:T(8,128)(2,1)S(1)}, u32[]{:S(2)}, u32[]{:S(2)}) collective-permute-start(bf16[256,1024]{1,0:T(8,128)(2,1)} %get-tuple-element.13), channel_id=1, source_target_pairs={{0,24},{8,0},{16,8},{24,16},{1,25},{9,1},{17,9},{25,17},{2,26},{10... | collective-permute-start | bytes 1572872 | tf_op jit(solution)/shard_map/exchange/ppermute | solution.py:24
  69.5 10.7 %copy-start.7 = (f32[2,256]{1,0:T(2,128)S(1)}, f32[2,256]{1,0:T(2,128)}, u32[]{:S(2)}) copy-start(f32[2,256]{1,0:T(2,128)} %param.27) | copy-start | bytes 6148
  69.5 10.9 %copy-start.5 = (f32[256,128]{1,0:T(8,128)S(1)}, f32[256,128]{1,0:T(8,128)}, u32[]{:S(2)}) copy-start(f32[256,128]{1,0:T(8,128)} %get-tuple-element.14) | copy-start | bytes 393220
  71.1 14.6 %copy-start.9 = (bf16[64,128]{1,0:T(8,128)(2,1)S(1)}, bf16[64,128]{1,0:T(8,128)(2,1)}, u32[]{:S(2)}) copy-start(bf16[64,128]{1,0:T(8,128)(2,1)} %param.25) | copy-start | bytes 49156
  71.1 14.6 %copy-start.10 = (f32[128]{0:T(128)S(1)}, f32[128]{0:T(128)}, u32[]{:S(2)}) copy-start(f32[128]{0:T(128)} %param.26) | copy-start | bytes 1540
  71.5 9.0 %collective-permute-start.7 = (bf16[256,320]{0,1:T(8,128)(2,1)S(1)}, bf16[256,320]{0,1:T(8,128)(2,1)S(1)}, u32[]{:S(2)}, u32[]{:S(2)}) collective-permute-start(bf16[256,320]{0,1:T(8,128)(2,1)S(1)} %convolution_convert_fusion.5), channel_id=1, source_target_pairs={{0,24},{8,0},{16,8},{24,16},{1,25},{9,1},{17,9},{25,17},{2,26},{10... | collective-permute-start | bytes 491528 | tf_op jit(solution)/shard_map/ppermute | solution.py:24
  74.6 7.6 %collective-permute-start.8 = (bf16[256,320]{0,1:T(8,128)(2,1)S(1)}, bf16[256,320]{0,1:T(8,128)(2,1)S(1)}, u32[]{:S(2)}, u32[]{:S(2)}) collective-permute-start(bf16[256,320]{0,1:T(8,128)(2,1)S(1)} %convolution_convert_fusion.4), channel_id=1, source_target_pairs={{0,16},{8,24},{16,0},{24,8},{1,17},{9,25},{17,1},{25,9},{2,18},{10... | collective-permute-start | bytes 491528 | tf_op jit(solution)/shard_map/ppermute | solution.py:24
  78.3 7.3 %collective-permute-start.9 = (bf16[256,320]{0,1:T(8,128)(2,1)S(1)}, bf16[256,320]{0,1:T(8,128)(2,1)S(1)}, u32[]{:S(2)}, u32[]{:S(2)}) collective-permute-start(bf16[256,320]{0,1:T(8,128)(2,1)S(1)} %convolution_convert_fusion.3), channel_id=1, source_target_pairs={{0,8},{8,16},{16,24},{24,0},{1,9},{9,17},{17,25},{25,1},{2,10},{10... | collective-permute-start | bytes 491528 | tf_op jit(solution)/shard_map/ppermute | solution.py:24
  80.5 10.7 %copy-start.6 = (f32[1,2,64,64]{3,2,1,0:T(8,128)S(1)}, f32[1,2,64,64]{3,2,1,0:T(8,128)}, u32[]{:S(2)}) copy-start(f32[1,2,64,64]{3,2,1,0:T(8,128)} %param.29) | copy-start | bytes 98308
  89.0 3.2 %collective-permute-start.10 = (f32[72,128]{1,0:T(8,128)S(1)}, f32[72,128]{1,0:T(8,128)S(1)}, u32[]{:S(2)}, u32[]{:S(2)}) collective-permute-start(f32[72,128]{1,0:T(8,128)S(1)} %maximum_maximum_fusion), channel_id=1, source_target_pairs={{0,32},{32,64},{64,96},{96,128},{128,160},{160,192},{192,224},{224... | collective-permute-start | bytes 110600 | tf_op jit(solution)/shard_map/scan/ppermute | solution.py:24
  92.2 6.1 %collective-permute-start.11 = (f32[72,128]{1,0:T(8,128)S(1)}, f32[72,128]{1,0:T(8,128)S(1)}, u32[]{:S(2)}, u32[]{:S(2)}) collective-permute-start(f32[72,128]{1,0:T(8,128)S(1)} %pad_maximum_fusion.4), channel_id=1, source_target_pairs={{0,64},{32,96},{64,128},{96,160},{128,192},{160,224},{192,256},{22... | collective-permute-start | bytes 110600 | tf_op jit(solution)/shard_map/scan/ppermute | solution.py:24
  98.3 10.4 %collective-permute-start.12 = (f32[72,128]{1,0:T(8,128)S(1)}, f32[72,128]{1,0:T(8,128)S(1)}, u32[]{:S(2)}, u32[]{:S(2)}) collective-permute-start(f32[72,128]{1,0:T(8,128)S(1)} %pad_maximum_fusion.5), channel_id=1, source_target_pairs={{0,128},{32,160},{64,192},{96,224},{128,256},{160,288},{192,320},{... | collective-permute-start | bytes 110600 | tf_op jit(solution)/shard_map/scan/ppermute | solution.py:24
  108.8 13.6 %collective-permute-start.13 = (f32[72,128]{1,0:T(8,128)S(1)}, f32[72,128]{1,0:T(8,128)S(1)}, u32[]{:S(2)}, u32[]{:S(2)}) collective-permute-start(f32[72,128]{1,0:T(8,128)S(1)} %pad_maximum_fusion.6), channel_id=1, source_target_pairs={{0,256},{32,288},{64,320},{96,352},{128,384},{160,416},{192,448},{... | collective-permute-start | bytes 110600 | tf_op jit(solution)/shard_map/scan/ppermute | solution.py:24
  122.6 11.2 %copy-start.3 = (bf16[256,1024]{1,0:T(8,128)(2,1)S(1)}, bf16[256,1024]{1,0:T(8,128)(2,1)}, u32[]{:S(2)}) copy-start(bf16[256,1024]{1,0:T(8,128)(2,1)} %get-tuple-element.10) | copy-start | bytes 1572868
  122.8 7.2 %copy-start.1 = (bf16[1024,1408]{1,0:T(8,128)(2,1)S(1)}, bf16[1024,1408]{1,0:T(8,128)(2,1)}, u32[]{:S(2)}) copy-start(bf16[1024,1408]{1,0:T(8,128)(2,1)} %all-gather.2.cloned.1.call-done) | copy-start | bytes 8650756
  124.5 9.7 %collective-permute-start.1 = (bf16[256,384]{1,0:T(8,128)(2,1)S(1)}, bf16[256,384]{1,0:T(8,128)(2,1)S(1)}, u32[]{:S(2)}, u32[]{:S(2)}) collective-permute-start(bf16[256,384]{1,0:T(8,128)(2,1)S(1)} %convolution_convert_fusion.2), channel_id=1, source_target_pairs={{0,24},{8,0},{16,8},{24,16},{1,25},{9,1},{17,9},{25,17},{2,26},{10... | collective-permute-start | bytes 589832 | tf_op jit(solution)/shard_map/ppermute | solution.py:24
  128.0 7.9 %collective-permute-start.3 = (bf16[256,384]{1,0:T(8,128)(2,1)S(1)}, bf16[256,384]{1,0:T(8,128)(2,1)S(1)}, u32[]{:S(2)}, u32[]{:S(2)}) collective-permute-start(bf16[256,384]{1,0:T(8,128)(2,1)S(1)} %convolution_convert_fusion.1), channel_id=1, source_target_pairs={{0,16},{8,24},{16,0},{24,8},{1,17},{9,25},{17,1},{25,9},{2,18},{10... | collective-permute-start | bytes 589832 | tf_op jit(solution)/shard_map/ppermute | solution.py:24
  130.4 8.8 %collective-permute-start.5 = (bf16[256,384]{1,0:T(8,128)(2,1)S(1)}, bf16[256,384]{1,0:T(8,128)(2,1)S(1)}, u32[]{:S(2)}, u32[]{:S(2)}) collective-permute-start(bf16[256,384]{1,0:T(8,128)(2,1)S(1)} %convolution_convert_fusion), channel_id=1, source_target_pairs={{0,8},{8,16},{16,24},{24,0},{1,9},{9,17},{17,25},{25,1},{2,10},{10... | collective-permute-start | bytes 589832 | tf_op jit(solution)/shard_map/ppermute | solution.py:24
  139.4 5.6 %collective-permute-start.6 = (bf16[15,128]{1,0:T(8,128)(2,1)S(1)}, bf16[15,128]{1,0:T(8,128)(2,1)S(1)}, u32[]{:S(2)}, u32[]{:S(2)}) collective-permute-start(bf16[15,128]{1,0:T(8,128)(2,1)S(1)} %slice.350), channel_id=1, source_target_pairs={{0,32},{32,64},{64,96},{96,128},{128,160},{160,192},{192,224},{224... | collective-permute-start | bytes 11528 | tf_op jit(solution)/shard_map/ppermute | solution.py:24
  145.0 29.9 %copy-start.2 = (bf16[1024,1408]{1,0:T(8,128)(2,1)S(1)}, bf16[1024,1408]{1,0:T(8,128)(2,1)}, u32[]{:S(2)}) copy-start(bf16[1024,1408]{1,0:T(8,128)(2,1)} %all-gather.2.cloned.1.call-done) | copy-start | bytes 8650756
  (3 other events, 8.4 us)
Sparse Core Ops, SparseCore 0:
  11.2 74.7 all-gather.1

commit v2 on v1

v2 whole, which is shorter than its diff:
```python
import jax
import jax.numpy as jnp
from jax import lax
from jax.experimental import pallas as pl
from jax.experimental.pallas import tpu as pltpu
from jax.sharding import PartitionSpec as P

BLOCK = 64
HEAD = 64
LANES = 128
HALO = 16
RUN_ROWS = 72
norm_eps = 1e-06
decay_temper = 16.0
highest = lax.Precision.HIGHEST
f32 = jnp.float32
bf16 = jnp.bfloat16


def shifted(x, axis, by, wrap):
    n = lax.axis_size(axis)
    if wrap:
        pairs = [(i, (i + by) % n) for i in range(n)]
    else:
        pairs = [(i, i + by) for i in range(n) if 0 <= i + by < n]
    return lax.ppermute(x, axis, pairs)


def call(kernel, outs, name, *args, scalars=1):
    smem = pl.BlockSpec(memory_space=pltpu.SMEM)
    vmem = pl.BlockSpec(memory_space=pltpu.VMEM)
    return pl.pallas_call(
        kernel,
        in_specs=[smem] * scalars + [vmem] * (len(args) - scalars),
        out_specs=[vmem] * len(outs),
        out_shape=outs,
        name=name,
    )(*args)


def struct(shape, dtype):
    return jax.ShapeDtypeStruct(shape, dtype)


def pack_kernel(key, value, pool, low, query, gate, pool_rows, state_rows, early, late):
    for out, refs in ((early, (key, value, pool, low)), (late, (query, gate, pool_rows, state_rows))):
        at = 0
        for r in refs:
            out[:, at : at + r.shape[1]] = r[...]
            at += r.shape[1]


def prep_kernel(own, act, gain, x0, x1, x2, x3, inverse):
    rows, width = act.shape
    outs = (x0, x1, x2, x3)
    half = lax.broadcasted_iota(jnp.int32, (rows, LANES), 1) < HEAD

    for f in range(4):

        @pl.when(own[0] == f)
        def _(f=f):
            squares = jnp.zeros((rows, LANES), f32)
            for p in range(width // 512):
                tiles = []
                for q in range(4):
                    at = p * 512 + q * LANES
                    t = act[:, at : at + LANES].astype(f32)
                    squares = squares + t * t
                    tiles.append(t * gain[:, at : at + LANES])
                blocks = []
                for a, b in ((tiles[0], tiles[2]), (tiles[1], tiles[3])):
                    blocks.append(jnp.where(half, a, pltpu.roll(b, HEAD, 1)).astype(bf16))
                    blocks.append(jnp.where(half, pltpu.roll(a, HEAD, 1), b).astype(bf16))
                for k in range(4):
                    outs[k][:, p * LANES : (p + 1) * LANES] = blocks[(f + k) % 4]
            total = jnp.sum(squares, axis=1, keepdims=True)
            inverse[...] = jnp.broadcast_to(lax.rsqrt(total / width + norm_eps), (rows, LANES))


def prepare(act, gain, own):
    tokens, width = act.shape
    rows = 64
    part = pl.BlockSpec((rows, width // 4), lambda i, own: (i, 0))
    return pl.pallas_call(
        prep_kernel,
        grid_spec=pltpu.PrefetchScalarGridSpec(
            num_scalar_prefetch=1,
            grid=(tokens // rows,),
            in_specs=[
                pl.BlockSpec((rows, width), lambda i, own: (i, 0)),
                pl.BlockSpec((1, width), lambda i, own: (0, 0)),
            ],
            out_specs=[part, part, part, part, pl.BlockSpec((rows, LANES), lambda i, own: (i, 0))],
        ),
        out_shape=[struct((tokens, width // 4), bf16)] * 4 + [struct((tokens, LANES), f32)],
        name="prep",
    )(own, act, gain)


def partial_kernel(own, x0, x1, x2, x3, w, out):
    tokens = x0.shape[0]
    wide = out.shape[1] // tokens * LANES
    columns = out.shape[1] * LANES // tokens
    half = lax.broadcasted_iota(jnp.int32, (tokens // 2, LANES), 1) < HEAD
    weight = w[:, :columns]
    for k, x in enumerate((x0, x1, x2, x3)):
        target = (own[0] - k + 4) % 4
        p = jnp.dot(x[...], weight, preferred_element_type=f32)
        for j in range(wide // LANES):
            out[target, j * tokens : (j + 1) * tokens] = p[:, j * LANES : (j + 1) * LANES].astype(bf16)
        if columns > wide:
            d = jnp.concatenate([p[:, wide:], p[:, wide:]], axis=1)
            d = jnp.where(half, d[: tokens // 2], d[tokens // 2 :])
            out[target, wide // LANES * tokens :] = d.astype(bf16)


def partials(own, xs, w, columns, name):
    tokens, _ = xs[0].shape
    (out,) = call(
        partial_kernel,
        [struct((4, tokens * columns // LANES, LANES), bf16)],
        name,
        own,
        *xs,
        w,
    )
    return out


def total_of(parts, at, rows):
    s = parts[0, at : at + rows].astype(f32)
    for k in (1, 2, 3):
        s = s + parts[k, at : at + rows].astype(f32)
    return s


def projected(parts, inverse, j):
    tokens = inverse.shape[0]
    return (total_of(parts, j * tokens, tokens) * inverse).astype(bf16)


def heads_of(x, half):
    return jnp.where(half, x[:HEAD], x[HEAD:])


def local_kernel(
    parts, inverse, second, bias, extra, keys, values, pool, tail, sums, prior, opening, run
):
    inv = inverse[...]
    tokens = inv.shape[0]
    keys[...] = projected(parts, inv, 0).astype(f32)
    values[...] = projected(parts, inv, 1).astype(f32)
    pooled = projected(parts, inv, 2)
    pool[...] = pooled
    tail[...] = pooled[tokens - HALO :]
    both = total_of(parts, 3 * tokens, tokens // 2)
    low = jnp.concatenate([both[:, :HEAD], both[:, HEAD:]], axis=0)
    low = (low * inv[:, :HEAD]).astype(bf16)
    x = jnp.dot(low, second[...], preferred_element_type=f32) + bias[...]
    rates = (jnp.minimum(x, 0.0) - jnp.log1p(jnp.exp(-jnp.abs(x)))) / decay_temper
    wide = lax.broadcasted_iota(jnp.int32, (2, LANES), 1) // HEAD
    pick = (wide == lax.broadcasted_iota(jnp.int32, (2, LANES), 0)).astype(f32)
    rates = rates + lax.dot_general(
        extra[...], pick, (((0,), (0,)), ((), ())), precision=highest, preferred_element_type=f32
    )
    r = lax.broadcasted_iota(jnp.int32, (BLOCK, BLOCK), 0)
    c = lax.broadcasted_iota(jnp.int32, (BLOCK, BLOCK), 1)
    lower = (r >= c).astype(f32)
    half = lax.broadcasted_iota(jnp.int32, (HEAD, LANES), 1) < HEAD
    state = jnp.zeros((HEAD, LANES), f32)
    before = jnp.zeros((1, LANES), f32)
    for n in range(tokens // BLOCK):
        at = slice(n * BLOCK, (n + 1) * BLOCK)
        total = jnp.dot(lower, rates[at], precision=highest, preferred_element_type=f32)
        sums[at] = total
        final = total[BLOCK - 1 :]
        pairs = lax.dot_general(
            values[at],
            keys[at] * jnp.exp(final - total),
            (((0,), (0,)), ((), ())),
            precision=highest,
            preferred_element_type=f32,
        )
        prior[at] = state
        opening[n : n + 1] = before
        state = jnp.exp(final) * state + heads_of(pairs, half)
        before = before + final
    run[:HEAD] = state
    run[HEAD:] = jnp.broadcast_to(before, (RUN_ROWS - HEAD, LANES))


def finish_kernel(
    where,
    runs,
    start,
    parts,
    inverse,
    keys,
    values,
    sums,
    prior,
    opening,
    gain,
    pool,
    previous,
    pool_weight,
    pool_scale,
    mine,
):
    inv = inverse[...]
    tokens = inv.shape[0]
    place = where[0]
    state = start[...]
    for j in range(runs.shape[0] // RUN_ROWS):
        at = j * RUN_ROWS
        log = runs[at + HEAD : at + HEAD + 1]
        folded = jnp.exp(log) * state + runs[at : at + HEAD]
        state = jnp.where(j < place, folded, state)
    queries = projected(parts, inv, 0).astype(f32) * HEAD ** (-0.5)
    outgate = projected(parts, inv, 1).astype(f32)
    half = lax.broadcasted_iota(jnp.int32, (HEAD, LANES), 1) < HEAD
    r = lax.broadcasted_iota(jnp.int32, (2 * BLOCK, BLOCK), 0) % BLOCK
    c = lax.broadcasted_iota(jnp.int32, (2 * BLOCK, BLOCK), 1)
    causal = r >= c

    def split(x):
        return jnp.concatenate([jnp.where(half, x, 0.0), jnp.where(half, 0.0, x)], axis=0)

    last = (((1,), (1,)), ((), ()))
    for n in range(tokens // BLOCK):
        at = slice(n * BLOCK, (n + 1) * BLOCK)
        total = sums[at]
        middle = total[BLOCK // 2 - 1 : BLOCK // 2]
        q = queries[at]
        scores = lax.dot_general(
            split(q * jnp.exp(total - middle)),
            keys[at] * jnp.exp(middle - total),
            last,
            precision=highest,
            preferred_element_type=f32,
        )
        scores = jnp.where(causal, scores, 0.0)
        within = jnp.dot(scores, values[at], precision=highest, preferred_element_type=f32)
        begin = prior[at] + jnp.exp(opening[n : n + 1]) * state
        carried = lax.dot_general(
            split(q * jnp.exp(total)),
            jnp.concatenate([begin, begin], axis=0),
            last,
            precision=highest,
            preferred_element_type=f32,
        )
        raw = heads_of(within + carried, half)
        square = raw * raw
        first = jnp.sum(jnp.where(half, square, 0.0), axis=1, keepdims=True)
        second = jnp.sum(jnp.where(half, 0.0, square), axis=1, keepdims=True)
        mean = jnp.where(half, first, second) / HEAD
        g = outgate[at]
        scaled = raw * lax.rsqrt(mean + norm_eps) * gain[...]
        mine[at, LANES:] = (scaled * (g / (1.0 + jnp.exp(-g)))).astype(bf16)

    current = pool[...].astype(f32)
    extended = jnp.concatenate([previous[...].astype(f32), current], axis=0)

    def back(x, by):
        return x + pltpu.roll(x, by, 0)

    two = back(extended, 1)
    four = back(two, 2)
    eight = back(four, 4)
    sixteen = back(eight, 8)
    level = where[1] % 4
    chosen = jnp.where(
        level == 0, two, jnp.where(level == 1, four, jnp.where(level == 2, eight, sixteen))
    )[HALO:]
    window = jnp.where(
        level == 0, 2.0, jnp.where(level == 1, 4.0, jnp.where(level == 2, 8.0, 16.0))
    )
    position = place * tokens + lax.broadcasted_iota(jnp.int32, (tokens, LANES), 0)
    counts = jnp.minimum(position.astype(f32) + 1.0, window)
    deviation = (chosen / counts - current).astype(bf16)
    mixture = jnp.dot(deviation, pool_weight[...], preferred_element_type=f32)
    mine[:, :LANES] = (mixture * pool_scale[...]).astype(bf16)


def output_kernel(core, same, other, late, out):
    first = 2 * LANES
    width = out.shape[1]
    total = jnp.zeros(out.shape, f32)
    for x in range(same.shape[0]):
        for z, c in ((same, core[0]), (other, 1 - core[0])):
            rows = pl.ds((2 * x + c) * LANES, LANES)
            total = total + jnp.dot(
                z[x, :, :LANES], late[rows, first : first + width], preferred_element_type=f32
            )
            total = total + jnp.dot(
                z[x, :, LANES:], late[rows, first + width :], preferred_element_type=f32
            )
    out[...] = total.astype(bf16)


def body(
    activations,
    input_norm_gain,
    pooling_channel_weight,
    query_projection_weight,
    key_projection_weight,
    value_projection_weight,
    output_gate_weight,
    decay_first_factor,
    decay_second_factor,
    decay_gate_bias,
    decay_extra_log,
    head_norm_gain,
    starting_state,
    pooling_group_weight,
    pooling_channel_scale,
    pooling_output_rows,
    attention_output_rows,
):
    _, tokens, width = activations.shape
    rows = key_projection_weight.shape[0]
    columns = pooling_output_rows.shape[1]
    own = lax.axis_index("fs").astype(jnp.int32).reshape(1)
    tp = lax.axis_index("tp").astype(jnp.int32)
    early, late = call(
        pack_kernel,
        [struct((rows, 3 * LANES + HEAD), bf16), struct((rows, 2 * LANES + 2 * columns), bf16)],
        "pack",
        key_projection_weight,
        value_projection_weight,
        pooling_channel_weight,
        decay_first_factor,
        query_projection_weight,
        output_gate_weight,
        pooling_output_rows,
        attention_output_rows,
        scalars=0,
    )
    late = lax.all_gather(late, "sp", axis=0, tiled=True)
    x0, x1, x2, x3, inverse = prepare(
        activations.reshape(tokens, width), input_norm_gain.reshape(1, width), own
    )
    with jax.named_scope("early"):
        early = lax.all_gather(early, "sp", axis=0, tiled=True)
    with jax.named_scope("exchange"):
        x1 = shifted(x1, "fs", 1, True)
        x2 = shifted(x2, "fs", 2, True)
        x3 = shifted(x3, "fs", 3, True)
    xs = (x0, x1, x2, x3)
    parts = partials(own, xs, early, early.shape[1], "early_parts")
    parts = lax.all_to_all(parts, "fs", 0, 0)
    wide = struct((tokens, LANES), f32)
    keys, values, pool, tail, sums, prior, opening, run = call(
        local_kernel,
        [
            wide,
            wide,
            struct((tokens, LANES), bf16),
            struct((HALO, LANES), bf16),
            wide,
            wide,
            struct((tokens // BLOCK, LANES), f32),
            struct((RUN_ROWS, LANES), f32),
        ],
        "local",
        parts,
        inverse,
        decay_second_factor,
        decay_gate_bias.reshape(1, LANES),
        decay_extra_log,
        scalars=0,
    )
    with jax.named_scope("halo"):
        previous = shifted(tail, "sp", 1, False)
    with jax.named_scope("states"):
        runs = lax.all_gather(run, "sp", axis=0, tiled=True)
    start = starting_state[0].transpose(2, 0, 1).reshape(HEAD, LANES)
    late, runs = lax.optimization_barrier((late, runs))
    parts = partials(own, xs, late, 2 * LANES, "late_parts")
    parts = lax.all_to_all(parts, "fs", 0, 0)
    (mine,) = call(
        finish_kernel,
        [struct((tokens, 2 * LANES), bf16)],
        "finish",
        jnp.stack([lax.axis_index("sp").astype(jnp.int32), tp]),
        runs,
        start,
        parts,
        inverse,
        keys,
        values,
        sums,
        prior,
        opening,
        head_norm_gain.reshape(1, LANES),
        pool,
        previous,
        pooling_group_weight[0],
        pooling_channel_scale.reshape(1, LANES),
    )
    peers = lax.axis_size("tp")
    groups = [[c + 2 * x for x in range(peers // 2)] for c in range(2)]
    same = lax.all_to_all(
        jnp.broadcast_to(mine[None], (peers // 2,) + mine.shape), "tp", 0, 0, axis_index_groups=groups
    )
    other = lax.ppermute(same, "tp", [(i, i ^ 1) for i in range(peers)])
    (result,) = call(
        output_kernel,
        [struct((tokens, columns), bf16)],
        "output",
        (tp % 2).reshape(1),
        same,
        other,
        late,
    )
    return result[None]


def solution(mesh):
    in_specs = (
        P("fs", "sp", None),
        P(),
        P(("sp", "fs"), "tp"),
        P(("sp", "fs"), "tp"),
        P(("sp", "fs"), "tp"),
        P(("sp", "fs"), "tp"),
        P(("sp", "fs"), "tp"),
        P(("sp", "fs"), None),
        P(None, "tp"),
        P("tp"),
        P("tp", "sp"),
        P("tp"),
        P("fs", "tp", None, None),
        P("tp", None, None),
        P("tp"),
        P("sp", "tp"),
        P("sp", "tp"),
    )
    out_specs = P("fs", "sp", "tp")
    return jax.shard_map(body, mesh=mesh, in_specs=in_specs, out_specs=out_specs, check_vma=False)
```

time: 188 us -> 181 us (0.963)
  blocking collectives: 69.8 us -> 96.3 us
  starting transfers between devices: 59 us -> 36.9 us
  Pallas kernels: 5.75 us -> 24.9 us
  matrix products: 13.5 us -> 0 us
  waiting for transfers between devices: 13.9 us -> 3.62 us
  local copies, waits for them, and re-layouts: 7.85 us -> 4.37 us
    ppermute x14 -> x4, starting transfers between devices: 59 us -> 15 us  [shifted(): return lax.ppermute(x, axis, pairs)]
    all_gather x0 -> x1, blocking collectives: none -> 25.2 us  [body(): runs = lax.all_gather(run, 'sp', axis=0, tiled=True)]
    pallas_call x0 -> x6, Pallas kernels: none -> 20.4 us  [call(): pl.pallas_call(kernel, in_specs=[smem] * scalars + [vmem] * (len(args) -...]
    ppermute x0 -> x1, starting transfers between devices: none -> 18.4 us  [body(): other = lax.ppermute(same, 'tp', [(i, i ^ 1) for i in range(peers)])]
    ppermute x14 -> x4, waiting for transfers between devices: 13.9 us -> 0.01 us  [shifted(): return lax.ppermute(x, axis, pairs)]
    dot_general x30 -> x0, matrix products: 13.5 us -> none  [the longest x4 4.16 us: body(): jnp.dot(x, rest, preferred_element_type=f32)]
    all_gather x1, blocking collectives: 40.3 us -> 46.2 us  [body(): early = lax.all_gather(early, 'sp', axis=0, tiled=True)]
    all_to_all x1 -> x2, blocking collectives: 29.5 us -> 25 us  [the longest x1 13.3 us: body(): parts = lax.all_to_all(parts, 'fs', 0, 0)]
  transfers between devices with their start and end apart: 15 -> 7, of which waited for: 8 -> 2; matrix products, arithmetic and copies ran while one was open for 7% -> 1% of each run, Pallas kernels for 3% -> 7%
where the time goes in v2:
time: 181 us; the launch traced here: 180 us
  blocking collectives  96.3 us (53%)
  starting transfers between devices  36.9 us (20%)
  Pallas kernels  24.9 us (14%)
  between operations  13.5 us (7%)
  local copies, waits for them, and re-layouts  4.37 us (2%)
  waiting for transfers between devices  3.62 us (2%)
    all_gather x1, blocking collectives, body(): early = lax.all_gather(early, 'sp', axis=0, tiled=True)  46.2 us
    all_gather x1, blocking collectives, body(): runs = lax.all_gather(run, 'sp', axis=0, tiled=True)  25.2 us
    pallas_call x6, Pallas kernels, call(): pl.pallas_call(kernel, in_specs=[smem] * scalars + [vmem] * (len(args) -...  20.4 us
    ppermute x1, starting transfers between devices, body(): other = lax.ppermute(same, 'tp', [(i, i ^ 1) for i in range(peers)])  18.4 us
    ppermute x4, starting transfers between devices, shifted(): return lax.ppermute(x, axis, pairs)  15 us
    all_to_all x1, blocking collectives, body(): parts = lax.all_to_all(parts, 'fs', 0, 0)  13.3 us
    all_to_all x1, blocking collectives, body(): lax.all_to_all(jnp.broadcast_to(mine[None], (peers // 2,) + mine.shape),...  11.7 us
    pallas_call x1, Pallas kernels, prepare(): pl.pallas_call(prep_kernel, grid_spec=pltpu.PrefetchScalarGridSpec(num_sc...  4.47 us
  transfers between devices with their start and end apart: 7, of which 2 were waited for; matrix products, arithmetic and copies ran while one was open for 1% of the time, Pallas kernels for 7%

profile of v2, /device:TPU:1, one launch (start us, length us, event | category | flops | bytes accessed | tf_op | source)
XLA Modules:
  0.0 180.2 jit_solution(12676329264970863949)
XLA Ops:
  6.5 1.7 pack.1
  8.2 4.5 %prep.1 = (bf16[256,1024]{1,0:T(8,128)(2,1)}, bf16[256,1024]{1,0:T(8,128)(2,1)}, bf16[256,1024]{1,0:T(8,128)(2,1)}, bf16[256,1024]{1,0:T(8,128)(2,1)}, f32[256,128]{1,0:T(8,128)}) custom-call(s32[1]{0:T(128)} %bitcast.3.own, bf16[256,4096]{1,0:T(8,128)(2,1)} %bitcast.16, f32[1,4096]{1,0:T(1,128)} %bitcast.19), custom_call_target="tpu_custom_call" | custom-call | tf_op jit(solution)/shard_map/prep/pallas_call | solution.py:84
  12.7 4.0 %collective-permute-start = (bf16[256,1024]{1,0:T(8,128)(2,1)}, bf16[256,1024]{1,0:T(8,128)(2,1)S(1)}, u32[]{:S(2)}, u32[]{:S(2)}) collective-permute-start(bf16[256,1024]{1,0:T(8,128)(2,1)} %get-tuple-element.24), channel_id=1, source_target_pairs={{0,8},{8,16},{16,24},{24,0},{1,9},{9,17},{17,25},{25,1},{2,10},{10... | collective-permute-start | bytes 1572872 | tf_op jit(solution)/shard_map/exchange/ppermute | solution.py:26
  16.7 4.5 %collective-permute-start.1 = (bf16[256,1024]{1,0:T(8,128)(2,1)}, bf16[256,1024]{1,0:T(8,128)(2,1)S(1)}, u32[]{:S(2)}, u32[]{:S(2)}) collective-permute-start(bf16[256,1024]{1,0:T(8,128)(2,1)} %get-tuple-element.25), channel_id=1, source_target_pairs={{0,16},{8,24},{16,0},{24,8},{1,17},{9,25},{17,1},{25,9},{2,18},{10... | collective-permute-start | bytes 1572872 | tf_op jit(solution)/shard_map/exchange/ppermute | solution.py:26
  21.2 3.0 %collective-permute-start.2 = (bf16[256,1024]{1,0:T(8,128)(2,1)}, bf16[256,1024]{1,0:T(8,128)(2,1)S(1)}, u32[]{:S(2)}, u32[]{:S(2)}) collective-permute-start(bf16[256,1024]{1,0:T(8,128)(2,1)} %get-tuple-element.26), channel_id=1, source_target_pairs={{0,24},{8,0},{16,8},{24,16},{1,25},{9,1},{17,9},{25,17},{2,26},{10... | collective-permute-start | bytes 1572872 | tf_op jit(solution)/shard_map/exchange/ppermute | solution.py:26
  24.2 46.2 %all_gather.10.w = bf16[1024,448]{1,0:T(8,128)(2,1)} all-gather(bf16[64,448]{1,0:T(8,128)(2,1)} %get-tuple-element.27), channel_id=1, replica_groups=mesh['sp'=16,'fs'=4,'tp'=8] {'sp'}, dimensions={0}, use_global_device_ids=true | all-gather | bytes 974848 | tf_op jit(solution)/shard_map/early/all_gather | solution.py:344
  70.4 0.8 copy-done.2
  71.6 4.1 %early_parts.1 = bf16[4,896,128]{2,1,0:T(8,128)(2,1)} custom-call(s32[1]{0:T(128)} %bitcast.3.own, bf16[256,1024]{1,0:T(8,128)(2,1)} %get-tuple-element.23.x0, bf16[256,1024]{1,0:T(8,128)(2,1)} %copy-done.2, bf16[256,1024]{1,0:T(8,128)(2,1)} %copy-done.3, bf16[256,1024]{1,0:T(8,128)(2,1)} %copy-done.4, bf16[1024,448]{1,0:T(8,128)(2,1)} %all_gather.10.w), custom_call_target="tpu_custom_call" | custom-call | tf_op jit(solution)/shard_map/early_parts/pallas_call | solution.py:32
  75.7 13.3 %all_to_all.15.parts = bf16[4,896,128]{2,1,0:T(8,128)(2,1)} all-to-all(bf16[4,896,128]{2,1,0:T(8,128)(2,1)} %early_parts.1), channel_id=1, replica_groups=mesh['sp'=16,'fs'=4,'tp'=8] {'fs'}, dimensions={0} | all-to-all | bytes 1835008 | tf_op jit(solution)/shard_map/all_to_all | solution.py:351
  89.1 3.3 %local.1 = (f32[256,128]{1,0:T(8,128)}, f32[256,128]{1,0:T(8,128)}, bf16[256,128]{1,0:T(8,128)(2,1)}, bf16[16,128]{1,0:T(8,128)(2,1)}, f32[256,128]{1,0:T(8,128)...) custom-call(bf16[4,896,128]{2,1,0:T(8,128)(2,1)} %all_to_all.15.parts, ...), custom_call_target="tpu_custom_call" | custom-call | tf_op jit(solution)/shard_map/local/pallas_call | solution.py:32
  92.4 25.2 %all_gather.11.runs = f32[1152,128]{1,0:T(8,128)} all-gather(f32[72,128]{1,0:T(8,128)} %get-tuple-element.29), channel_id=1, replica_groups=mesh['sp'=16,'fs'=4,'tp'=8] {'sp'}, dimensions={0}, use_global_device_ids=true | all-gather | bytes 626688 | tf_op jit(solution)/shard_map/states/all_gather | solution.py:376
  117.5 3.9 %late_parts.1 = bf16[4,512,128]{2,1,0:T(8,128)(2,1)} custom-call(s32[1]{0:T(128)} %bitcast.3.own, bf16[256,1024]{1,0:T(8,128)(2,1)} %get-tuple-element.23.x0, bf16[256,1024]{1,0:T(8,128)(2,1)} %copy-done.2, bf16[256,1024]{1,0:T(8,128)(2,1)} %copy-done.3, bf16[256,1024]{1,0:T(8,128)(2,1)} %copy-done.4, bf16[1024,1280]{1,0:T(8,128)(2,1)} %all-gather.2.cloned.1.call-done.w.late), custom_call_target="tpu_custom_call" | custom-call | tf_op jit(solution)/shard_map/late_parts/pallas_call | solution.py:32
  121.5 3.5 %all-to-all-start.1 = ((bf16[4,512,128]{2,1,0:T(8,128)(2,1)}), bf16[4,512,128]{2,1,0:T(8,128)(2,1)S(1)}, u32[]{:S(2)}, u32[]{:S(2)}) async-start(bf16[4,512,128]{2,1,0:T(8,128)(2,1)} %late_parts.1), calls=%async_computation.1 | async-start | bytes 1048576 | tf_op jit(solution)/shard_map/all_to_all | solution.py:380
  125.0 3.5 %collective-permute-start.3 = (bf16[16,128]{1,0:T(8,128)(2,1)S(1)}, bf16[16,128]{1,0:T(8,128)(2,1)S(1)}, u32[]{:S(2)}, u32[]{:S(2)}) collective-permute-start(bf16[16,128]{1,0:T(8,128)(2,1)S(1)} %copy-done.8), channel_id=1, source_target_pairs={{0,32},{32,64},{64,96},{96,128},{128,160},{160,192},{192,224},{224... | collective-permute-start | bytes 12296 | tf_op jit(solution)/shard_map/halo/ppermute | solution.py:26
  129.1 0.7 copy.19.start
  129.8 2.1 %all-to-all-done.1.parts = bf16[4,512,128]{2,1,0:T(8,128)(2,1)S(1)} async-done(((bf16[4,512,128]{2,1,0:T(8,128)(2,1)}), bf16[4,512,128]{2,1,0:T(8,128)(2,1)S(1)}, u32[]{:S(2)}, u32[]{:S(2)}) %all-to-all-start.1) | async-done | bytes 524320 | tf_op jit(solution)/shard_map/all_to_all | solution.py:380
  131.8 0.8 copy-done
  132.6 3.4 %finish.1 = bf16[256,256]{1,0:T(8,128)(2,1)} custom-call(s32[2]{0:T(128)} %pad_add_fusion.where, f32[1152,128]{1,0:T(8,128)} %all_gather.11.runs, f32[64,128]{1,0:T(8,128)} %copy.19.start, bf16[4,512,128]{2,1,0:T(8,128)(2,1)} %copy-done, f32[256,128]{1,0:T(8,128)} %get-tuple-element.28.inverse, f32[256,128]{1,0:T(8,128)} %get-tuple-element.32.keys, ...), custom_call_target="tpu_custom_call" | custom-call | tf_op jit(solution)/shard_map/finish/pallas_call | solution.py:32
  136.0 0.9 broadcast_in_dim.4
  137.0 11.7 %all_to_all.16.same = bf16[4,256,256]{2,1,0:T(8,128)(2,1)S(1)} all-to-all(bf16[4,256,256]{2,1,0:T(8,128)(2,1)S(1)} %broadcast_in_dim.4), channel_id=1, replica_groups={{0,2,4,6},{1,3,5,7},{8,10,12,14},{9,11,13,15},{16,18,20,22},{17,19,21,2..., dimensions={0} | all-to-all | bytes 1048576 | tf_op jit(solution)/shard_map/all_to_all | solution.py:403
  148.6 18.4 %collective-permute-start.4 = (bf16[4,256,256]{2,1,0:T(8,128)(2,1)S(1)}, bf16[4,256,256]{2,1,0:T(8,128)(2,1)S(1)}, u32[]{:S(2)}, u32[]{:S(2)}) collective-permute-start(bf16[4,256,256]{2,1,0:T(8,128)(2,1)S(1)} %all_to_all.16.same), channel_id=1, source_target_pairs={{0,1},{1,0},{2,3},{3,2},{4,5},{5,4},{6,7},{7,6},{8,9},{9,8},{10,11... | collective-permute-start | bytes 1572872 | tf_op jit(solution)/shard_map/ppermute | solution.py:406
  167.1 1.5 collective-permute-done.4.other
  168.6 0.8 copy-done.5
  169.4 4.0 %output.1 = bf16[256,512]{1,0:T(8,128)(2,1)} custom-call(s32[1]{0:T(128)} %bitcast.core, bf16[4,256,256]{2,1,0:T(8,128)(2,1)} %copy-done.1, bf16[4,256,256]{2,1,0:T(8,128)(2,1)} %copy-done.5, bf16[1024,1280]{1,0:T(8,128)(2,1)} %all-gather.2.cloned.1.call-done.w.late), custom_call_target="tpu_custom_call" | custom-call | tf_op jit(solution)/shard_map/output/pallas_call | solution.py:32
  (23 shorter events, 1.0 us)
Async XLA Ops:
  6.5 111.0 %all-gather.2.cloned.1.call-start = ((), (), s32[]{:S(2)}) async-start(), calls=%async_computation.3 | async-start | bytes 2785280 | tf_op jit(solution)/shard_map/all_gather | solution.py:339
  12.7 57.7 %collective-permute-start = (bf16[256,1024]{1,0:T(8,128)(2,1)}, bf16[256,1024]{1,0:T(8,128)(2,1)S(1)}, u32[]{:S(2)}, u32[]{:S(2)}) collective-permute-start(bf16[256,1024]{1,0:T(8,128)(2,1)} %get-tuple-element.24), channel_id=1, source_target_pairs={{0,8},{8,16},{16,24},{24,0},{1,9},{9,17},{17,25},{25,1},{2,10},{10... | collective-permute-start | bytes 1572872 | tf_op jit(solution)/shard_map/exchange/ppermute | solution.py:26
  16.7 53.7 %collective-permute-start.1 = (bf16[256,1024]{1,0:T(8,128)(2,1)}, bf16[256,1024]{1,0:T(8,128)(2,1)S(1)}, u32[]{:S(2)}, u32[]{:S(2)}) collective-permute-start(bf16[256,1024]{1,0:T(8,128)(2,1)} %get-tuple-element.25), channel_id=1, source_target_pairs={{0,16},{8,24},{16,0},{24,8},{1,17},{9,25},{17,1},{25,9},{2,18},{10... | collective-permute-start | bytes 1572872 | tf_op jit(solution)/shard_map/exchange/ppermute | solution.py:26
  21.2 49.2 %collective-permute-start.2 = (bf16[256,1024]{1,0:T(8,128)(2,1)}, bf16[256,1024]{1,0:T(8,128)(2,1)S(1)}, u32[]{:S(2)}, u32[]{:S(2)}) collective-permute-start(bf16[256,1024]{1,0:T(8,128)(2,1)} %get-tuple-element.26), channel_id=1, source_target_pairs={{0,24},{8,0},{16,8},{24,16},{1,25},{9,1},{17,9},{25,17},{2,26},{10... | collective-permute-start | bytes 1572872 | tf_op jit(solution)/shard_map/exchange/ppermute | solution.py:26
  70.4 0.8 copy-start.2
  70.4 1.0 copy-start.3
  70.4 1.2 copy-start.4
  117.5 7.4 %copy-start.8 = (bf16[16,128]{1,0:T(8,128)(2,1)S(1)}, bf16[16,128]{1,0:T(8,128)(2,1)}, u32[]{:S(2)}) copy-start(bf16[16,128]{1,0:T(8,128)(2,1)} %get-tuple-element.38) | copy-start | bytes 12292
  117.5 11.5 %copy-start.6 = (f32[1,2,64,64]{3,2,1,0:T(8,128)S(1)}, f32[1,2,64,64]{3,2,1,0:T(8,128)}, u32[]{:S(2)}) copy-start(f32[1,2,64,64]{3,2,1,0:T(8,128)} %param.29) | copy-start | bytes 98308
  121.5 10.4 %all-to-all-start.1 = ((bf16[4,512,128]{2,1,0:T(8,128)(2,1)}), bf16[4,512,128]{2,1,0:T(8,128)(2,1)S(1)}, u32[]{:S(2)}, u32[]{:S(2)}) async-start(bf16[4,512,128]{2,1,0:T(8,128)(2,1)} %late_parts.1), calls=%async_computation.1 | async-start | bytes 1048576 | tf_op jit(solution)/shard_map/all_to_all | solution.py:380
  125.0 4.8 %collective-permute-start.3 = (bf16[16,128]{1,0:T(8,128)(2,1)S(1)}, bf16[16,128]{1,0:T(8,128)(2,1)S(1)}, u32[]{:S(2)}, u32[]{:S(2)}) collective-permute-start(bf16[16,128]{1,0:T(8,128)(2,1)S(1)} %copy-done.8), channel_id=1, source_target_pairs={{0,32},{32,64},{64,96},{96,128},{128,160},{160,192},{192,224},{224... | collective-permute-start | bytes 12296 | tf_op jit(solution)/shard_map/halo/ppermute | solution.py:26
  129.8 2.1 %copy-start.7 = (bf16[16,128]{1,0:T(8,128)(2,1)}, bf16[16,128]{1,0:T(8,128)(2,1)S(1)}, u32[]{:S(2)}) copy-start(bf16[16,128]{1,0:T(8,128)(2,1)S(1)} %collective-permute-done.3.previous) | copy-start | bytes 12292
  131.8 0.8 copy-start
  148.6 20.0 %copy-start.1 = (bf16[4,256,256]{2,1,0:T(8,128)(2,1)}, bf16[4,256,256]{2,1,0:T(8,128)(2,1)S(1)}, u32[]{:S(2)}) copy-start(bf16[4,256,256]{2,1,0:T(8,128)(2,1)S(1)} %all_to_all.16.same) | copy-start | bytes 1572868
  148.6 19.9 %collective-permute-start.4 = (bf16[4,256,256]{2,1,0:T(8,128)(2,1)S(1)}, bf16[4,256,256]{2,1,0:T(8,128)(2,1)S(1)}, u32[]{:S(2)}, u32[]{:S(2)}) collective-permute-start(bf16[4,256,256]{2,1,0:T(8,128)(2,1)S(1)} %all_to_all.16.same), channel_id=1, source_target_pairs={{0,1},{1,0},{2,3},{3,2},{4,5},{5,4},{6,7},{7,6},{8,9},{9,8},{10,11... | collective-permute-start | bytes 1572872 | tf_op jit(solution)/shard_map/ppermute | solution.py:406
  168.6 0.8 copy-start.5
Sparse Core Ops, SparseCore 0:
  9.4 73.0 all-gather.1

commit v3 on v2

--- a/solution.py
+++ b/solution.py
@@ -38,16 +38,26 @@
     )(*args)
 
 
+def near(x):
+    return pltpu.with_memory_space_constraint(x, pltpu.VMEM)
+
+
 def struct(shape, dtype):
     return jax.ShapeDtypeStruct(shape, dtype)
 
 
-def pack_kernel(key, value, pool, low, query, gate, pool_rows, state_rows, early, late):
-    for out, refs in ((early, (key, value, pool, low)), (late, (query, gate, pool_rows, state_rows))):
-        at = 0
-        for r in refs:
-            out[:, at : at + r.shape[1]] = r[...]
-            at += r.shape[1]
+def pack_kernel(
+    own, key, value, pool, low, query, gate, pool_rows, state_rows, early, late
+):
+    at = 0
+    for r in (key, value, pool, low):
+        early[:, at : at + r.shape[1]] = r[...]
+        at += r.shape[1]
+    mine = pl.ds(pl.multiple_of(own[0] * LANES, LANES), LANES)
+    for j, block in enumerate(
+        (query[...], gate[...], pool_rows[:, mine], state_rows[:, mine])
+    ):
+        late[:, j * LANES : (j + 1) * LANES] = block
 
 
 def prep_kernel(own, act, gain, x0, x1, x2, x3, inverse):
@@ -97,34 +107,46 @@
     )(own, act, gain)
 
 
-def partial_kernel(own, x0, x1, x2, x3, w, out):
+def partial_kernel(own, x0, x1, x2, x3, w, out, *rest):
+    *rest, held, arrived = rest
+    copies = []
+    for k, x in enumerate((x0, x1, x2, x3)):
+        copies.append(pltpu.make_async_copy(x, held.at[k], arrived.at[k]))
+        copies[k].start()
     tokens = x0.shape[0]
     wide = out.shape[1] // tokens * LANES
     columns = out.shape[1] * LANES // tokens
     half = lax.broadcasted_iota(jnp.int32, (tokens // 2, LANES), 1) < HEAD
     weight = w[:, :columns]
-    for k, x in enumerate((x0, x1, x2, x3)):
+    for k in range(4):
         target = (own[0] - k + 4) % 4
-        p = jnp.dot(x[...], weight, preferred_element_type=f32)
+        copies[k].wait()
+        p = jnp.dot(held[k], weight, preferred_element_type=f32)
         for j in range(wide // LANES):
             out[target, j * tokens : (j + 1) * tokens] = p[:, j * LANES : (j + 1) * LANES].astype(bf16)
         if columns > wide:
             d = jnp.concatenate([p[:, wide:], p[:, wide:]], axis=1)
             d = jnp.where(half, d[: tokens // 2], d[tokens // 2 :])
             out[target, wide // LANES * tokens :] = d.astype(bf16)
+    for r in rest:
+        r[...] = w[:, columns:]
 
 
 def partials(own, xs, w, columns, name):
     tokens, _ = xs[0].shape
-    (out,) = call(
+    outs = [struct((4, tokens * columns // LANES, LANES), bf16)]
+    if w.shape[1] > columns:
+        outs.append(struct((w.shape[0], w.shape[1] - columns), bf16))
+    anywhere = pl.BlockSpec(memory_space=pl.ANY)
+    vmem = pl.BlockSpec(memory_space=pltpu.VMEM)
+    return pl.pallas_call(
         partial_kernel,
-        [struct((4, tokens * columns // LANES, LANES), bf16)],
-        name,
-        own,
-        *xs,
-        w,
-    )
-    return out
+        in_specs=[pl.BlockSpec(memory_space=pltpu.SMEM)] + [anywhere] * 4 + [vmem],
+        out_specs=[vmem] * len(outs),
+        out_shape=outs,
+        scratch_shapes=[pltpu.VMEM((4,) + xs[0].shape, bf16), pltpu.SemaphoreType.DMA((4,))],
+        name=name,
+    )(own, *xs, w)
 
 
 def total_of(parts, at, rows):
@@ -282,19 +304,19 @@
     mine[:, :LANES] = (mixture * pool_scale[...]).astype(bf16)
 
 
-def output_kernel(core, same, other, late, out):
-    first = 2 * LANES
-    width = out.shape[1]
+def output_kernel(core, same, other, rows, out):
     total = jnp.zeros(out.shape, f32)
     for x in range(same.shape[0]):
         for z, c in ((same, core[0]), (other, 1 - core[0])):
-            rows = pl.ds((2 * x + c) * LANES, LANES)
-            total = total + jnp.dot(
-                z[x, :, :LANES], late[rows, first : first + width], preferred_element_type=f32
+            at = pl.ds(pl.multiple_of((2 * x + c) * LANES, LANES), LANES)
+            w = jnp.concatenate(
+                [
+                    jnp.concatenate([rows[f, at, :LANES], rows[f, at, LANES:]], axis=0)
+                    for f in range(rows.shape[0])
+                ],
+                axis=1,
             )
-            total = total + jnp.dot(
-                z[x, :, LANES:], late[rows, first + width :], preferred_element_type=f32
-            )
+            total = total + jnp.dot(z[x], w, preferred_element_type=f32)
     out[...] = total.astype(bf16)
 
 
@@ -324,8 +346,9 @@
     tp = lax.axis_index("tp").astype(jnp.int32)
     early, late = call(
         pack_kernel,
-        [struct((rows, 3 * LANES + HEAD), bf16), struct((rows, 2 * LANES + 2 * columns), bf16)],
+        [struct((rows, 3 * LANES + HEAD), bf16), struct((rows, 4 * LANES), bf16)],
         "pack",
+        own,
         key_projection_weight,
         value_projection_weight,
         pooling_channel_weight,
@@ -334,7 +357,6 @@
         output_gate_weight,
         pooling_output_rows,
         attention_output_rows,
-        scalars=0,
     )
     late = lax.all_gather(late, "sp", axis=0, tiled=True)
     x0, x1, x2, x3, inverse = prepare(
@@ -347,19 +369,20 @@
         x2 = shifted(x2, "fs", 2, True)
         x3 = shifted(x3, "fs", 3, True)
     xs = (x0, x1, x2, x3)
-    parts = partials(own, xs, early, early.shape[1], "early_parts")
-    parts = lax.all_to_all(parts, "fs", 0, 0)
-    wide = struct((tokens, LANES), f32)
+    inverse = near(inverse)
+    (parts,) = partials(own, xs, near(early), early.shape[1], "early_parts")
+    parts = near(lax.all_to_all(parts, "fs", 0, 0))
+    wide = pltpu.VMEM((tokens, LANES), f32)
     keys, values, pool, tail, sums, prior, opening, run = call(
         local_kernel,
         [
             wide,
             wide,
-            struct((tokens, LANES), bf16),
+            pltpu.VMEM((tokens, LANES), bf16),
             struct((HALO, LANES), bf16),
             wide,
             wide,
-            struct((tokens // BLOCK, LANES), f32),
+            pltpu.VMEM((tokens // BLOCK, LANES), f32),
             struct((RUN_ROWS, LANES), f32),
         ],
         "local",
@@ -372,29 +395,33 @@
     )
     with jax.named_scope("halo"):
         previous = shifted(tail, "sp", 1, False)
+    start = starting_state[0].transpose(2, 0, 1).reshape(HEAD, LANES)
+    late, run = lax.optimization_barrier((late, run))
+    late_parts, quarter = partials(own, xs, late, 2 * LANES, "late_parts")
+    late_parts, quarter, run = lax.optimization_barrier((late_parts, quarter, run))
+    with jax.named_scope("rows"):
+        out_rows = lax.all_gather(quarter, "fs")
+    with jax.named_scope("late_back"):
+        late_parts = lax.all_to_all(late_parts, "fs", 0, 0)
     with jax.named_scope("states"):
         runs = lax.all_gather(run, "sp", axis=0, tiled=True)
-    start = starting_state[0].transpose(2, 0, 1).reshape(HEAD, LANES)
-    late, runs = lax.optimization_barrier((late, runs))
-    parts = partials(own, xs, late, 2 * LANES, "late_parts")
-    parts = lax.all_to_all(parts, "fs", 0, 0)
     (mine,) = call(
         finish_kernel,
         [struct((tokens, 2 * LANES), bf16)],
         "finish",
         jnp.stack([lax.axis_index("sp").astype(jnp.int32), tp]),
-        runs,
-        start,
-        parts,
+        near(runs),
+        near(start),
+        near(late_parts),
         inverse,
-        keys,
-        values,
-        sums,
-        prior,
-        opening,
+        near(keys),
+        near(values),
+        near(sums),
+        near(prior),
+        near(opening),
         head_norm_gain.reshape(1, LANES),
-        pool,
-        previous,
+        near(pool),
+        near(previous),
         pooling_group_weight[0],
         pooling_channel_scale.reshape(1, LANES),
     )
@@ -409,9 +436,9 @@
         [struct((tokens, columns), bf16)],
         "output",
         (tp % 2).reshape(1),
-        same,
-        other,
-        late,
+        near(same),
+        near(other),
+        near(out_rows),
     )
     return result[None]
 

time: 181 us -> 163 us (0.901)
  blocking collectives: 96.3 us -> 88.9 us
  starting transfers between devices: 36.9 us -> 31.8 us
  Pallas kernels: 24.9 us -> 22 us
  waiting for transfers between devices: 3.62 us -> 1.55 us
    pallas_call x6 -> x4, Pallas kernels: 20.4 us -> 8.53 us  [call(): pl.pallas_call(kernel, in_specs=[smem] * scalars + [vmem] * (len(args) -...]
    pallas_call x0 -> x2, Pallas kernels: none -> 9.01 us  [partials(): pl.pallas_call(partial_kernel, in_specs=[pl.BlockSpec(memory_space=pltpu....]
    all_gather x1, blocking collectives: 46.2 us -> 38.3 us  [body(): early = lax.all_gather(early, 'sp', axis=0, tiled=True)]
    ppermute x1, starting transfers between devices: 18.4 us -> 14.6 us  [body(): other = lax.ppermute(same, 'tp', [(i, i ^ 1) for i in range(peers)])]
    all_to_all x1, waiting for transfers between devices: 2.09 us -> 0.01 us  [body(): late_parts = lax.all_to_all(late_parts, 'fs', 0, 0)]
    all_gather x1, blocking collectives: 25.2 us -> 27.2 us  [body(): runs = lax.all_gather(run, 'sp', axis=0, tiled=True)]
  transfers between devices with their start and end apart: 7 -> 8, of which waited for: 2 -> 1; matrix products, arithmetic and copies ran while one was open for 1% -> 1% of each run, Pallas kernels for 7% -> 9%
where the time goes in v3:
time: 163 us; the launch traced here: 162 us
  blocking collectives  88.9 us (55%)
  starting transfers between devices  31.8 us (20%)
  Pallas kernels  22 us (13%)
  between operations  13.6 us (8%)
  local copies, waits for them, and re-layouts  3.78 us (2%)
    all_gather x1, blocking collectives, body(): early = lax.all_gather(early, 'sp', axis=0, tiled=True)  38.3 us
    all_gather x1, blocking collectives, body(): runs = lax.all_gather(run, 'sp', axis=0, tiled=True)  27.2 us
    ppermute x1, starting transfers between devices, body(): other = lax.ppermute(same, 'tp', [(i, i ^ 1) for i in range(peers)])  14.6 us
    ppermute x4, starting transfers between devices, shifted(): return lax.ppermute(x, axis, pairs)  13.7 us
    all_to_all x1, blocking collectives, body(): parts = near(lax.all_to_all(parts, 'fs', 0, 0))  12.5 us
    all_to_all x1, blocking collectives, body(): lax.all_to_all(jnp.broadcast_to(mine[None], (peers // 2,) + mine.shape),...  10.8 us
    pallas_call x2, Pallas kernels, partials(): pl.pallas_call(partial_kernel, in_specs=[pl.BlockSpec(memory_space=pltpu....  9.01 us
    pallas_call x4, Pallas kernels, call(): pl.pallas_call(kernel, in_specs=[smem] * scalars + [vmem] * (len(args) -...  8.53 us
  transfers between devices with their start and end apart: 8, of which 1 were waited for; matrix products, arithmetic and copies ran while one was open for 1% of the time, Pallas kernels for 9%

profile of v3, /device:TPU:1, one launch (start us, length us, event | category | flops | bytes accessed | tf_op | source)
XLA Modules:
  0.0 162.2 jit_solution(7113296042582699091)
XLA Ops:
  6.5 1.7 %pack.1 = (bf16[64,448]{1,0:T(8,128)(2,1)}, bf16[64,512]{1,0:T(8,128)(2,1)}) custom-call(s32[1]{0:T(128)} %bitcast.3.own, bf16[64,128]{1,0:T(8,128)(2,1)} %key.1, bf16[64,128]{1,0:T(8,128)(2,1)} %value.1, bf16[64,128]{1,0:T(8,128)(2,1)} %pool.1, bf16[64,64]{1,0:T(8,128)(2,1)} %low.1, bf16[64,128]{1,0:T(8,128)(2,1)} %query.1, bf16[64,128]{1,0:T(8,128)(2,1)} %gate.1, ...), custom_call_target="tpu_custom_call" | custom-call | tf_op jit(solution)/shard_map/pack/pallas_call | solution.py:32
  8.3 4.4 %prep.1 = (bf16[256,1024]{1,0:T(8,128)(2,1)}, bf16[256,1024]{1,0:T(8,128)(2,1)}, bf16[256,1024]{1,0:T(8,128)(2,1)}, bf16[256,1024]{1,0:T(8,128)(2,1)}, f32[256,128]{1,0:T(8,128)}) custom-call(s32[1]{0:T(128)} %bitcast.3.own, bf16[256,4096]{1,0:T(8,128)(2,1)} %bitcast.18, f32[1,4096]{1,0:T(1,128)} %bitcast.21), custom_call_target="tpu_custom_call" | custom-call | tf_op jit(solution)/shard_map/prep/pallas_call | solution.py:94
  12.7 4.0 %collective-permute-start = (bf16[256,1024]{1,0:T(8,128)(2,1)}, bf16[256,1024]{1,0:T(8,128)(2,1)S(1)}, u32[]{:S(2)}, u32[]{:S(2)}) collective-permute-start(bf16[256,1024]{1,0:T(8,128)(2,1)} %get-tuple-element.28), channel_id=1, source_target_pairs={{0,8},{8,16},{16,24},{24,0},{1,9},{9,17},{17,25},{25,1},{2,10},{10... | collective-permute-start | bytes 1572872 | tf_op jit(solution)/shard_map/exchange/ppermute | solution.py:26
  16.7 4.5 %collective-permute-start.1 = (bf16[256,1024]{1,0:T(8,128)(2,1)}, bf16[256,1024]{1,0:T(8,128)(2,1)S(1)}, u32[]{:S(2)}, u32[]{:S(2)}) collective-permute-start(bf16[256,1024]{1,0:T(8,128)(2,1)} %get-tuple-element.29), channel_id=1, source_target_pairs={{0,16},{8,24},{16,0},{24,8},{1,17},{9,25},{17,1},{25,9},{2,18},{10... | collective-permute-start | bytes 1572872 | tf_op jit(solution)/shard_map/exchange/ppermute | solution.py:26
  21.2 3.0 %collective-permute-start.2 = (bf16[256,1024]{1,0:T(8,128)(2,1)}, bf16[256,1024]{1,0:T(8,128)(2,1)S(1)}, u32[]{:S(2)}, u32[]{:S(2)}) collective-permute-start(bf16[256,1024]{1,0:T(8,128)(2,1)} %get-tuple-element.30), channel_id=1, source_target_pairs={{0,24},{8,0},{16,8},{24,16},{1,25},{9,1},{17,9},{25,17},{2,26},{10... | collective-permute-start | bytes 1572872 | tf_op jit(solution)/shard_map/exchange/ppermute | solution.py:26
  24.2 38.3 %all_gather.16.w = bf16[1024,448]{1,0:T(8,128)(2,1)S(1)} all-gather(bf16[64,448]{1,0:T(8,128)(2,1)S(1)} %copy-done.5), channel_id=1, replica_groups=mesh['sp'=16,'fs'=4,'tp'=8] {'sp'}, dimensions={0}, use_global_device_ids=true | all-gather | bytes 974848 | tf_op jit(solution)/shard_map/early/all_gather | solution.py:366
  62.6 0.7 copy-done.2
  63.3 0.2 copy-done.3
  63.5 0.2 copy-done.4
  63.7 4.1 %early_parts.1 = bf16[4,896,128]{2,1,0:T(8,128)(2,1)} custom-call(s32[1]{0:T(128)} %bitcast.3.own, bf16[256,1024]{1,0:T(8,128)(2,1)} %get-tuple-element.27.x0, bf16[256,1024]{1,0:T(8,128)(2,1)} %copy-done.2, bf16[256,1024]{1,0:T(8,128)(2,1)} %copy-done.3, bf16[256,1024]{1,0:T(8,128)(2,1)} %copy-done.4, bf16[1024,448]{1,0:T(8,128)(2,1)S(1)} %all_gather.16.w), custom_call_target="tpu_custom_call" | custom-call | tf_op jit(solution)/shard_map/early_parts/pallas_call | solution.py:142
  67.8 12.5 %all_to_all.15.parts = bf16[4,896,128]{2,1,0:T(8,128)(2,1)S(1)} all-to-all(bf16[4,896,128]{2,1,0:T(8,128)(2,1)} %early_parts.1), channel_id=1, replica_groups=mesh['sp'=16,'fs'=4,'tp'=8] {'fs'}, dimensions={0} | all-to-all | bytes 1835008 | tf_op jit(solution)/shard_map/all_to_all | solution.py:374
  80.4 2.8 %local.1 = (f32[256,128]{1,0:T(8,128)S(1)}, f32[256,128]{1,0:T(8,128)S(1)}, bf16[256,128]{1,0:T(8,128)(2,1)S(1)}, bf16[16,128]{1,0:T(8,128)(2,1)}, f32[256,128]{...) custom-call(bf16[4,896,128]{2,1,0:T(8,128)(2,1)S(1)} %all_to_all.15.parts, ...), custom_call_target="tpu_custom_call" | custom-call | tf_op jit(solution)/shard_map/local/pallas_call | solution.py:32
  83.1 4.9 %late_parts.1 = (bf16[4,512,128]{2,1,0:T(8,128)(2,1)}, bf16[1024,256]{1,0:T(8,128)(2,1)}) custom-call(s32[1]{0:T(128)} %bitcast.3.own, bf16[256,1024]{1,0:T(8,128)(2,1)} %get-tuple-element.27.x0, bf16[256,1024]{1,0:T(8,128)(2,1)} %copy-done.2, bf16[256,1024]{1,0:T(8,128)(2,1)} %copy-done.3, bf16[256,1024]{1,0:T(8,128)(2,1)} %copy-done.4, ...), custom_call_target="tpu_custom_call" | custom-call | tf_op jit(solution)/shard_map/late_parts/pallas_call | solution.py:142
  88.1 3.5 %all-to-all-start.1 = ((bf16[4,512,128]{2,1,0:T(8,128)(2,1)}), bf16[4,512,128]{2,1,0:T(8,128)(2,1)S(1)}, u32[]{:S(2)}, u32[]{:S(2)}) async-start(bf16[4,512,128]{2,1,0:T(8,128)(2,1)} %get-tuple-element.40), calls=%async_computation.1 | async-start | bytes 1048576 | tf_op jit(solution)/shard_map/late_back/all_to_all | solution.py:405
  91.7 0.7 pad_add_fusion.where
  92.4 2.2 %collective-permute-start.3 = (bf16[16,128]{1,0:T(8,128)(2,1)S(1)}, bf16[16,128]{1,0:T(8,128)(2,1)S(1)}, u32[]{:S(2)}, u32[]{:S(2)}) collective-permute-start(bf16[16,128]{1,0:T(8,128)(2,1)S(1)} %copy-done.8), channel_id=1, source_target_pairs={{0,32},{32,64},{64,96},{96,128},{128,160},{160,192},{192,224},{224... | collective-permute-start | bytes 12296 | tf_op jit(solution)/shard_map/halo/ppermute | solution.py:26
  94.6 27.2 %all_gather.17.runs = f32[1152,128]{1,0:T(8,128)S(1)} all-gather(f32[72,128]{1,0:T(8,128)S(1)} %copy-done.7), channel_id=1, replica_groups=mesh['sp'=16,'fs'=4,'tp'=8] {'sp'}, dimensions={0}, use_global_device_ids=true | all-gather | bytes 626688 | tf_op jit(solution)/shard_map/states/all_gather | solution.py:407
  121.8 2.7 %finish.1 = bf16[256,256]{1,0:T(8,128)(2,1)} custom-call(s32[2]{0:T(128)} %pad_add_fusion.where, f32[1152,128]{1,0:T(8,128)S(1)} %all_gather.17.runs, f32[64,128]{1,0:T(8,128)S(1)} %copy.19.start, bf16[4,512,128]{2,1,0:T(8,128)(2,1)S(1)} %all-to-all-done.1.parts, f32[256,128]{1,0:T(8,128)S(1)} %copy-done.1, f32[256,128]{1,0:T(8,128)S(1)} %get-tuple-element.41.keys, ...), custom_call_target="tpu_custom_call" | custom-call | tf_op jit(solution)/shard_map/finish/pallas_call | solution.py:32
  124.5 0.9 broadcast_in_dim.4
  125.5 10.8 %all_to_all.16.same = bf16[4,256,256]{2,1,0:T(8,128)(2,1)S(1)} all-to-all(bf16[4,256,256]{2,1,0:T(8,128)(2,1)S(1)} %broadcast_in_dim.4), channel_id=1, replica_groups={{0,2,4,6},{1,3,5,7},{8,10,12,14},{9,11,13,15},{16,18,20,22},{17,19,21,2..., dimensions={0} | all-to-all | bytes 1048576 | tf_op jit(solution)/shard_map/all_to_all | solution.py:430
  136.3 14.6 %collective-permute-start.4 = (bf16[4,256,256]{2,1,0:T(8,128)(2,1)S(1)}, bf16[4,256,256]{2,1,0:T(8,128)(2,1)S(1)}, u32[]{:S(2)}, u32[]{:S(2)}) collective-permute-start(bf16[4,256,256]{2,1,0:T(8,128)(2,1)S(1)} %all_to_all.16.same), channel_id=1, source_target_pairs={{0,1},{1,0},{2,3},{3,2},{4,5},{5,4},{6,7},{7,6},{8,9},{9,8},{10,11... | collective-permute-start | bytes 1572872 | tf_op jit(solution)/shard_map/ppermute | solution.py:433
  150.9 1.5 collective-permute-done.4.other
  152.4 1.6 copy-done
  154.0 1.4 output.1
  (26 shorter events, 0.2 us)
Async XLA Ops:
  6.5 76.6 %all-gather.4.cloned.1.call-start = ((), (), s32[]{:S(2)}) async-start(), calls=%async_computation.3 | async-start | bytes 1114112 | tf_op jit(solution)/shard_map/all_gather | solution.py:361
  8.2 16.0 %copy-start.5 = (bf16[64,448]{1,0:T(8,128)(2,1)S(1)}, bf16[64,448]{1,0:T(8,128)(2,1)}, u32[]{:S(2)}) copy-start(bf16[64,448]{1,0:T(8,128)(2,1)} %get-tuple-element.32) | copy-start | bytes 172036
  8.2 144.2 %all-gather.6.cloned.1.call-start = ((), (), s32[]{:S(2)}) async-start(), calls=%async_computation.4 | async-start | bytes 2621440 | tf_op jit(solution)/shard_map/rows/all_gather | solution.py:403
  12.7 49.9 %collective-permute-start = (bf16[256,1024]{1,0:T(8,128)(2,1)}, bf16[256,1024]{1,0:T(8,128)(2,1)S(1)}, u32[]{:S(2)}, u32[]{:S(2)}) collective-permute-start(bf16[256,1024]{1,0:T(8,128)(2,1)} %get-tuple-element.28), channel_id=1, source_target_pairs={{0,8},{8,16},{16,24},{24,0},{1,9},{9,17},{17,25},{25,1},{2,10},{10... | collective-permute-start | bytes 1572872 | tf_op jit(solution)/shard_map/exchange/ppermute | solution.py:26
  16.7 45.9 %collective-permute-start.1 = (bf16[256,1024]{1,0:T(8,128)(2,1)}, bf16[256,1024]{1,0:T(8,128)(2,1)S(1)}, u32[]{:S(2)}, u32[]{:S(2)}) collective-permute-start(bf16[256,1024]{1,0:T(8,128)(2,1)} %get-tuple-element.29), channel_id=1, source_target_pairs={{0,16},{8,24},{16,0},{24,8},{1,17},{9,25},{17,1},{25,9},{2,18},{10... | collective-permute-start | bytes 1572872 | tf_op jit(solution)/shard_map/exchange/ppermute | solution.py:26
  21.2 41.4 %collective-permute-start.2 = (bf16[256,1024]{1,0:T(8,128)(2,1)}, bf16[256,1024]{1,0:T(8,128)(2,1)S(1)}, u32[]{:S(2)}, u32[]{:S(2)}) collective-permute-start(bf16[256,1024]{1,0:T(8,128)(2,1)} %get-tuple-element.30), channel_id=1, source_target_pairs={{0,24},{8,0},{16,8},{24,16},{1,25},{9,1},{17,9},{25,17},{2,26},{10... | collective-permute-start | bytes 1572872 | tf_op jit(solution)/shard_map/exchange/ppermute | solution.py:26
  62.5 0.8 copy-start.2
  62.5 1.0 copy-start.3
  62.6 1.2 copy-start.4
  63.7 16.6 %copy-start.1 = (f32[256,128]{1,0:T(8,128)S(1)}, f32[256,128]{1,0:T(8,128)}, u32[]{:S(2)}) copy-start(f32[256,128]{1,0:T(8,128)} %get-tuple-element.33.inverse) | copy-start | bytes 393220
  83.1 8.5 %copy-start.6 = (f32[1,2,64,64]{3,2,1,0:T(8,128)S(1)}, f32[1,2,64,64]{3,2,1,0:T(8,128)}, u32[]{:S(2)}) copy-start(f32[1,2,64,64]{3,2,1,0:T(8,128)} %param.29) | copy-start | bytes 98308
  83.1 9.2 %copy-start.8 = (bf16[16,128]{1,0:T(8,128)(2,1)S(1)}, bf16[16,128]{1,0:T(8,128)(2,1)}, u32[]{:S(2)}) copy-start(bf16[16,128]{1,0:T(8,128)(2,1)} %get-tuple-element.47) | copy-start | bytes 12292
  83.1 11.5 %copy-start.7 = (f32[72,128]{1,0:T(8,128)S(1)}, f32[72,128]{1,0:T(8,128)}, u32[]{:S(2)}) copy-start(f32[72,128]{1,0:T(8,128)} %get-tuple-element.39) | copy-start | bytes 110596
  88.1 33.7 %all-to-all-start.1 = ((bf16[4,512,128]{2,1,0:T(8,128)(2,1)}), bf16[4,512,128]{2,1,0:T(8,128)(2,1)S(1)}, u32[]{:S(2)}, u32[]{:S(2)}) async-start(bf16[4,512,128]{2,1,0:T(8,128)(2,1)} %get-tuple-element.40), calls=%async_computation.1 | async-start | bytes 1048576 | tf_op jit(solution)/shard_map/late_back/all_to_all | solution.py:405
  92.4 29.5 %collective-permute-start.3 = (bf16[16,128]{1,0:T(8,128)(2,1)S(1)}, bf16[16,128]{1,0:T(8,128)(2,1)S(1)}, u32[]{:S(2)}, u32[]{:S(2)}) collective-permute-start(bf16[16,128]{1,0:T(8,128)(2,1)S(1)} %copy-done.8), channel_id=1, source_target_pairs={{0,32},{32,64},{64,96},{96,128},{128,160},{160,192},{192,224},{224... | collective-permute-start | bytes 12296 | tf_op jit(solution)/shard_map/halo/ppermute | solution.py:26
  136.3 16.1 %collective-permute-start.4 = (bf16[4,256,256]{2,1,0:T(8,128)(2,1)S(1)}, bf16[4,256,256]{2,1,0:T(8,128)(2,1)S(1)}, u32[]{:S(2)}, u32[]{:S(2)}) collective-permute-start(bf16[4,256,256]{2,1,0:T(8,128)(2,1)S(1)} %all_to_all.16.same), channel_id=1, source_target_pairs={{0,1},{1,0},{2,3},{3,2},{4,5},{5,4},{6,7},{7,6},{8,9},{9,8},{10,11... | collective-permute-start | bytes 1572872 | tf_op jit(solution)/shard_map/ppermute | solution.py:433
  152.4 1.6 copy-start
Sparse Core Ops, SparseCore 0:
  9.4 67.0 all-gather.3
  88.2 41.1 all-gather.5

commit v4 on v3

v4 whole, which is shorter than its diff:
```python
import jax
import jax.numpy as jnp
from jax import lax
from jax.experimental import pallas as pl
from jax.experimental.pallas import tpu as pltpu
from jax.sharding import PartitionSpec as P


BLOCK = 64
HEAD = 64
LANES = 128
HALO = 16
RUN_ROWS = 80
norm_eps = 1e-06
decay_temper = 16.0
highest = lax.Precision.HIGHEST
f32 = jnp.float32
bf16 = jnp.bfloat16
limit = pltpu.CompilerParams(vmem_limit_bytes=24 << 20)


def shifted(x, axis, by, wrap):
    n = lax.axis_size(axis)
    if wrap:
        pairs = [(i, (i + by) % n) for i in range(n)]
    else:
        pairs = [(i, i + by) for i in range(n) if 0 <= i + by < n]
    return lax.ppermute(x, axis, pairs)


def call(kernel, outs, name, *args, scalars=1, aliases={}):
    smem = pl.BlockSpec(memory_space=pltpu.SMEM)
    vmem = pl.BlockSpec(memory_space=pltpu.VMEM)
    return pl.pallas_call(
        kernel,
        in_specs=[smem] * scalars + [vmem] * (len(args) - scalars),
        out_specs=[vmem] * len(outs),
        out_shape=outs,
        input_output_aliases=aliases,
        compiler_params=limit if name == "local" else None,
    )(*args)


def near(x):
    return pltpu.with_memory_space_constraint(x, pltpu.VMEM)


def struct(shape, dtype):
    return jax.ShapeDtypeStruct(shape, dtype)


def pack_kernel(
    own, key, value, pool, low, query, gate, pool_rows, state_rows, early, late
):
    at = 0
    for r in (key, value, pool, low):
        early[:, at : at + r.shape[1]] = r[...]
        at += r.shape[1]
    mine = pl.ds(pl.multiple_of(own[0] * LANES, LANES), LANES)
    for j, block in enumerate(
        (query[...], gate[...], pool_rows[:, mine], state_rows[:, mine])
    ):
        late[:, j * LANES : (j + 1) * LANES] = block


def prep_kernel(act, gain, x, inverse, held, arrived):
    tokens, width = act.shape
    rows = tokens // 4
    copies = []
    for c in range(4):
        at = pl.ds(c * rows, rows)
        copies.append(pltpu.make_async_copy(act.at[at], held.at[at], arrived.at[c]))
        copies[c].start()
    half = lax.broadcasted_iota(jnp.int32, (rows, LANES), 1) < HEAD
    for c in range(4):
        copies[c].wait()
        block = pl.ds(c * rows, rows)
        squares = jnp.zeros((rows, LANES), f32)
        for p in range(width // 512):
            tiles = []
            for q in range(4):
                at = p * 512 + q * LANES
                t = held[block, at : at + LANES].astype(f32)
                squares = squares + t * t
                tiles.append(t * gain[:, at : at + LANES])
            to = slice(p * LANES, (p + 1) * LANES)
            for j, (a, b) in enumerate(((tiles[0], tiles[2]), (tiles[1], tiles[3]))):
                x[2 * j, block, to] = jnp.where(half, a, pltpu.roll(b, HEAD, 1)).astype(bf16)
                x[2 * j + 1, block, to] = jnp.where(half, pltpu.roll(a, HEAD, 1), b).astype(bf16)
        total = jnp.sum(squares, axis=1, keepdims=True)
        inverse[block] = jnp.broadcast_to(lax.rsqrt(total / width + norm_eps), (rows, LANES))


def prepare(act, gain):
    tokens, width = act.shape
    vmem = pl.BlockSpec(memory_space=pltpu.VMEM)
    return pl.pallas_call(
        prep_kernel,
        in_specs=[pl.BlockSpec(memory_space=pl.ANY), vmem],
        out_specs=[vmem, vmem],
        out_shape=[struct((4, tokens, width // 4), bf16), struct((tokens, LANES), f32)],
        scratch_shapes=[pltpu.VMEM((tokens, width), bf16), pltpu.SemaphoreType.DMA((4,))],
        name="prep",
    )(act, gain)


def thirds(x):
    first = x.astype(bf16)
    left = x - first.astype(f32)
    second = left.astype(bf16)
    return first, second, (left - second.astype(f32)).astype(bf16)


def early_kernel(x, w, out, same_x, made, left):
    tokens = x.shape[1]
    half = lax.broadcasted_iota(jnp.int32, (tokens // 2, LANES), 1) < HEAD
    weight = w[...]
    copies = []
    for f in range(4):
        p = jnp.dot(x[f], weight, preferred_element_type=f32)
        for j in range(3):
            at = slice(j * tokens, (j + 1) * tokens)
            made[f, at] = p[:, j * LANES : (j + 1) * LANES].astype(bf16)
        d = jnp.concatenate([p[:, 3 * LANES :], p[:, 3 * LANES :]], axis=1)
        d = jnp.where(half, d[: tokens // 2], d[tokens // 2 :])
        made[f, 3 * tokens :] = d.astype(bf16)
        copies.append(pltpu.make_async_copy(made.at[f], out.at[f], left.at[f]))
        copies[f].start()
    for c in copies:
        c.wait()


def late_kernel(x, w, out, quarter, held, made, arrived, left):
    tokens = x.shape[1]
    columns = 2 * LANES
    into = pltpu.make_async_copy(w.at[:, :columns], held, arrived)
    into.start()
    across = pltpu.make_async_copy(w.at[:, columns:], quarter, left.at[4])
    across.start()
    into.wait()
    weight = held[...]
    copies = [across]
    for f in range(4):
        p = jnp.dot(x[f], weight, preferred_element_type=f32)
        made[f, :tokens] = p[:, :LANES].astype(bf16)
        made[f, tokens:] = p[:, LANES:].astype(bf16)
        copies.append(pltpu.make_async_copy(made.at[f], out.at[f], left.at[f]))
        copies[f + 1].start()
    for c in copies:
        c.wait()


def early_partials(x, w):
    _, tokens, _ = x.shape
    vmem = pl.BlockSpec(memory_space=pltpu.VMEM)
    anywhere = pl.BlockSpec(memory_space=pl.ANY)
    shape = (4, tokens * w.shape[1] // LANES, LANES)
    return pl.pallas_call(
        early_kernel,
        in_specs=[vmem, vmem],
        out_specs=[anywhere, vmem],
        out_shape=[struct(shape, bf16), pltpu.VMEM(x.shape, bf16)],
        scratch_shapes=[pltpu.VMEM(shape, bf16), pltpu.SemaphoreType.DMA((4,))],
        input_output_aliases={0: 1},
        compiler_params=limit,
        name="early_parts",
    )(x, w)


def late_partials(x, w):
    _, tokens, depth = x.shape
    vmem = pl.BlockSpec(memory_space=pltpu.VMEM)
    anywhere = pl.BlockSpec(memory_space=pl.ANY)
    shape = (4, 2 * tokens, LANES)
    return pl.pallas_call(
        late_kernel,
        in_specs=[vmem, anywhere],
        out_specs=[anywhere, anywhere],
        out_shape=[struct(shape, bf16), struct((depth, w.shape[1] - 2 * LANES), bf16)],
        scratch_shapes=[
            pltpu.VMEM((depth, 2 * LANES), bf16),
            pltpu.VMEM(shape, bf16),
            pltpu.SemaphoreType.DMA,
            pltpu.SemaphoreType.DMA((5,)),
        ],
        compiler_params=limit,
        name="late_parts",
    )(x, w)


def total_of(parts, at, rows):
    s = parts[0, at : at + rows].astype(f32)
    for k in (1, 2, 3):
        s = s + parts[k, at : at + rows].astype(f32)
    return s


def projected(parts, inverse, j):
    tokens = inverse.shape[0]
    return (total_of(parts, j * tokens, tokens) * inverse).astype(bf16)


def heads_of(x, half):
    return jnp.where(half, x[:HEAD], x[HEAD:])


def thirds(x):
    first = x.astype(bf16)
    left = x - first.astype(f32)
    second = left.astype(bf16)
    return first, second, (left - second.astype(f32)).astype(bf16)


def local_kernel(
    parts, inverse, second, bias, extra, keys, values, pool, tail, sums, prior, opening, run
):
    inv = inverse[...]
    tokens = inv.shape[0]
    keys[...] = projected(parts, inv, 0).astype(f32)
    values[...] = projected(parts, inv, 1).astype(f32)
    pooled = projected(parts, inv, 2)
    pool[...] = pooled
    tail[...] = pooled[tokens - HALO :]
    both = total_of(parts, 3 * tokens, tokens // 2)
    low = jnp.concatenate([both[:, :HEAD], both[:, HEAD:]], axis=0)
    low = (low * inv[:, :HEAD]).astype(bf16)
    x = jnp.dot(low, second[...], preferred_element_type=f32) + bias[...]
    rates = (jnp.minimum(x, 0.0) - jnp.log1p(jnp.exp(-jnp.abs(x)))) / decay_temper
    wide = lax.broadcasted_iota(jnp.int32, (2, LANES), 1) // HEAD
    pick = (wide == lax.broadcasted_iota(jnp.int32, (2, LANES), 0)).astype(f32)
    rates = rates + lax.dot_general(
        extra[...], pick, (((0,), (0,)), ((), ())), precision=highest, preferred_element_type=f32
    )
    r = lax.broadcasted_iota(jnp.int32, (BLOCK, BLOCK), 0)
    c = lax.broadcasted_iota(jnp.int32, (BLOCK, BLOCK), 1)
    lower = (r >= c).astype(f32)
    half = lax.broadcasted_iota(jnp.int32, (HEAD, LANES), 1) < HEAD
    state = jnp.zeros((HEAD, LANES), f32)
    before = jnp.zeros((1, LANES), f32)
    for n in range(tokens // BLOCK):
        at = slice(n * BLOCK, (n + 1) * BLOCK)
        total = jnp.dot(lower, rates[at], precision=highest, preferred_element_type=f32)
        sums[at] = total
        final = total[BLOCK - 1 :]
        pairs = lax.dot_general(
            values[at],
            keys[at] * jnp.exp(final - total),
            (((0,), (0,)), ((), ())),
            precision=highest,
            preferred_element_type=f32,
        )
        prior[at] = state
        opening[n : n + 1] = before
        state = jnp.exp(final) * state + heads_of(pairs, half)
        before = before + final
    run[:HEAD] = state.astype(bf16)
    row = lax.broadcasted_iota(jnp.int32, (RUN_ROWS - HEAD, LANES), 0)
    logs = jnp.zeros((RUN_ROWS - HEAD, LANES), f32)
    for j, part in enumerate(thirds(before)):
        logs = jnp.where(row == j, part.astype(f32), logs)
    run[HEAD:] = logs.astype(bf16)


def finish_kernel(
    sp,
    tp,
    runs,
    start,
    parts,
    inverse,
    pool,
    previous,
    keys,
    values,
    sums,
    prior,
    opening,
    gain,
    pool_weight,
    pool_scale,
    mine,
):
    inv = inverse[...]
    tokens = inv.shape[0]
    place = sp[0]
    state = start[...]
    for j in range(runs.shape[0] // RUN_ROWS):
        at = j * RUN_ROWS
        came = runs[at : at + RUN_ROWS].astype(f32)
        log = came[HEAD : HEAD + 1] + came[HEAD + 1 : HEAD + 2] + came[HEAD + 2 : HEAD + 3]
        state = jnp.where(j < place, jnp.exp(log) * state + came[:HEAD], state)
    queries = projected(parts, inv, 0).astype(f32) * HEAD ** (-0.5)
    outgate = projected(parts, inv, 1).astype(f32)
    half = lax.broadcasted_iota(jnp.int32, (HEAD, LANES), 1) < HEAD
    r = lax.broadcasted_iota(jnp.int32, (2 * BLOCK, BLOCK), 0) % BLOCK
    c = lax.broadcasted_iota(jnp.int32, (2 * BLOCK, BLOCK), 1)
    causal = r >= c

    def split(x):
        return jnp.concatenate([jnp.where(half, x, 0.0), jnp.where(half, 0.0, x)], axis=0)

    last = (((1,), (1,)), ((), ()))
    for n in range(tokens // BLOCK):
        at = slice(n * BLOCK, (n + 1) * BLOCK)
        total = sums[at]
        middle = total[BLOCK // 2 - 1 : BLOCK // 2]
        q = queries[at]
        scores = lax.dot_general(
            split(q * jnp.exp(total - middle)),
            keys[at] * jnp.exp(middle - total),
            last,
            precision=highest,
            preferred_element_type=f32,
        )
        scores = jnp.where(causal, scores, 0.0)
        within = jnp.dot(scores, values[at], precision=highest, preferred_element_type=f32)
        begin = prior[at] + jnp.exp(opening[n : n + 1]) * state
        carried = lax.dot_general(
            split(q * jnp.exp(total)),
            jnp.concatenate([begin, begin], axis=0),
            last,
            precision=highest,
            preferred_element_type=f32,
        )
        raw = heads_of(within + carried, half)
        square = raw * raw
        first = jnp.sum(jnp.where(half, square, 0.0), axis=1, keepdims=True)
        second = jnp.sum(jnp.where(half, 0.0, square), axis=1, keepdims=True)
        mean = jnp.where(half, first, second) / HEAD
        g = outgate[at]
        scaled = raw * lax.rsqrt(mean + norm_eps) * gain[...]
        done = (scaled * (g / (1.0 + jnp.exp(-g)))).astype(bf16)
        for to in range(mine.shape[0]):
            mine[to, at, LANES:] = done

    current = pool[...].astype(f32)
    extended = jnp.concatenate([previous[...].astype(f32), current], axis=0)

    def back(x, by):
        return x + pltpu.roll(x, by, 0)

    two = back(extended, 1)
    four = back(two, 2)
    eight = back(four, 4)
    sixteen = back(eight, 8)
    level = tp[0] % 4
    chosen = jnp.where(
        level == 0, two, jnp.where(level == 1, four, jnp.where(level == 2, eight, sixteen))
    )[HALO:]
    window = jnp.where(
        level == 0, 2.0, jnp.where(level == 1, 4.0, jnp.where(level == 2, 8.0, 16.0))
    )
    position = place * tokens + lax.broadcasted_iota(jnp.int32, (tokens, LANES), 0)
    counts = jnp.minimum(position.astype(f32) + 1.0, window)
    deviation = (chosen / counts - current).astype(bf16)
    mixture = jnp.dot(deviation, pool_weight[...], preferred_element_type=f32)
    done = (mixture * pool_scale[...]).astype(bf16)
    for to in range(mine.shape[0]):
        mine[to, :, :LANES] = done


def output_kernel(core, same, other, rows, out, held, arrived):
    steps = [(x, z, c) for z, c in ((same, core[0]), (other, 1 - core[0])) for x in range(same.shape[0])]
    copies = []
    for j, (x, _, c) in enumerate(steps):
        at = pl.ds(pl.multiple_of((2 * x + c) * LANES, LANES), LANES)
        copies.append(pltpu.make_async_copy(rows.at[:, at], held.at[j], arrived.at[j]))
        copies[j].start()
    total = jnp.zeros(out.shape, f32)
    for j, (x, z, _) in enumerate(steps):
        copies[j].wait()
        w = jnp.concatenate(
            [
                jnp.concatenate([held[j, f, :, :LANES], held[j, f, :, LANES:]], axis=0)
                for f in range(rows.shape[0])
            ],
            axis=1,
        )
        total = total + jnp.dot(z[x], w, preferred_element_type=f32)
    out[...] = total.astype(bf16)


def output(core, same, other, rows):
    tokens = same.shape[1]
    parts, _, width = rows.shape
    steps = 2 * same.shape[0]
    vmem = pl.BlockSpec(memory_space=pltpu.VMEM)
    return pl.pallas_call(
        output_kernel,
        in_specs=[
            pl.BlockSpec(memory_space=pltpu.SMEM),
            vmem,
            vmem,
            pl.BlockSpec(memory_space=pl.ANY),
        ],
        out_specs=vmem,
        out_shape=struct((tokens, parts * LANES), bf16),
        scratch_shapes=[
            pltpu.VMEM((steps, parts, LANES, width), bf16),
            pltpu.SemaphoreType.DMA((steps,)),
        ],
        name="output",
    )(core, same, other, rows)


def body(
    activations,
    input_norm_gain,
    pooling_channel_weight,
    query_projection_weight,
    key_projection_weight,
    value_projection_weight,
    output_gate_weight,
    decay_first_factor,
    decay_second_factor,
    decay_gate_bias,
    decay_extra_log,
    head_norm_gain,
    starting_state,
    pooling_group_weight,
    pooling_channel_scale,
    pooling_output_rows,
    attention_output_rows,
):
    _, tokens, width = activations.shape
    rows = key_projection_weight.shape[0]
    own = lax.axis_index("fs").astype(jnp.int32).reshape(1)
    tp = lax.axis_index("tp").astype(jnp.int32)
    early, late = call(
        pack_kernel,
        [struct((rows, 3 * LANES + HEAD), bf16), struct((rows, 4 * LANES), bf16)],
        "pack",
        own,
        key_projection_weight,
        value_projection_weight,
        pooling_channel_weight,
        decay_first_factor,
        query_projection_weight,
        output_gate_weight,
        pooling_output_rows,
        attention_output_rows,
    )
    late, early, activations = lax.optimization_barrier((late, early, activations))
    late = lax.all_gather(late, "sp", axis=0, tiled=True)
    x, inverse = prepare(activations.reshape(tokens, width), input_norm_gain.reshape(1, width))
    x = lax.all_to_all(x, "fs", 0, 0)
    early = lax.all_gather(early, "sp", axis=0, tiled=True)
    inverse = near(inverse)
    parts, x = early_partials(near(x), near(early))
    parts = lax.all_to_all(parts, "fs", 0, 0)
    wide = pltpu.VMEM((tokens, LANES), f32)
    keys, values, pool, tail, sums, prior, opening, run = call(
        local_kernel,
        [
            wide,
            wide,
            pltpu.VMEM((tokens, LANES), bf16),
            struct((HALO, LANES), bf16),
            wide,
            wide,
            pltpu.VMEM((tokens // BLOCK, LANES), f32),
            struct((RUN_ROWS, LANES), bf16),
        ],
        "local",
        near(parts),
        inverse,
        decay_second_factor,
        decay_gate_bias.reshape(1, LANES),
        decay_extra_log,
        scalars=0,
    )
    previous = shifted(tail, "sp", 1, False)
    start = starting_state[0].transpose(2, 0, 1).reshape(HEAD, LANES)
    late, run = lax.optimization_barrier((late, run))
    late, quarter = late_partials(near(x), late)
    late, quarter, run = lax.optimization_barrier((late, quarter, run))
    out_rows = lax.all_gather(quarter, "fs")
    late = lax.all_to_all(late, "fs", 0, 0)
    runs = lax.all_gather(run, "sp", axis=0, tiled=True)
    peers = lax.axis_size("tp")
    (mine,) = call(
        finish_kernel,
        [struct((peers // 2, tokens, 2 * LANES), bf16)],
        "finish",
        lax.axis_index("sp").astype(jnp.int32).reshape(1),
        tp.reshape(1),
        near(runs),
        near(start),
        near(late),
        inverse,
        near(pool),
        near(previous),
        near(keys),
        near(values),
        near(sums),
        near(prior),
        near(opening),
        head_norm_gain.reshape(1, LANES),
        pooling_group_weight[0],
        pooling_channel_scale.reshape(1, LANES),
        scalars=2,
    )
    groups = [[c + 2 * x for x in range(peers // 2)] for c in range(2)]
    same = lax.all_to_all(mine, "tp", 0, 0, axis_index_groups=groups)
    other = lax.ppermute(same, "tp", [(i, i ^ 1) for i in range(peers)])
    return output((tp & 1).reshape(1), near(same), near(other), out_rows)[None]


def solution(mesh):
    in_specs = (
        P("fs", "sp", None),
        P(),
        P(("sp", "fs"), "tp"),
        P(("sp", "fs"), "tp"),
        P(("sp", "fs"), "tp"),
        P(("sp", "fs"), "tp"),
        P(("sp", "fs"), "tp"),
        P(("sp", "fs"), None),
        P(None, "tp"),
        P("tp"),
        P("tp", "sp"),
        P("tp"),
        P("fs", "tp", None, None),
        P("tp", None, None),
        P("tp"),
        P("sp", "tp"),
        P("sp", "tp"),
    )
    out_specs = P("fs", "sp", "tp")

    return jax.shard_map(body, mesh=mesh, in_specs=in_specs, out_specs=out_specs, check_vma=False)
```

time: 163 us -> 165 us (1.012)
  waiting for transfers between devices: 1.55 us -> 14.8 us
  blocking collectives: 88.9 us -> 83.6 us
  Pallas kernels: 22 us -> 17.8 us
  local copies, waits for them, and re-layouts: 3.78 us -> 1.31 us
    all_gather x1, waiting for transfers between devices: 0.01 us -> 12.5 us  [body(): late = lax.all_gather(late, 'sp', axis=0, tiled=True)]
    ppermute x4 -> x1, starting transfers between devices: 13.7 us -> 2.52 us  [shifted(): return lax.ppermute(x, axis, pairs)]
    ppermute x1, starting transfers between devices: 14.6 us -> 21.3 us  [body(): other = lax.ppermute(same, 'tp', [(i, i ^ 1) for i in range(peers)])]
    all_to_all x1 -> x2, starting transfers between devices: 3.48 us -> 9.45 us  [the longest x1 5.14 us: body(): x = lax.all_to_all(x, 'fs', 0, 0)]
    all_gather x1, blocking collectives: 27.2 us -> 21.9 us  [body(): runs = lax.all_gather(run, 'sp', axis=0, tiled=True)]
    pallas_call x4 -> x3, Pallas kernels: 8.53 us -> 5.88 us  [call(): pl.pallas_call(kernel, in_specs=[smem] * scalars + [vmem] * (len(args) -...]
    pallas_call x3 -> x4, Pallas kernels: 13.4 us -> 11.9 us  [the longest x1 4.41 us: prepare(): pl.pallas_call(prep_kernel, in_specs=[pl.BlockSpec(memory_space=pl.ANY),...]
  transfers between devices with their start and end apart: 8 -> 6, of which waited for: 1 -> 2; matrix products, arithmetic and copies ran while one was open for 1% -> 0% of each run, Pallas kernels for 9% -> 5%
where the time goes in v4:
time: 165 us; the launch traced here: 164 us
  blocking collectives  83.6 us (51%)
  starting transfers between devices  33.3 us (20%)
  Pallas kernels  17.8 us (11%)
  waiting for transfers between devices  14.8 us (9%)
  between operations  13.5 us (8%)
    all_gather x1, blocking collectives, body(): early = lax.all_gather(early, 'sp', axis=0, tiled=True)  37.1 us
    all_gather x1, blocking collectives, body(): runs = lax.all_gather(run, 'sp', axis=0, tiled=True)  21.9 us
    ppermute x1, starting transfers between devices, body(): other = lax.ppermute(same, 'tp', [(i, i ^ 1) for i in range(peers)])  21.3 us
    all_to_all x1, blocking collectives, body(): parts = lax.all_to_all(parts, 'fs', 0, 0)  13.8 us
    all_gather x1, waiting for transfers between devices, body(): late = lax.all_gather(late, 'sp', axis=0, tiled=True)  12.5 us
    all_to_all x1, blocking collectives, body(): same = lax.all_to_all(mine, 'tp', 0, 0, axis_index_groups=groups)  10.8 us
    pallas_call x3, Pallas kernels, call(): pl.pallas_call(kernel, in_specs=[smem] * scalars + [vmem] * (len(args) -...  5.88 us
    all_to_all x1, starting transfers between devices, body(): x = lax.all_to_all(x, 'fs', 0, 0)  5.14 us
  transfers between devices with their start and end apart: 6, of which 2 were waited for; matrix products, arithmetic and copies ran while one was open for 0% of the time, Pallas kernels for 5%

profile of v4, /device:TPU:1, one launch (start us, length us, event | category | flops | bytes accessed | tf_op | source)
XLA Modules:
  0.0 164.3 jit_solution(7606972697050758450)
XLA Ops:
  6.5 1.6 %shard_map.163 = (bf16[64,448]{1,0:T(8,128)(2,1)}, bf16[64,512]{1,0:T(8,128)(2,1)}) custom-call(s32[1]{0:T(128)} %bitcast.3.own, bf16[64,128]{1,0:T(8,128)(2,1)} %key.1, bf16[64,128]{1,0:T(8,128)(2,1)} %value.1, bf16[64,128]{1,0:T(8,128)(2,1)} %pool.1, bf16[64,64]{1,0:T(8,128)(2,1)} %low.1, bf16[64,128]{1,0:T(8,128)(2,1)} %query.1, bf16[64,128]{1,0:T(8,128)(2,1)} %gate.1, ...), custom_call_target="tpu_custom_call" | custom-call | tf_op jit(solution)/shard_map/pallas_call | solution.py:34
  8.2 4.4 %prep.1 = (bf16[4,256,1024]{2,1,0:T(8,128)(2,1)}, f32[256,128]{1,0:T(8,128)}) custom-call(bf16[256,4096]{1,0:T(8,128)(2,1)} %bitcast.18, f32[1,4096]{1,0:T(1,128)} %bitcast.22), custom_call_target="tpu_custom_call" | custom-call | tf_op jit(solution)/shard_map/prep/pallas_call | solution.py:97
  12.6 5.1 %all-to-all-start = ((bf16[4,256,1024]{2,1,0:T(8,128)(2,1)}), bf16[4,256,1024]{2,1,0:T(8,128)(2,1)S(1)}, u32[]{:S(2)}, u32[]{:S(2)}) async-start(bf16[4,256,1024]{2,1,0:T(8,128)(2,1)} %get-tuple-element.32), calls=%async_computation | async-start | bytes 4194304 | tf_op jit(solution)/shard_map/all_to_all | solution.py:446
  17.8 0.7 all-gather.4.cloned.1.call-update
  18.5 0.0 all-gather.6.cloned.1.call-start
  18.5 37.1 %all_gather.15.w = bf16[1024,448]{1,0:T(8,128)(2,1)S(1)} all-gather(bf16[64,448]{1,0:T(8,128)(2,1)S(1)} %copy-done.5), channel_id=1, replica_groups=mesh['sp'=16,'fs'=4,'tp'=8] {'sp'}, dimensions={0}, use_global_device_ids=true | all-gather | bytes 974848 | tf_op jit(solution)/shard_map/all_gather | solution.py:447
  55.7 0.0 all-to-all-done.x
  55.7 3.2 %early_parts.1 = (bf16[4,896,128]{2,1,0:T(8,128)(2,1)S(1)}, bf16[4,256,1024]{2,1,0:T(8,128)(2,1)S(1)}) custom-call(bf16[4,256,1024]{2,1,0:T(8,128)(2,1)S(1)} %all-to-all-done.x, bf16[1024,448]{1,0:T(8,128)(2,1)S(1)} %all_gather.15.w), custom_call_target="tpu_custom_call", output_to_operand_aliasing={{1}: (0, {})} | custom-call | tf_op jit(solution)/shard_map/early_parts/pallas_call | solution.py:158
  58.9 13.8 %all_to_all.20.parts = bf16[4,896,128]{2,1,0:T(8,128)(2,1)S(1)} all-to-all(bf16[4,896,128]{2,1,0:T(8,128)(2,1)S(1)} %get-tuple-element.36), channel_id=1, replica_groups=mesh['sp'=16,'fs'=4,'tp'=8] {'fs'}, dimensions={0} | all-to-all | bytes 1835008 | tf_op jit(solution)/shard_map/all_to_all | solution.py:450
  72.7 1.4 shard_map.164
  74.1 12.5 %all-gather.4.cloned.1.call-done.w = bf16[1024,512]{1,0:T(8,128)(2,1)} async-done(((bf16[64,512]{1,0:T(8,128)(2,1)}), bf16[1024,512]{1,0:T(8,128)(2,1)}) %all-gather.4.cloned.1.call-update) | async-done | bytes 1048592 | tf_op jit(solution)/shard_map/all_gather | solution.py:444
  86.6 1.2 copy-done
  87.9 1.5 late_parts.1
  89.4 0.0 all-gather.6.cloned.1.call-update
  89.4 4.3 %all-to-all-start.2 = ((bf16[4,512,128]{2,1,0:T(8,128)(2,1)}), bf16[4,512,128]{2,1,0:T(8,128)(2,1)S(1)}, u32[]{:S(2)}, u32[]{:S(2)}) async-start(bf16[4,512,128]{2,1,0:T(8,128)(2,1)} %get-tuple-element.44), calls=%async_computation.2 | async-start | bytes 1048576 | tf_op jit(solution)/shard_map/all_to_all | solution.py:478
  93.7 0.1 copy.20.start
  93.8 2.5 %collective-permute-start = (bf16[16,128]{1,0:T(8,128)(2,1)S(1)}, bf16[16,128]{1,0:T(8,128)(2,1)S(1)}, u32[]{:S(2)}, u32[]{:S(2)}) collective-permute-start(bf16[16,128]{1,0:T(8,128)(2,1)S(1)} %get-tuple-element.46), channel_id=1, source_target_pairs={{0,32},{32,64},{64,96},{96,128},{128,160},{160,192},{192,224},{224... | collective-permute-start | bytes 12296 | tf_op jit(solution)/shard_map/ppermute | solution.py:28
  96.3 21.9 %all_gather.17.runs = bf16[1280,128]{1,0:T(8,128)(2,1)S(1)} all-gather(bf16[80,128]{1,0:T(8,128)(2,1)S(1)} %get-tuple-element.43), channel_id=1, replica_groups=mesh['sp'=16,'fs'=4,'tp'=8] {'sp'}, dimensions={0}, use_global_device_ids=true | all-gather | bytes 348160 | tf_op jit(solution)/shard_map/all_gather | solution.py:479
  118.2 0.0 all-to-all-done.2.parts
  118.2 2.8 %shard_map.165 = bf16[4,256,256]{2,1,0:T(8,128)(2,1)} custom-call(s32[1]{0:T(128)} %bitcast.1.sp, s32[1]{0:T(128)} %bitcast.2.tp, bf16[1280,128]{1,0:T(8,128)(2,1)S(1)} %all_gather.17.runs, f32[64,128]{1,0:T(8,128)S(1)} %copy.20.start, bf16[4,512,128]{2,1,0:T(8,128)(2,1)S(1)} %all-to-all-done.2.parts, f32[256,128]{1,0:T(8,128)S(1)} %copy-done.1, ...), custom_call_target="tpu_custom_call" | custom-call | tf_op jit(solution)/shard_map/pallas_call | solution.py:34
  121.0 10.8 %all_to_all.21.same = bf16[4,256,256]{2,1,0:T(8,128)(2,1)S(1)} all-to-all(bf16[4,256,256]{2,1,0:T(8,128)(2,1)} %shard_map.165), channel_id=1, replica_groups={{0,2,4,6},{1,3,5,7},{8,10,12,14},{9,11,13,15},{16,18,20,22},{17,19,21,2..., dimensions={0} | all-to-all | bytes 1048576 | tf_op jit(solution)/shard_map/all_to_all | solution.py:504
  131.8 21.3 %collective-permute-start.1 = (bf16[4,256,256]{2,1,0:T(8,128)(2,1)S(1)}, bf16[4,256,256]{2,1,0:T(8,128)(2,1)S(1)}, u32[]{:S(2)}, u32[]{:S(2)}) collective-permute-start(bf16[4,256,256]{2,1,0:T(8,128)(2,1)S(1)} %all_to_all.21.same), channel_id=1, source_target_pairs={{0,1},{1,0},{2,3},{3,2},{4,5},{5,4},{6,7},{7,6},{8,9},{9,8},{10,11... | collective-permute-start | bytes 1572872 | tf_op jit(solution)/shard_map/ppermute | solution.py:505
  153.1 1.5 collective-permute-done.1.other
  154.6 2.8 %output.1 = bf16[256,512]{1,0:T(8,128)(2,1)} custom-call(s32[1]{0:T(128)} %bitcast.core, bf16[4,256,256]{2,1,0:T(8,128)(2,1)S(1)} %all_to_all.21.same, bf16[4,256,256]{2,1,0:T(8,128)(2,1)S(1)} %collective-permute-done.1.other, bf16[4,1024,256]{2,1,0:T(8,128)(2,1)} %bitcast.19), custom_call_target="tpu_custom_call" | custom-call | tf_op jit(solution)/shard_map/output/pallas_call | solution.py:388
  (16 shorter events, 0.0 us)
Async XLA Ops:
  12.6 5.9 %copy-start.5 = (bf16[64,448]{1,0:T(8,128)(2,1)S(1)}, bf16[64,448]{1,0:T(8,128)(2,1)}, u32[]{:S(2)}) copy-start(bf16[64,448]{1,0:T(8,128)(2,1)} %get-tuple-element.33) | copy-start | bytes 172036
  12.6 43.1 %all-to-all-start = ((bf16[4,256,1024]{2,1,0:T(8,128)(2,1)}), bf16[4,256,1024]{2,1,0:T(8,128)(2,1)S(1)}, u32[]{:S(2)}, u32[]{:S(2)}) async-start(bf16[4,256,1024]{2,1,0:T(8,128)(2,1)} %get-tuple-element.32), calls=%async_computation | async-start | bytes 4194304 | tf_op jit(solution)/shard_map/all_to_all | solution.py:446
  17.8 68.9 %all-gather.4.cloned.1.call-start = ((), (), s32[]{:S(2)}) async-start(), calls=%async_computation.4 | async-start | bytes 1114112 | tf_op jit(solution)/shard_map/all_gather | solution.py:444
  18.5 136.1 %all-gather.6.cloned.1.call-start = ((), (), s32[]{:S(2)}) async-start(), calls=%async_computation.5 | async-start | bytes 2621440 | tf_op jit(solution)/shard_map/all_gather | solution.py:477
  55.7 17.0 %copy-start.1 = (f32[256,128]{1,0:T(8,128)S(1)}, f32[256,128]{1,0:T(8,128)}, u32[]{:S(2)}) copy-start(f32[256,128]{1,0:T(8,128)} %get-tuple-element.37.inverse) | copy-start | bytes 393220
  55.7 17.0 %copy-start.2 = (bf16[64,128]{1,0:T(8,128)(2,1)S(1)}, bf16[64,128]{1,0:T(8,128)(2,1)}, u32[]{:S(2)}) copy-start(bf16[64,128]{1,0:T(8,128)(2,1)} %second.1) | copy-start | bytes 49156
  55.7 17.0 %copy-start.3 = (f32[2,256]{1,0:T(2,128)S(1)}, f32[2,256]{1,0:T(2,128)}, u32[]{:S(2)}) copy-start(f32[2,256]{1,0:T(2,128)} %extra.1) | copy-start | bytes 6148
  55.7 17.0 %copy-start.4 = (f32[128]{0:T(128)S(1)}, f32[128]{0:T(128)}, u32[]{:S(2)}) copy-start(f32[128]{0:T(128)} %param.26) | copy-start | bytes 1540
  86.6 1.2 copy-start
  87.9 5.8 %copy-start.6 = (f32[1,2,64,64]{3,2,1,0:T(8,128)S(1)}, f32[1,2,64,64]{3,2,1,0:T(8,128)}, u32[]{:S(2)}) copy-start(f32[1,2,64,64]{3,2,1,0:T(8,128)} %param.29) | copy-start | bytes 98308
  89.4 28.8 %all-to-all-start.2 = ((bf16[4,512,128]{2,1,0:T(8,128)(2,1)}), bf16[4,512,128]{2,1,0:T(8,128)(2,1)S(1)}, u32[]{:S(2)}, u32[]{:S(2)}) async-start(bf16[4,512,128]{2,1,0:T(8,128)(2,1)} %get-tuple-element.44), calls=%async_computation.2 | async-start | bytes 1048576 | tf_op jit(solution)/shard_map/all_to_all | solution.py:478
  93.8 24.4 %collective-permute-start = (bf16[16,128]{1,0:T(8,128)(2,1)S(1)}, bf16[16,128]{1,0:T(8,128)(2,1)S(1)}, u32[]{:S(2)}, u32[]{:S(2)}) collective-permute-start(bf16[16,128]{1,0:T(8,128)(2,1)S(1)} %get-tuple-element.46), channel_id=1, source_target_pairs={{0,32},{32,64},{64,96},{96,128},{128,160},{160,192},{192,224},{224... | collective-permute-start | bytes 12296 | tf_op jit(solution)/shard_map/ppermute | solution.py:28
  131.8 22.8 %collective-permute-start.1 = (bf16[4,256,256]{2,1,0:T(8,128)(2,1)S(1)}, bf16[4,256,256]{2,1,0:T(8,128)(2,1)S(1)}, u32[]{:S(2)}, u32[]{:S(2)}) collective-permute-start(bf16[4,256,256]{2,1,0:T(8,128)(2,1)S(1)} %all_to_all.21.same), channel_id=1, source_target_pairs={{0,1},{1,0},{2,3},{3,2},{4,5},{5,4},{6,7},{7,6},{8,9},{9,8},{10,11... | collective-permute-start | bytes 1572872 | tf_op jit(solution)/shard_map/ppermute | solution.py:505
Sparse Core Ops, SparseCore 0:
  20.6 65.9 all-gather.3
  89.5 45.3 all-gather.5

commit v5 on v4

--- a/solution.py
+++ b/solution.py
@@ -10,22 +10,13 @@
 HEAD = 64
 LANES = 128
 HALO = 16
-RUN_ROWS = 80
+RUN_ROWS = 96
 norm_eps = 1e-06
 decay_temper = 16.0
 highest = lax.Precision.HIGHEST
 f32 = jnp.float32
 bf16 = jnp.bfloat16
 limit = pltpu.CompilerParams(vmem_limit_bytes=24 << 20)
-
-
-def shifted(x, axis, by, wrap):
-    n = lax.axis_size(axis)
-    if wrap:
-        pairs = [(i, (i + by) % n) for i in range(n)]
-    else:
-        pairs = [(i, i + by) for i in range(n) if 0 <= i + by < n]
-    return lax.ppermute(x, axis, pairs)
 
 
 def call(kernel, outs, name, *args, scalars=1, aliases={}):
@@ -50,17 +41,35 @@
 
 
 def pack_kernel(
-    own, key, value, pool, low, query, gate, pool_rows, state_rows, early, late
+    own, key, value, pool, low, query, gate, pool_rows, state_rows, early, late, moved
 ):
-    at = 0
-    for r in (key, value, pool, low):
-        early[:, at : at + r.shape[1]] = r[...]
-        at += r.shape[1]
     mine = pl.ds(pl.multiple_of(own[0] * LANES, LANES), LANES)
-    for j, block in enumerate(
-        (query[...], gate[...], pool_rows[:, mine], state_rows[:, mine])
+    moves = []
+    for out, blocks in (
+        (late, (query, gate, pool_rows.at[:, mine], state_rows.at[:, mine])),
+        (early, (key, value, pool, low)),
     ):
-        late[:, j * LANES : (j + 1) * LANES] = block
+        at = 0
+        for block in blocks:
+            width = block.shape[1]
+            to = out.at[:, at : at + width]
+            moves.append(pltpu.make_async_copy(block, to, moved.at[len(moves)]))
+            moves[-1].start()
+            at += width
+    for move in moves:
+        move.wait()
+
+
+def pack(own, blocks, outs):
+    anywhere = pl.BlockSpec(memory_space=pl.ANY)
+    return pl.pallas_call(
+        pack_kernel,
+        in_specs=[pl.BlockSpec(memory_space=pltpu.SMEM)] + [anywhere] * len(blocks),
+        out_specs=[anywhere] * len(outs),
+        out_shape=outs,
+        scratch_shapes=[pltpu.SemaphoreType.DMA((len(blocks),))],
+        name="pack",
+    )(own, *blocks)
 
 
 def prep_kernel(act, gain, x, inverse, held, arrived):
@@ -174,7 +183,7 @@
     shape = (4, 2 * tokens, LANES)
     return pl.pallas_call(
         late_kernel,
-        in_specs=[vmem, anywhere],
+        in_specs=[vmem, pl.BlockSpec(memory_space=pltpu.HBM)],
         out_specs=[anywhere, anywhere],
         out_shape=[struct(shape, bf16), struct((depth, w.shape[1] - 2 * LANES), bf16)],
         scratch_shapes=[
@@ -185,7 +194,7 @@
         ],
         compiler_params=limit,
         name="late_parts",
-    )(x, w)
+    )(x, pltpu.with_memory_space_constraint(w, pltpu.HBM))
 
 
 def total_of(parts, at, rows):
@@ -212,7 +221,7 @@
 
 
 def local_kernel(
-    parts, inverse, second, bias, extra, keys, values, pool, tail, sums, prior, opening, run
+    parts, inverse, second, bias, extra, keys, values, pool, sums, prior, opening, run
 ):
     inv = inverse[...]
     tokens = inv.shape[0]
@@ -220,7 +229,7 @@
     values[...] = projected(parts, inv, 1).astype(f32)
     pooled = projected(parts, inv, 2)
     pool[...] = pooled
-    tail[...] = pooled[tokens - HALO :]
+    run[RUN_ROWS - HALO :] = pooled[tokens - HALO :]
     both = total_of(parts, 3 * tokens, tokens // 2)
     low = jnp.concatenate([both[:, :HEAD], both[:, HEAD:]], axis=0)
     low = (low * inv[:, :HEAD]).astype(bf16)
@@ -254,11 +263,11 @@
         state = jnp.exp(final) * state + heads_of(pairs, half)
         before = before + final
     run[:HEAD] = state.astype(bf16)
-    row = lax.broadcasted_iota(jnp.int32, (RUN_ROWS - HEAD, LANES), 0)
-    logs = jnp.zeros((RUN_ROWS - HEAD, LANES), f32)
+    row = lax.broadcasted_iota(jnp.int32, (HALO, LANES), 0)
+    logs = jnp.zeros((HALO, LANES), f32)
     for j, part in enumerate(thirds(before)):
         logs = jnp.where(row == j, part.astype(f32), logs)
-    run[HEAD:] = logs.astype(bf16)
+    run[HEAD : HEAD + HALO] = logs.astype(bf16)
 
 
 def finish_kernel(
@@ -269,7 +278,6 @@
     parts,
     inverse,
     pool,
-    previous,
     keys,
     values,
     sums,
@@ -284,9 +292,8 @@
     tokens = inv.shape[0]
     place = sp[0]
     state = start[...]
-    for j in range(runs.shape[0] // RUN_ROWS):
-        at = j * RUN_ROWS
-        came = runs[at : at + RUN_ROWS].astype(f32)
+    for j in range(runs.shape[0]):
+        came = runs[j].astype(f32)
         log = came[HEAD : HEAD + 1] + came[HEAD + 1 : HEAD + 2] + came[HEAD + 2 : HEAD + 3]
         state = jnp.where(j < place, jnp.exp(log) * state + came[:HEAD], state)
     queries = projected(parts, inv, 0).astype(f32) * HEAD ** (-0.5)
@@ -334,7 +341,9 @@
             mine[to, at, LANES:] = done
 
     current = pool[...].astype(f32)
-    extended = jnp.concatenate([previous[...].astype(f32), current], axis=0)
+    previous = runs[jnp.maximum(place - 1, 0), RUN_ROWS - HALO :].astype(f32)
+    previous = jnp.where(place > 0, previous, 0.0)
+    extended = jnp.concatenate([previous, current], axis=0)
 
     def back(x, by):
         return x + pltpu.roll(x, by, 0)
@@ -359,48 +368,48 @@
         mine[to, :, :LANES] = done
 
 
-def output_kernel(core, same, other, rows, out, held, arrived):
-    steps = [(x, z, c) for z, c in ((same, core[0]), (other, 1 - core[0])) for x in range(same.shape[0])]
+def output_kernel(core, z, rows, *rest):
+    *before, out, held, arrived = rest
     copies = []
-    for j, (x, _, c) in enumerate(steps):
-        at = pl.ds(pl.multiple_of((2 * x + c) * LANES, LANES), LANES)
-        copies.append(pltpu.make_async_copy(rows.at[:, at], held.at[j], arrived.at[j]))
-        copies[j].start()
+    for x in range(z.shape[0]):
+        at = pl.ds(pl.multiple_of((2 * x + core[0]) * LANES, LANES), LANES)
+        copies.append(pltpu.make_async_copy(rows.at[:, at], held.at[x], arrived.at[x]))
+        copies[x].start()
     total = jnp.zeros(out.shape, f32)
-    for j, (x, z, _) in enumerate(steps):
-        copies[j].wait()
+    for b in before:
+        total = b[...]
+    for x in range(z.shape[0]):
+        copies[x].wait()
         w = jnp.concatenate(
             [
-                jnp.concatenate([held[j, f, :, :LANES], held[j, f, :, LANES:]], axis=0)
+                jnp.concatenate([held[x, f, :, :LANES], held[x, f, :, LANES:]], axis=0)
                 for f in range(rows.shape[0])
             ],
             axis=1,
         )
         total = total + jnp.dot(z[x], w, preferred_element_type=f32)
-    out[...] = total.astype(bf16)
-
-
-def output(core, same, other, rows):
-    tokens = same.shape[1]
+    out[...] = total.astype(out.dtype)
+
+
+def output(core, z, rows, before, out):
+    vmem = pl.BlockSpec(memory_space=pltpu.VMEM)
+    steps = z.shape[0]
     parts, _, width = rows.shape
-    steps = 2 * same.shape[0]
-    vmem = pl.BlockSpec(memory_space=pltpu.VMEM)
     return pl.pallas_call(
         output_kernel,
         in_specs=[
             pl.BlockSpec(memory_space=pltpu.SMEM),
             vmem,
-            vmem,
             pl.BlockSpec(memory_space=pl.ANY),
-        ],
+        ]
+        + [vmem] * len(before),
         out_specs=vmem,
-        out_shape=struct((tokens, parts * LANES), bf16),
+        out_shape=out,
         scratch_shapes=[
             pltpu.VMEM((steps, parts, LANES, width), bf16),
             pltpu.SemaphoreType.DMA((steps,)),
         ],
-        name="output",
-    )(core, same, other, rows)
+    )(core, near(z), rows, *before)
 
 
 def body(
@@ -424,38 +433,38 @@
 ):
     _, tokens, width = activations.shape
     rows = key_projection_weight.shape[0]
+    columns = pooling_output_rows.shape[1]
     own = lax.axis_index("fs").astype(jnp.int32).reshape(1)
     tp = lax.axis_index("tp").astype(jnp.int32)
-    early, late = call(
-        pack_kernel,
+    early, late = pack(
+        own,
+        (
+            key_projection_weight,
+            value_projection_weight,
+            pooling_channel_weight,
+            decay_first_factor,
+            query_projection_weight,
+            output_gate_weight,
+            pooling_output_rows,
+            attention_output_rows,
+        ),
         [struct((rows, 3 * LANES + HEAD), bf16), struct((rows, 4 * LANES), bf16)],
-        "pack",
-        own,
-        key_projection_weight,
-        value_projection_weight,
-        pooling_channel_weight,
-        decay_first_factor,
-        query_projection_weight,
-        output_gate_weight,
-        pooling_output_rows,
-        attention_output_rows,
     )
     late, early, activations = lax.optimization_barrier((late, early, activations))
     late = lax.all_gather(late, "sp", axis=0, tiled=True)
     x, inverse = prepare(activations.reshape(tokens, width), input_norm_gain.reshape(1, width))
     x = lax.all_to_all(x, "fs", 0, 0)
-    early = lax.all_gather(early, "sp", axis=0, tiled=True)
+    early = lax.all_gather(early, "sp").reshape(-1, early.shape[1])
     inverse = near(inverse)
     parts, x = early_partials(near(x), near(early))
     parts = lax.all_to_all(parts, "fs", 0, 0)
     wide = pltpu.VMEM((tokens, LANES), f32)
-    keys, values, pool, tail, sums, prior, opening, run = call(
+    keys, values, pool, sums, prior, opening, run = call(
         local_kernel,
         [
             wide,
             wide,
             pltpu.VMEM((tokens, LANES), bf16),
-            struct((HALO, LANES), bf16),
             wide,
             wide,
             pltpu.VMEM((tokens // BLOCK, LANES), f32),
@@ -469,14 +478,13 @@
         decay_extra_log,
         scalars=0,
     )
-    previous = shifted(tail, "sp", 1, False)
     start = starting_state[0].transpose(2, 0, 1).reshape(HEAD, LANES)
     late, run = lax.optimization_barrier((late, run))
     late, quarter = late_partials(near(x), late)
     late, quarter, run = lax.optimization_barrier((late, quarter, run))
     out_rows = lax.all_gather(quarter, "fs")
     late = lax.all_to_all(late, "fs", 0, 0)
-    runs = lax.all_gather(run, "sp", axis=0, tiled=True)
+    runs = lax.all_gather(run, "sp")
     peers = lax.axis_size("tp")
     (mine,) = call(
         finish_kernel,
@@ -489,7 +497,6 @@
         near(late),
         inverse,
         near(pool),
-        near(previous),
         near(keys),
         near(values),
         near(sums),
@@ -502,8 +509,12 @@
     )
     groups = [[c + 2 * x for x in range(peers // 2)] for c in range(2)]
     same = lax.all_to_all(mine, "tp", 0, 0, axis_index_groups=groups)
+    same, out_rows = lax.optimization_barrier((same, out_rows))
     other = lax.ppermute(same, "tp", [(i, i ^ 1) for i in range(peers)])
-    return output((tp & 1).reshape(1), near(same), near(other), out_rows)[None]
+    core = (tp & 1).reshape(1)
+    half = output(core, same, out_rows, (), pltpu.VMEM((tokens, columns), f32))
+    result = output(1 - core, other, out_rows, (near(half),), struct((tokens, columns), bf16))
+    return result[None]
 
 
 def solution(mesh):

time: 165 us -> 181 us (1.097)
  Pallas kernels: 17.8 us -> 37.9 us
  starting transfers between devices: 33.3 us -> 26.7 us
  waiting for transfers between devices: 14.8 us -> 17.6 us
    pallas_call x1 -> x2, Pallas kernels: 1.5 us -> 22.2 us  [the longest x1 17 us: late_partials(): pl.pallas_call(late_kernel, in_specs=[vmem, pl.BlockSpec(memory_space=plt...]
    all_gather x1, waiting for transfers between devices: 0.01 us -> 4.32 us  [body(): out_rows = lax.all_gather(quarter, 'fs')]
    ppermute x1, starting transfers between devices: 21.3 us -> 17.2 us  [body(): other = lax.ppermute(same, 'tp', [(i, i ^ 1) for i in range(peers)])]
    ppermute x1 -> x0, starting transfers between devices: 2.52 us -> none  [shifted(): return lax.ppermute(x, axis, pairs)]
    pallas_call x3 -> x2, Pallas kernels: 5.88 us -> 4.23 us  [call(): pl.pallas_call(kernel, in_specs=[smem] * scalars + [vmem] * (len(args) -...]
    pallas_call x1 -> x2, Pallas kernels: 2.81 us -> 3.88 us  [output(): pl.pallas_call(output_kernel, in_specs=[pl.BlockSpec(memory_space=pltpu.S...]
  transfers between devices with their start and end apart: 6 -> 5, of which waited for: 2 -> 2; matrix products, arithmetic and copies ran while one was open for 0% -> 0% of each run, Pallas kernels for 5% -> 5%
where the time goes in v5:
time: 181 us
  blocking collectives  84.9 us (47%)
  Pallas kernels  37.9 us (21%)
  starting transfers between devices  26.7 us (15%)
  waiting for transfers between devices  17.6 us (10%)
  between operations  13.5 us (7%)
    all_gather x1, blocking collectives, body(): early = lax.all_gather(early, 'sp').reshape(-1, early.shape[1])  37.1 us
    all_gather x1, blocking collectives, body(): runs = lax.all_gather(run, 'sp')  23.2 us
    ppermute x1, starting transfers between devices, body(): other = lax.ppermute(same, 'tp', [(i, i ^ 1) for i in range(peers)])  17.2 us
    pallas_call x1, Pallas kernels, late_partials(): pl.pallas_call(late_kernel, in_specs=[vmem, pl.BlockSpec(memory_space=plt...  17 us
    all_to_all x1, blocking collectives, body(): parts = lax.all_to_all(parts, 'fs', 0, 0)  13.8 us
    all_gather x1, waiting for transfers between devices, body(): late = lax.all_gather(late, 'sp', axis=0, tiled=True)  12.5 us
    all_to_all x1, blocking collectives, body(): same = lax.all_to_all(mine, 'tp', 0, 0, axis_index_groups=groups)  10.8 us
    all_to_all x1, starting transfers between devices, body(): x = lax.all_to_all(x, 'fs', 0, 0)  5.14 us
  transfers between devices with their start and end apart: 5, of which 2 were waited for; matrix products, arithmetic and copies ran while one was open for 0% of the time, Pallas kernels for 5%

profile of v5, /device:TPU:1, one launch (start us, length us, event | category | flops | bytes accessed | tf_op | source)
XLA Modules:
  0.0 180.7 jit_solution(10478834051965803135)
XLA Ops:
  6.5 5.1 %pack.1 = (bf16[64,448]{1,0:T(8,128)(2,1)}, bf16[64,512]{1,0:T(8,128)(2,1)}) custom-call(s32[1]{0:T(128)} %bitcast.3.own, bf16[64,128]{1,0:T(8,128)(2,1)} %key.1, bf16[64,128]{1,0:T(8,128)(2,1)} %value.1, bf16[64,128]{1,0:T(8,128)(2,1)} %pool.1, bf16[64,64]{1,0:T(8,128)(2,1)} %low.1, bf16[64,128]{1,0:T(8,128)(2,1)} %query.1, bf16[64,128]{1,0:T(8,128)(2,1)} %gate.1, ...), custom_call_target="tpu_custom_call" | custom-call | tf_op jit(solution)/shard_map/pack/pallas_call | solution.py:65
  11.7 4.4 %prep.1 = (bf16[4,256,1024]{2,1,0:T(8,128)(2,1)}, f32[256,128]{1,0:T(8,128)}) custom-call(bf16[256,4096]{1,0:T(8,128)(2,1)} %bitcast.22, f32[1,4096]{1,0:T(1,128)} %bitcast.25), custom_call_target="tpu_custom_call" | custom-call | tf_op jit(solution)/shard_map/prep/pallas_call | solution.py:106
  16.1 5.1 %all-to-all-start = ((bf16[4,256,1024]{2,1,0:T(8,128)(2,1)}), bf16[4,256,1024]{2,1,0:T(8,128)(2,1)S(1)}, u32[]{:S(2)}, u32[]{:S(2)}) async-start(bf16[4,256,1024]{2,1,0:T(8,128)(2,1)} %get-tuple-element.33), calls=%async_computation | async-start | bytes 4194304 | tf_op jit(solution)/shard_map/all_to_all | solution.py:456
  21.2 0.7 all-gather.6.cloned.1.call-update
  21.9 0.0 all-gather.8.cloned.1.call-start
  22.0 37.1 %all-gather.w = bf16[1024,448]{1,0:T(8,128)(2,1)S(1)} all-gather(bf16[64,448]{1,0:T(8,128)(2,1)S(1)} %copy-done.4), channel_id=2, replica_groups=mesh['sp'=16,'fs'=4,'tp'=8] {'sp'}, dimensions={0}, use_global_device_ids=true | all-gather | bytes 974848 | tf_op jit(solution)/shard_map/all_gather | solution.py:457
  59.1 0.0 all-to-all-done.x
  59.1 3.2 %early_parts.1 = (bf16[4,896,128]{2,1,0:T(8,128)(2,1)S(1)}, bf16[4,256,1024]{2,1,0:T(8,128)(2,1)S(1)}) custom-call(bf16[4,256,1024]{2,1,0:T(8,128)(2,1)S(1)} %all-to-all-done.x, bf16[1024,448]{1,0:T(8,128)(2,1)S(1)} %all-gather.w), custom_call_target="tpu_custom_call", output_to_operand_aliasing={{1}: (0, {})} | custom-call | tf_op jit(solution)/shard_map/early_parts/pallas_call | solution.py:167
  62.4 13.8 %all_to_all.20.parts = bf16[4,896,128]{2,1,0:T(8,128)(2,1)S(1)} all-to-all(bf16[4,896,128]{2,1,0:T(8,128)(2,1)S(1)} %get-tuple-element.37), channel_id=1, replica_groups=mesh['sp'=16,'fs'=4,'tp'=8] {'fs'}, dimensions={0} | all-to-all | bytes 1835008 | tf_op jit(solution)/shard_map/all_to_all | solution.py:460
  76.2 1.4 shard_map.163
  77.6 12.5 %all-gather.6.cloned.1.call-done.w = bf16[1024,512]{1,0:T(8,128)(2,1)} async-done(((bf16[64,512]{1,0:T(8,128)(2,1)}), bf16[1024,512]{1,0:T(8,128)(2,1)}) %all-gather.6.cloned.1.call-update) | async-done | bytes 1048592 | tf_op jit(solution)/shard_map/all_gather | solution.py:454
  90.1 17.0 %late_parts.1 = (bf16[4,512,128]{2,1,0:T(8,128)(2,1)}, bf16[1024,256]{1,0:T(8,128)(2,1)}) custom-call(bf16[4,256,1024]{2,1,0:T(8,128)(2,1)S(1)} %get-tuple-element.35.x, bf16[1024,512]{1,0:T(8,128)(2,1)} %all-gather.6.cloned.1.call-done.w), custom_call_target="tpu_custom_call" | custom-call | tf_op jit(solution)/shard_map/late_parts/pallas_call | solution.py:184
  107.2 0.0 all-gather.8.cloned.1.call-update
  107.2 4.3 %all-to-all-start.2 = ((bf16[4,512,128]{2,1,0:T(8,128)(2,1)}), bf16[4,512,128]{2,1,0:T(8,128)(2,1)S(1)}, u32[]{:S(2)}, u32[]{:S(2)}) async-start(bf16[4,512,128]{2,1,0:T(8,128)(2,1)} %get-tuple-element.45), calls=%async_computation.2 | async-start | bytes 1048576 | tf_op jit(solution)/shard_map/all_to_all | solution.py:486
  111.5 0.1 copy.20.start
  111.6 23.2 %all-gather.1 = bf16[1536,128]{1,0:T(8,128)(2,1)S(1)} all-gather(bf16[96,128]{1,0:T(8,128)(2,1)S(1)} %get-tuple-element.44), channel_id=3, replica_groups=mesh['sp'=16,'fs'=4,'tp'=8] {'sp'}, dimensions={0}, use_global_device_ids=true | all-gather | bytes 417792 | tf_op jit(solution)/shard_map/all_gather | solution.py:487
  134.7 0.0 all-to-all-done.2.parts
  134.7 2.8 %shard_map.164 = bf16[4,256,256]{2,1,0:T(8,128)(2,1)} custom-call(s32[1]{0:T(128)} %bitcast.1.sp, s32[1]{0:T(128)} %bitcast.2.tp, bf16[16,96,128]{2,1,0:T(8,128)(2,1)S(1)} %bitcast.18, f32[64,128]{1,0:T(8,128)S(1)} %copy.20.start, bf16[4,512,128]{2,1,0:T(8,128)(2,1)S(1)} %all-to-all-done.2.parts, f32[256,128]{1,0:T(8,128)S(1)} %copy-done, ...), custom_call_target="tpu_custom_call" | custom-call | tf_op jit(solution)/shard_map/pallas_call | solution.py:25
  137.6 10.8 %all_to_all.21.z = bf16[4,256,256]{2,1,0:T(8,128)(2,1)S(1)} all-to-all(bf16[4,256,256]{2,1,0:T(8,128)(2,1)} %shard_map.164), channel_id=1, replica_groups={{0,2,4,6},{1,3,5,7},{8,10,12,14},{9,11,13,15},{16,18,20,22},{17,19,21,2..., dimensions={0} | all-to-all | bytes 1048576 | tf_op jit(solution)/shard_map/all_to_all | solution.py:511
  148.4 4.3 %all-gather.8.cloned.1.call-done = bf16[4096,256]{1,0:T(8,128)(2,1)} async-done(((bf16[1024,256]{1,0:T(8,128)(2,1)}), bf16[4096,256]{1,0:T(8,128)(2,1)}) %all-gather.8.cloned.1.call-update) | async-done | bytes 2097168 | tf_op jit(solution)/shard_map/all_gather | solution.py:485
  152.7 17.2 %collective-permute-start = (bf16[4,256,256]{2,1,0:T(8,128)(2,1)S(1)}, bf16[4,256,256]{2,1,0:T(8,128)(2,1)S(1)}, u32[]{:S(2)}, u32[]{:S(2)}) collective-permute-start(bf16[4,256,256]{2,1,0:T(8,128)(2,1)S(1)} %all_to_all.21.z), channel_id=1, source_target_pairs={{0,1},{1,0},{2,3},{3,2},{4,5},{5,4},{6,7},{7,6},{8,9},{9,8},{10,11... | collective-permute-start | bytes 1572872 | tf_op jit(solution)/shard_map/ppermute | solution.py:513
  169.9 1.6 shard_map.165.rest_0_
  171.5 0.0 collective-permute-done.z
  171.5 2.3 %shard_map.166 = bf16[256,512]{1,0:T(8,128)(2,1)} custom-call(s32[1]{0:T(128)S(6)} %sub.3.core, bf16[4,256,256]{2,1,0:T(8,128)(2,1)S(1)} %collective-permute-done.z, bf16[4,1024,256]{2,1,0:T(8,128)(2,1)} %bitcast.21, f32[256,512]{1,0:T(8,128)S(1)} %shard_map.165.rest_0_), custom_call_target="tpu_custom_call" | custom-call | tf_op jit(solution)/shard_map/pallas_call | solution.py:398
  (13 shorter events, 0.0 us)
Async XLA Ops:
  16.1 5.9 %copy-start.4 = (bf16[64,448]{1,0:T(8,128)(2,1)S(1)}, bf16[64,448]{1,0:T(8,128)(2,1)}, u32[]{:S(2)}) copy-start(bf16[64,448]{1,0:T(8,128)(2,1)} %get-tuple-element.34) | copy-start | bytes 172036
  16.1 43.1 %all-to-all-start = ((bf16[4,256,1024]{2,1,0:T(8,128)(2,1)}), bf16[4,256,1024]{2,1,0:T(8,128)(2,1)S(1)}, u32[]{:S(2)}, u32[]{:S(2)}) async-start(bf16[4,256,1024]{2,1,0:T(8,128)(2,1)} %get-tuple-element.33), calls=%async_computation | async-start | bytes 4194304 | tf_op jit(solution)/shard_map/all_to_all | solution.py:456
  21.2 68.9 %all-gather.6.cloned.1.call-start = ((), (), s32[]{:S(2)}) async-start(), calls=%async_computation.4 | async-start | bytes 1114112 | tf_op jit(solution)/shard_map/all_gather | solution.py:454
  21.9 130.8 %all-gather.8.cloned.1.call-start = ((), (), s32[]{:S(2)}) async-start(), calls=%async_computation.5 | async-start | bytes 2621440 | tf_op jit(solution)/shard_map/all_gather | solution.py:485
  59.1 17.0 %copy-start = (f32[256,128]{1,0:T(8,128)S(1)}, f32[256,128]{1,0:T(8,128)}, u32[]{:S(2)}) copy-start(f32[256,128]{1,0:T(8,128)} %get-tuple-element.38.inverse) | copy-start | bytes 393220
  59.1 17.0 %copy-start.1 = (bf16[64,128]{1,0:T(8,128)(2,1)S(1)}, bf16[64,128]{1,0:T(8,128)(2,1)}, u32[]{:S(2)}) copy-start(bf16[64,128]{1,0:T(8,128)(2,1)} %second.1) | copy-start | bytes 49156
  59.1 17.0 %copy-start.2 = (f32[2,256]{1,0:T(2,128)S(1)}, f32[2,256]{1,0:T(2,128)}, u32[]{:S(2)}) copy-start(f32[2,256]{1,0:T(2,128)} %extra.1) | copy-start | bytes 6148
  59.1 17.0 %copy-start.3 = (f32[128]{0:T(128)S(1)}, f32[128]{0:T(128)}, u32[]{:S(2)}) copy-start(f32[128]{0:T(128)} %param.26) | copy-start | bytes 1540
  90.1 21.4 %copy-start.5 = (f32[1,2,64,64]{3,2,1,0:T(8,128)S(1)}, f32[1,2,64,64]{3,2,1,0:T(8,128)}, u32[]{:S(2)}) copy-start(f32[1,2,64,64]{3,2,1,0:T(8,128)} %param.29) | copy-start | bytes 98308
  107.2 27.5 %all-to-all-start.2 = ((bf16[4,512,128]{2,1,0:T(8,128)(2,1)}), bf16[4,512,128]{2,1,0:T(8,128)(2,1)S(1)}, u32[]{:S(2)}, u32[]{:S(2)}) async-start(bf16[4,512,128]{2,1,0:T(8,128)(2,1)} %get-tuple-element.45), calls=%async_computation.2 | async-start | bytes 1048576 | tf_op jit(solution)/shard_map/all_to_all | solution.py:486
  152.7 18.8 %collective-permute-start = (bf16[4,256,256]{2,1,0:T(8,128)(2,1)S(1)}, bf16[4,256,256]{2,1,0:T(8,128)(2,1)S(1)}, u32[]{:S(2)}, u32[]{:S(2)}) collective-permute-start(bf16[4,256,256]{2,1,0:T(8,128)(2,1)S(1)} %all_to_all.21.z), channel_id=1, source_target_pairs={{0,1},{1,0},{2,3},{3,2},{4,5},{5,4},{6,7},{7,6},{8,9},{9,8},{10,11... | collective-permute-start | bytes 1572872 | tf_op jit(solution)/shard_map/ppermute | solution.py:513
Sparse Core Ops, SparseCore 0:
  24.1 65.9 all-gather.5
  107.3 45.3 all-gather.7

commit v6 on v5

--- a/solution.py
+++ b/solution.py
@@ -40,36 +40,15 @@
     return jax.ShapeDtypeStruct(shape, dtype)
 
 
-def pack_kernel(
-    own, key, value, pool, low, query, gate, pool_rows, state_rows, early, late, moved
-):
+def pack_kernel(own, key, value, pool, low, query, gate, pool_rows, state_rows, early, late):
+    at = 0
+    for r in (key, value, pool, low):
+        early[:, at : at + r.shape[1]] = r[...]
+        at += r.shape[1]
     mine = pl.ds(pl.multiple_of(own[0] * LANES, LANES), LANES)
-    moves = []
-    for out, blocks in (
-        (late, (query, gate, pool_rows.at[:, mine], state_rows.at[:, mine])),
-        (early, (key, value, pool, low)),
-    ):
-        at = 0
-        for block in blocks:
-            width = block.shape[1]
-            to = out.at[:, at : at + width]
-            moves.append(pltpu.make_async_copy(block, to, moved.at[len(moves)]))
-            moves[-1].start()
-            at += width
-    for move in moves:
-        move.wait()
-
-
-def pack(own, blocks, outs):
-    anywhere = pl.BlockSpec(memory_space=pl.ANY)
-    return pl.pallas_call(
-        pack_kernel,
-        in_specs=[pl.BlockSpec(memory_space=pltpu.SMEM)] + [anywhere] * len(blocks),
-        out_specs=[anywhere] * len(outs),
-        out_shape=outs,
-        scratch_shapes=[pltpu.SemaphoreType.DMA((len(blocks),))],
-        name="pack",
-    )(own, *blocks)
+    blocks = (query[...], gate[...], pool_rows[:, mine], state_rows[:, mine])
+    for j, block in enumerate(blocks):
+        late[:, j * LANES : (j + 1) * LANES] = block
 
 
 def prep_kernel(act, gain, x, inverse, held, arrived):
@@ -142,12 +121,12 @@
 def late_kernel(x, w, out, quarter, held, made, arrived, left):
     tokens = x.shape[1]
     columns = 2 * LANES
-    into = pltpu.make_async_copy(w.at[:, :columns], held, arrived)
+    into = pltpu.make_async_copy(w, held, arrived)
     into.start()
-    across = pltpu.make_async_copy(w.at[:, columns:], quarter, left.at[4])
+    into.wait()
+    across = pltpu.make_async_copy(held.at[:, columns:], quarter, left.at[4])
     across.start()
-    into.wait()
-    weight = held[...]
+    weight = held[:, :columns]
     copies = [across]
     for f in range(4):
         p = jnp.dot(x[f], weight, preferred_element_type=f32)
@@ -187,7 +166,7 @@
         out_specs=[anywhere, anywhere],
         out_shape=[struct(shape, bf16), struct((depth, w.shape[1] - 2 * LANES), bf16)],
         scratch_shapes=[
-            pltpu.VMEM((depth, 2 * LANES), bf16),
+            pltpu.VMEM(w.shape, bf16),
             pltpu.VMEM(shape, bf16),
             pltpu.SemaphoreType.DMA,
             pltpu.SemaphoreType.DMA((5,)),
@@ -436,19 +415,19 @@
     columns = pooling_output_rows.shape[1]
     own = lax.axis_index("fs").astype(jnp.int32).reshape(1)
     tp = lax.axis_index("tp").astype(jnp.int32)
-    early, late = pack(
+    early, late = call(
+        pack_kernel,
+        [struct((rows, 3 * LANES + HEAD), bf16), struct((rows, 4 * LANES), bf16)],
+        "pack",
         own,
-        (
-            key_projection_weight,
-            value_projection_weight,
-            pooling_channel_weight,
-            decay_first_factor,
-            query_projection_weight,
-            output_gate_weight,
-            pooling_output_rows,
-            attention_output_rows,
-        ),
-        [struct((rows, 3 * LANES + HEAD), bf16), struct((rows, 4 * LANES), bf16)],
+        key_projection_weight,
+        value_projection_weight,
+        pooling_channel_weight,
+        decay_first_factor,
+        query_projection_weight,
+        output_gate_weight,
+        pooling_output_rows,
+        attention_output_rows,
     )
     late, early, activations = lax.optimization_barrier((late, early, activations))
     late = lax.all_gather(late, "sp", axis=0, tiled=True)

time: 181 us -> 163 us (0.901)
  Pallas kernels: 37.9 us -> 20.1 us
    pallas_call x1, Pallas kernels: 17 us -> 2.71 us  [late_partials(): pl.pallas_call(late_kernel, in_specs=[vmem, pl.BlockSpec(memory_space=plt...]
    pallas_call x1 -> x0, Pallas kernels: 5.14 us -> none  [pack(): pl.pallas_call(pack_kernel, in_specs=[pl.BlockSpec(memory_space=pltpu.SME...]
    pallas_call x2 -> x3, Pallas kernels: 4.23 us -> 5.88 us  [call(): pl.pallas_call(kernel, in_specs=[smem] * scalars + [vmem] * (len(args) -...]
  transfers between devices with their start and end apart: 5 -> 5, of which waited for: 2 -> 2; matrix products, arithmetic and copies ran while one was open for 0% -> 0% of each run, Pallas kernels for 5% -> 6%
where the time goes in v6:
time: 163 us
  blocking collectives  84.9 us (52%)
  starting transfers between devices  26.7 us (16%)
  Pallas kernels  20.1 us (12%)
  waiting for transfers between devices  17.6 us (11%)
  between operations  13.5 us (8%)
    all_gather x1, blocking collectives, body(): early = lax.all_gather(early, 'sp').reshape(-1, early.shape[1])  37.1 us
    all_gather x1, blocking collectives, body(): runs = lax.all_gather(run, 'sp')  23.2 us
    ppermute x1, starting transfers between devices, body(): other = lax.ppermute(same, 'tp', [(i, i ^ 1) for i in range(peers)])  17.2 us
    all_to_all x1, blocking collectives, body(): parts = lax.all_to_all(parts, 'fs', 0, 0)  13.8 us
    all_gather x1, waiting for transfers between devices, body(): late = lax.all_gather(late, 'sp', axis=0, tiled=True)  12.5 us
    all_to_all x1, blocking collectives, body(): same = lax.all_to_all(mine, 'tp', 0, 0, axis_index_groups=groups)  10.8 us
    pallas_call x3, Pallas kernels, call(): pl.pallas_call(kernel, in_specs=[smem] * scalars + [vmem] * (len(args) -...  5.88 us
    all_to_all x1, starting transfers between devices, body(): x = lax.all_to_all(x, 'fs', 0, 0)  5.14 us
  transfers between devices with their start and end apart: 5, of which 2 were waited for; matrix products, arithmetic and copies ran while one was open for 0% of the time, Pallas kernels for 6%

profile of v6, /device:TPU:1, one launch (start us, length us, event | category | flops | bytes accessed | tf_op | source)
XLA Modules:
  0.0 162.8 jit_solution(6334823904490773826)
XLA Ops:
  6.5 1.6 %shard_map.163 = (bf16[64,448]{1,0:T(8,128)(2,1)}, bf16[64,512]{1,0:T(8,128)(2,1)}) custom-call(s32[1]{0:T(128)} %bitcast.3.own, bf16[64,128]{1,0:T(8,128)(2,1)} %key.1, bf16[64,128]{1,0:T(8,128)(2,1)} %value.1, bf16[64,128]{1,0:T(8,128)(2,1)} %pool.1, bf16[64,64]{1,0:T(8,128)(2,1)} %low.1, bf16[64,128]{1,0:T(8,128)(2,1)} %query.1, bf16[64,128]{1,0:T(8,128)(2,1)} %gate.1, ...), custom_call_target="tpu_custom_call" | custom-call | tf_op jit(solution)/shard_map/pallas_call | solution.py:25
  8.2 4.4 %prep.1 = (bf16[4,256,1024]{2,1,0:T(8,128)(2,1)}, f32[256,128]{1,0:T(8,128)}) custom-call(bf16[256,4096]{1,0:T(8,128)(2,1)} %bitcast.22, f32[1,4096]{1,0:T(1,128)} %bitcast.25), custom_call_target="tpu_custom_call" | custom-call | tf_op jit(solution)/shard_map/prep/pallas_call | solution.py:85
  12.6 5.1 %all-to-all-start = ((bf16[4,256,1024]{2,1,0:T(8,128)(2,1)}), bf16[4,256,1024]{2,1,0:T(8,128)(2,1)S(1)}, u32[]{:S(2)}, u32[]{:S(2)}) async-start(bf16[4,256,1024]{2,1,0:T(8,128)(2,1)} %get-tuple-element.33), calls=%async_computation | async-start | bytes 4194304 | tf_op jit(solution)/shard_map/all_to_all | solution.py:435
  17.7 0.7 all-gather.6.cloned.1.call-update
  18.4 0.0 all-gather.8.cloned.1.call-start
  18.5 37.1 %all-gather.w = bf16[1024,448]{1,0:T(8,128)(2,1)S(1)} all-gather(bf16[64,448]{1,0:T(8,128)(2,1)S(1)} %copy-done.4), channel_id=2, replica_groups=mesh['sp'=16,'fs'=4,'tp'=8] {'sp'}, dimensions={0}, use_global_device_ids=true | all-gather | bytes 974848 | tf_op jit(solution)/shard_map/all_gather | solution.py:436
  55.6 0.0 all-to-all-done.x
  55.6 3.2 %early_parts.1 = (bf16[4,896,128]{2,1,0:T(8,128)(2,1)S(1)}, bf16[4,256,1024]{2,1,0:T(8,128)(2,1)S(1)}) custom-call(bf16[4,256,1024]{2,1,0:T(8,128)(2,1)S(1)} %all-to-all-done.x, bf16[1024,448]{1,0:T(8,128)(2,1)S(1)} %all-gather.w), custom_call_target="tpu_custom_call", output_to_operand_aliasing={{1}: (0, {})} | custom-call | tf_op jit(solution)/shard_map/early_parts/pallas_call | solution.py:146
  58.9 13.8 %all_to_all.20.parts = bf16[4,896,128]{2,1,0:T(8,128)(2,1)S(1)} all-to-all(bf16[4,896,128]{2,1,0:T(8,128)(2,1)S(1)} %get-tuple-element.37), channel_id=1, replica_groups=mesh['sp'=16,'fs'=4,'tp'=8] {'fs'}, dimensions={0} | all-to-all | bytes 1835008 | tf_op jit(solution)/shard_map/all_to_all | solution.py:439
  72.7 1.4 shard_map.164
  74.1 12.5 %all-gather.6.cloned.1.call-done.w = bf16[1024,512]{1,0:T(8,128)(2,1)} async-done(((bf16[64,512]{1,0:T(8,128)(2,1)}), bf16[1024,512]{1,0:T(8,128)(2,1)}) %all-gather.6.cloned.1.call-update) | async-done | bytes 1048592 | tf_op jit(solution)/shard_map/all_gather | solution.py:433
  86.6 2.7 %late_parts.1 = (bf16[4,512,128]{2,1,0:T(8,128)(2,1)}, bf16[1024,256]{1,0:T(8,128)(2,1)}) custom-call(bf16[4,256,1024]{2,1,0:T(8,128)(2,1)S(1)} %get-tuple-element.35.x, bf16[1024,512]{1,0:T(8,128)(2,1)} %all-gather.6.cloned.1.call-done.w), custom_call_target="tpu_custom_call" | custom-call | tf_op jit(solution)/shard_map/late_parts/pallas_call | solution.py:163
  89.3 0.0 all-gather.8.cloned.1.call-update
  89.4 4.3 %all-to-all-start.2 = ((bf16[4,512,128]{2,1,0:T(8,128)(2,1)}), bf16[4,512,128]{2,1,0:T(8,128)(2,1)S(1)}, u32[]{:S(2)}, u32[]{:S(2)}) async-start(bf16[4,512,128]{2,1,0:T(8,128)(2,1)} %get-tuple-element.45), calls=%async_computation.2 | async-start | bytes 1048576 | tf_op jit(solution)/shard_map/all_to_all | solution.py:465
  93.7 0.1 copy.20.start
  93.7 23.2 %all-gather.1 = bf16[1536,128]{1,0:T(8,128)(2,1)S(1)} all-gather(bf16[96,128]{1,0:T(8,128)(2,1)S(1)} %get-tuple-element.44), channel_id=3, replica_groups=mesh['sp'=16,'fs'=4,'tp'=8] {'sp'}, dimensions={0}, use_global_device_ids=true | all-gather | bytes 417792 | tf_op jit(solution)/shard_map/all_gather | solution.py:466
  116.9 0.0 all-to-all-done.2.parts
  116.9 2.8 %shard_map.165 = bf16[4,256,256]{2,1,0:T(8,128)(2,1)} custom-call(s32[1]{0:T(128)} %bitcast.1.sp, s32[1]{0:T(128)} %bitcast.2.tp, bf16[16,96,128]{2,1,0:T(8,128)(2,1)S(1)} %bitcast.18, f32[64,128]{1,0:T(8,128)S(1)} %copy.20.start, bf16[4,512,128]{2,1,0:T(8,128)(2,1)S(1)} %all-to-all-done.2.parts, f32[256,128]{1,0:T(8,128)S(1)} %copy-done, ...), custom_call_target="tpu_custom_call" | custom-call | tf_op jit(solution)/shard_map/pallas_call | solution.py:25
  119.7 10.8 %all_to_all.21.z = bf16[4,256,256]{2,1,0:T(8,128)(2,1)S(1)} all-to-all(bf16[4,256,256]{2,1,0:T(8,128)(2,1)} %shard_map.165), channel_id=1, replica_groups={{0,2,4,6},{1,3,5,7},{8,10,12,14},{9,11,13,15},{16,18,20,22},{17,19,21,2..., dimensions={0} | all-to-all | bytes 1048576 | tf_op jit(solution)/shard_map/all_to_all | solution.py:490
  130.6 4.3 %all-gather.8.cloned.1.call-done = bf16[4096,256]{1,0:T(8,128)(2,1)} async-done(((bf16[1024,256]{1,0:T(8,128)(2,1)}), bf16[4096,256]{1,0:T(8,128)(2,1)}) %all-gather.8.cloned.1.call-update) | async-done | bytes 2097168 | tf_op jit(solution)/shard_map/all_gather | solution.py:464
  134.9 17.2 %collective-permute-start = (bf16[4,256,256]{2,1,0:T(8,128)(2,1)S(1)}, bf16[4,256,256]{2,1,0:T(8,128)(2,1)S(1)}, u32[]{:S(2)}, u32[]{:S(2)}) collective-permute-start(bf16[4,256,256]{2,1,0:T(8,128)(2,1)S(1)} %all_to_all.21.z), channel_id=1, source_target_pairs={{0,1},{1,0},{2,3},{3,2},{4,5},{5,4},{6,7},{7,6},{8,9},{9,8},{10,11... | collective-permute-start | bytes 1572872 | tf_op jit(solution)/shard_map/ppermute | solution.py:492
  152.1 1.6 shard_map.166.rest_0_
  153.7 0.0 collective-permute-done.z
  153.7 2.3 %shard_map.167 = bf16[256,512]{1,0:T(8,128)(2,1)} custom-call(s32[1]{0:T(128)S(6)} %sub.3.core, bf16[4,256,256]{2,1,0:T(8,128)(2,1)S(1)} %collective-permute-done.z, bf16[4,1024,256]{2,1,0:T(8,128)(2,1)} %bitcast.21, f32[256,512]{1,0:T(8,128)S(1)} %shard_map.166.rest_0_), custom_call_target="tpu_custom_call" | custom-call | tf_op jit(solution)/shard_map/pallas_call | solution.py:377
  (13 shorter events, 0.0 us)
Async XLA Ops:
  12.6 5.9 %copy-start.4 = (bf16[64,448]{1,0:T(8,128)(2,1)S(1)}, bf16[64,448]{1,0:T(8,128)(2,1)}, u32[]{:S(2)}) copy-start(bf16[64,448]{1,0:T(8,128)(2,1)} %get-tuple-element.34) | copy-start | bytes 172036
  12.6 43.1 %all-to-all-start = ((bf16[4,256,1024]{2,1,0:T(8,128)(2,1)}), bf16[4,256,1024]{2,1,0:T(8,128)(2,1)S(1)}, u32[]{:S(2)}, u32[]{:S(2)}) async-start(bf16[4,256,1024]{2,1,0:T(8,128)(2,1)} %get-tuple-element.33), calls=%async_computation | async-start | bytes 4194304 | tf_op jit(solution)/shard_map/all_to_all | solution.py:435
  17.7 68.9 %all-gather.6.cloned.1.call-start = ((), (), s32[]{:S(2)}) async-start(), calls=%async_computation.4 | async-start | bytes 1114112 | tf_op jit(solution)/shard_map/all_gather | solution.py:433
  18.4 116.4 %all-gather.8.cloned.1.call-start = ((), (), s32[]{:S(2)}) async-start(), calls=%async_computation.5 | async-start | bytes 2621440 | tf_op jit(solution)/shard_map/all_gather | solution.py:464
  55.6 17.0 %copy-start = (f32[256,128]{1,0:T(8,128)S(1)}, f32[256,128]{1,0:T(8,128)}, u32[]{:S(2)}) copy-start(f32[256,128]{1,0:T(8,128)} %get-tuple-element.38.inverse) | copy-start | bytes 393220
  55.6 17.0 %copy-start.1 = (bf16[64,128]{1,0:T(8,128)(2,1)S(1)}, bf16[64,128]{1,0:T(8,128)(2,1)}, u32[]{:S(2)}) copy-start(bf16[64,128]{1,0:T(8,128)(2,1)} %second.1) | copy-start | bytes 49156
  55.6 17.0 %copy-start.2 = (f32[2,256]{1,0:T(2,128)S(1)}, f32[2,256]{1,0:T(2,128)}, u32[]{:S(2)}) copy-start(f32[2,256]{1,0:T(2,128)} %extra.1) | copy-start | bytes 6148
  55.6 17.0 %copy-start.3 = (f32[128]{0:T(128)S(1)}, f32[128]{0:T(128)}, u32[]{:S(2)}) copy-start(f32[128]{0:T(128)} %param.26) | copy-start | bytes 1540
  86.6 7.1 %copy-start.5 = (f32[1,2,64,64]{3,2,1,0:T(8,128)S(1)}, f32[1,2,64,64]{3,2,1,0:T(8,128)}, u32[]{:S(2)}) copy-start(f32[1,2,64,64]{3,2,1,0:T(8,128)} %param.29) | copy-start | bytes 98308
  89.4 27.5 %all-to-all-start.2 = ((bf16[4,512,128]{2,1,0:T(8,128)(2,1)}), bf16[4,512,128]{2,1,0:T(8,128)(2,1)S(1)}, u32[]{:S(2)}, u32[]{:S(2)}) async-start(bf16[4,512,128]{2,1,0:T(8,128)(2,1)} %get-tuple-element.45), calls=%async_computation.2 | async-start | bytes 1048576 | tf_op jit(solution)/shard_map/all_to_all | solution.py:465
  134.9 18.8 %collective-permute-start = (bf16[4,256,256]{2,1,0:T(8,128)(2,1)S(1)}, bf16[4,256,256]{2,1,0:T(8,128)(2,1)S(1)}, u32[]{:S(2)}, u32[]{:S(2)}) collective-permute-start(bf16[4,256,256]{2,1,0:T(8,128)(2,1)S(1)} %all_to_all.21.z), channel_id=1, source_target_pairs={{0,1},{1,0},{2,3},{3,2},{4,5},{5,4},{6,7},{7,6},{8,9},{9,8},{10,11... | collective-permute-start | bytes 1572872 | tf_op jit(solution)/shard_map/ppermute | solution.py:492
Sparse Core Ops, SparseCore 0:
  20.6 65.9 all-gather.5
  89.5 45.3 all-gather.7

commit v7 on v6

--- a/solution.py
+++ b/solution.py
@@ -28,7 +28,7 @@
         out_specs=[vmem] * len(outs),
         out_shape=outs,
         input_output_aliases=aliases,
-        compiler_params=limit if name == "local" else None,
+        compiler_params=limit if name in ("local", "finish") else None,
     )(*args)
 
 
@@ -200,7 +200,7 @@
 
 
 def local_kernel(
-    parts, inverse, second, bias, extra, keys, values, pool, sums, prior, opening, run
+    parts, inverse, second, bias, extra, keys, values, pool, sums, prior, opening, spread
 ):
     inv = inverse[...]
     tokens = inv.shape[0]
@@ -208,7 +208,6 @@
     values[...] = projected(parts, inv, 1).astype(f32)
     pooled = projected(parts, inv, 2)
     pool[...] = pooled
-    run[RUN_ROWS - HALO :] = pooled[tokens - HALO :]
     both = total_of(parts, 3 * tokens, tokens // 2)
     low = jnp.concatenate([both[:, :HEAD], both[:, HEAD:]], axis=0)
     low = (low * inv[:, :HEAD]).astype(bf16)
@@ -241,18 +240,51 @@
         opening[n : n + 1] = before
         state = jnp.exp(final) * state + heads_of(pairs, half)
         before = before + final
-    run[:HEAD] = state.astype(bf16)
+    for to in range(spread.shape[0]):
+        write_run(spread, to, state, before, pooled[tokens - HALO :])
+
+
+def write_run(out, to, state, log, tail):
     row = lax.broadcasted_iota(jnp.int32, (HALO, LANES), 0)
     logs = jnp.zeros((HALO, LANES), f32)
-    for j, part in enumerate(thirds(before)):
+    for j, part in enumerate(thirds(log)):
         logs = jnp.where(row == j, part.astype(f32), logs)
-    run[HEAD : HEAD + HALO] = logs.astype(bf16)
+    out[to, :HEAD] = state.astype(bf16)
+    out[to, HEAD : HEAD + HALO] = logs.astype(bf16)
+    out[to, HEAD + HALO :] = tail
+
+
+def read_run(came):
+    came = came.astype(f32)
+    log = came[HEAD : HEAD + 1] + came[HEAD + 1 : HEAD + 2] + came[HEAD + 2 : HEAD + 3]
+    return came[:HEAD], log
+
+
+def quad_kernel(sp, quad, total, within, log_within, previous):
+    place = sp[0] % 4
+    state = jnp.zeros((HEAD, LANES), f32)
+    log = jnp.zeros((1, LANES), f32)
+    for j in range(4):
+
+        @pl.when(place == j)
+        def _(state=state, log=log):
+            within[...] = state
+            log_within[...] = jnp.broadcast_to(log, log_within.shape)
+
+        s, decay = read_run(quad[j])
+        state = jnp.exp(decay) * state + s
+        log = log + decay
+    write_run(total, 0, state, log, quad[3, HEAD + HALO :])
+    previous[...] = quad[jnp.maximum(place - 1, 0), HEAD + HALO :]
 
 
 def finish_kernel(
     sp,
     tp,
     runs,
+    within_quad,
+    log_within,
+    previous,
     start,
     parts,
     inverse,
@@ -272,9 +304,9 @@
     place = sp[0]
     state = start[...]
     for j in range(runs.shape[0]):
-        came = runs[j].astype(f32)
-        log = came[HEAD : HEAD + 1] + came[HEAD + 1 : HEAD + 2] + came[HEAD + 2 : HEAD + 3]
-        state = jnp.where(j < place, jnp.exp(log) * state + came[:HEAD], state)
+        came, log = read_run(runs[j])
+        state = jnp.where(j < place // 4, jnp.exp(log) * state + came, state)
+    state = jnp.exp(log_within[:1]) * state + within_quad[...]
     queries = projected(parts, inv, 0).astype(f32) * HEAD ** (-0.5)
     outgate = projected(parts, inv, 1).astype(f32)
     half = lax.broadcasted_iota(jnp.int32, (HEAD, LANES), 1) < HEAD
@@ -320,9 +352,10 @@
             mine[to, at, LANES:] = done
 
     current = pool[...].astype(f32)
-    previous = runs[jnp.maximum(place - 1, 0), RUN_ROWS - HALO :].astype(f32)
-    previous = jnp.where(place > 0, previous, 0.0)
-    extended = jnp.concatenate([previous, current], axis=0)
+    outside = runs[jnp.maximum(place // 4 - 1, 0), HEAD + HALO :].astype(f32)
+    outside = jnp.where(place >= 4, outside, 0.0)
+    before = jnp.where(place % 4 > 0, previous[...].astype(f32), outside)
+    extended = jnp.concatenate([before, current], axis=0)
 
     def back(x, by):
         return x + pltpu.roll(x, by, 0)
@@ -438,7 +471,7 @@
     parts, x = early_partials(near(x), near(early))
     parts = lax.all_to_all(parts, "fs", 0, 0)
     wide = pltpu.VMEM((tokens, LANES), f32)
-    keys, values, pool, sums, prior, opening, run = call(
+    keys, values, pool, sums, prior, opening, spread = call(
         local_kernel,
         [
             wide,
@@ -447,7 +480,7 @@
             wide,
             wide,
             pltpu.VMEM((tokens // BLOCK, LANES), f32),
-            struct((RUN_ROWS, LANES), bf16),
+            struct((4, RUN_ROWS, LANES), bf16),
         ],
         "local",
         near(parts),
@@ -458,20 +491,39 @@
         scalars=0,
     )
     start = starting_state[0].transpose(2, 0, 1).reshape(HEAD, LANES)
-    late, run = lax.optimization_barrier((late, run))
+    quads = [[4 * a + b for b in range(4)] for a in range(lax.axis_size("sp") // 4)]
+    late, _ = lax.optimization_barrier((late, spread))
+    quad = lax.all_to_all(spread, "sp", 0, 0, axis_index_groups=quads)
     late, quarter = late_partials(near(x), late)
-    late, quarter, run = lax.optimization_barrier((late, quarter, run))
+    _, _, quad = lax.optimization_barrier((late, quarter, quad))
     out_rows = lax.all_gather(quarter, "fs")
     late = lax.all_to_all(late, "fs", 0, 0)
-    runs = lax.all_gather(run, "sp")
+    sp = lax.axis_index("sp").astype(jnp.int32).reshape(1)
+    total, within, log_within, previous = call(
+        quad_kernel,
+        [
+            struct((1, RUN_ROWS, LANES), bf16),
+            pltpu.VMEM((HEAD, LANES), f32),
+            pltpu.VMEM((8, LANES), f32),
+            pltpu.VMEM((HALO, LANES), bf16),
+        ],
+        "quad_total",
+        sp,
+        near(quad),
+    )
+    strided = [list(column) for column in zip(*quads)]
+    runs = lax.all_gather(total[0], "sp", axis_index_groups=strided)
     peers = lax.axis_size("tp")
     (mine,) = call(
         finish_kernel,
         [struct((peers // 2, tokens, 2 * LANES), bf16)],
         "finish",
-        lax.axis_index("sp").astype(jnp.int32).reshape(1),
+        sp,
         tp.reshape(1),
         near(runs),
+        near(within),
+        near(log_within),
+        near(previous),
         near(start),
         near(late),
         inverse,

time: 163 us -> 159 us (0.975)
  starting transfers between devices: 26.7 us -> 18.9 us
  waiting for transfers between devices: 17.6 us -> 22.2 us
    all_gather x1, blocking collectives: 23.2 us -> 14.7 us  [body(): runs = lax.all_gather(total[0], 'sp', axis_index_groups=strided)]
    all_to_all x0 -> x1, blocking collectives: none -> 7.74 us  [body(): quad = lax.all_to_all(spread, 'sp', 0, 0, axis_index_groups=quads)]
    ppermute x1, starting transfers between devices: 17.2 us -> 9.49 us  [body(): other = lax.ppermute(same, 'tp', [(i, i ^ 1) for i in range(peers)])]
    all_gather x1, waiting for transfers between devices: 4.31 us -> 8.81 us  [body(): out_rows = lax.all_gather(quarter, 'fs')]
    pallas_call x3 -> x4, Pallas kernels: 5.88 us -> 5.01 us  [call(): pl.pallas_call(kernel, in_specs=[smem] * scalars + [vmem] * (len(args) -...]
  transfers between devices with their start and end apart: 5 -> 5, of which waited for: 2 -> 2; matrix products, arithmetic and copies ran while one was open for 0% -> 0% of each run, Pallas kernels for 6% -> 5%
where the time goes in v7:
time: 159 us; the launch traced here: 158 us
  blocking collectives  84.3 us (53%)
  waiting for transfers between devices  22.2 us (14%)
  Pallas kernels  19.2 us (12%)
  starting transfers between devices  18.9 us (12%)
  between operations  13.6 us (9%)
    all_gather x1, blocking collectives, body(): early = lax.all_gather(early, 'sp').reshape(-1, early.shape[1])  37.1 us
    all_gather x1, blocking collectives, body(): runs = lax.all_gather(total[0], 'sp', axis_index_groups=strided)  14.7 us
    all_to_all x1, blocking collectives, body(): parts = lax.all_to_all(parts, 'fs', 0, 0)  13.8 us
    all_gather x1, waiting for transfers between devices, body(): late = lax.all_gather(late, 'sp', axis=0, tiled=True)  12.6 us
    all_to_all x1, blocking collectives, body(): same = lax.all_to_all(mine, 'tp', 0, 0, axis_index_groups=groups)  10.9 us
    ppermute x1, starting transfers between devices, body(): other = lax.ppermute(same, 'tp', [(i, i ^ 1) for i in range(peers)])  9.49 us
    all_gather x1, waiting for transfers between devices, body(): out_rows = lax.all_gather(quarter, 'fs')  8.81 us
    all_to_all x1, blocking collectives, body(): quad = lax.all_to_all(spread, 'sp', 0, 0, axis_index_groups=quads)  7.74 us
  transfers between devices with their start and end apart: 5, of which 2 were waited for; matrix products, arithmetic and copies ran while one was open for 0% of the time, Pallas kernels for 5%

profile of v7, /device:TPU:1, one launch (start us, length us, event | category | flops | bytes accessed | tf_op | source)
XLA Modules:
  0.0 158.2 jit_solution(10700084781784044423)
XLA Ops:
  6.5 1.7 %shard_map.163 = (bf16[64,448]{1,0:T(8,128)(2,1)}, bf16[64,512]{1,0:T(8,128)(2,1)}) custom-call(s32[1]{0:T(128)} %bitcast.3.own, bf16[64,128]{1,0:T(8,128)(2,1)} %key.1, bf16[64,128]{1,0:T(8,128)(2,1)} %value.1, bf16[64,128]{1,0:T(8,128)(2,1)} %pool.1, bf16[64,64]{1,0:T(8,128)(2,1)} %low.1, bf16[64,128]{1,0:T(8,128)(2,1)} %query.1, bf16[64,128]{1,0:T(8,128)(2,1)} %gate.1, ...), custom_call_target="tpu_custom_call" | custom-call | tf_op jit(solution)/shard_map/pallas_call | solution.py:25
  8.2 4.4 %prep.1 = (bf16[4,256,1024]{2,1,0:T(8,128)(2,1)}, f32[256,128]{1,0:T(8,128)}) custom-call(bf16[256,4096]{1,0:T(8,128)(2,1)} %bitcast.23, f32[1,4096]{1,0:T(1,128)} %bitcast.25), custom_call_target="tpu_custom_call" | custom-call | tf_op jit(solution)/shard_map/prep/pallas_call | solution.py:85
  12.6 5.1 %all-to-all-start = ((bf16[4,256,1024]{2,1,0:T(8,128)(2,1)}), bf16[4,256,1024]{2,1,0:T(8,128)(2,1)S(1)}, u32[]{:S(2)}, u32[]{:S(2)}) async-start(bf16[4,256,1024]{2,1,0:T(8,128)(2,1)} %get-tuple-element.34), calls=%async_computation | async-start | bytes 4194304 | tf_op jit(solution)/shard_map/all_to_all | solution.py:468
  17.7 0.7 all-gather.5.cloned.1.call-update
  18.5 0.0 all-gather.7.cloned.1.call-start
  18.5 37.1 %all-gather.w = bf16[1024,448]{1,0:T(8,128)(2,1)S(1)} all-gather(bf16[64,448]{1,0:T(8,128)(2,1)S(1)} %copy-done.7), channel_id=2, replica_groups=mesh['sp'=16,'fs'=4,'tp'=8] {'sp'}, dimensions={0}, use_global_device_ids=true | all-gather | bytes 974848 | tf_op jit(solution)/shard_map/all_gather | solution.py:469
  55.6 0.0 all-to-all-done.x
  55.7 3.2 %early_parts.1 = (bf16[4,896,128]{2,1,0:T(8,128)(2,1)S(1)}, bf16[4,256,1024]{2,1,0:T(8,128)(2,1)S(1)}) custom-call(bf16[4,256,1024]{2,1,0:T(8,128)(2,1)S(1)} %all-to-all-done.x, bf16[1024,448]{1,0:T(8,128)(2,1)S(1)} %all-gather.w), custom_call_target="tpu_custom_call", output_to_operand_aliasing={{1}: (0, {})} | custom-call | tf_op jit(solution)/shard_map/early_parts/pallas_call | solution.py:146
  58.9 13.8 %all_to_all.25.parts = bf16[4,896,128]{2,1,0:T(8,128)(2,1)S(1)} all-to-all(bf16[4,896,128]{2,1,0:T(8,128)(2,1)S(1)} %get-tuple-element.38), channel_id=1, replica_groups=mesh['sp'=16,'fs'=4,'tp'=8] {'fs'}, dimensions={0} | all-to-all | bytes 1835008 | tf_op jit(solution)/shard_map/all_to_all | solution.py:472
  72.7 1.4 shard_map.164
  74.1 12.6 %all-gather.5.cloned.1.call-done.w = bf16[1024,512]{1,0:T(8,128)(2,1)} async-done(((bf16[64,512]{1,0:T(8,128)(2,1)}), bf16[1024,512]{1,0:T(8,128)(2,1)}) %all-gather.5.cloned.1.call-update) | async-done | bytes 1048592 | tf_op jit(solution)/shard_map/all_gather | solution.py:466
  86.7 2.7 %late_parts.1 = (bf16[4,512,128]{2,1,0:T(8,128)(2,1)}, bf16[1024,256]{1,0:T(8,128)(2,1)}) custom-call(bf16[4,256,1024]{2,1,0:T(8,128)(2,1)S(1)} %get-tuple-element.36.x, bf16[1024,512]{1,0:T(8,128)(2,1)} %all-gather.5.cloned.1.call-done.w), custom_call_target="tpu_custom_call" | custom-call | tf_op jit(solution)/shard_map/late_parts/pallas_call | solution.py:163
  89.5 0.0 all-gather.7.cloned.1.call-update
  89.5 7.7 %all_to_all.26.quad = bf16[4,96,128]{2,1,0:T(8,128)(2,1)S(1)} all-to-all(bf16[4,96,128]{2,1,0:T(8,128)(2,1)S(1)} %get-tuple-element.40), channel_id=1, replica_groups={{0,32,64,96},{128,160,192,224},{256,288,320,352},{384,416,448,480},{1,3..., dimensions={0} | all-to-all | bytes 196608 | tf_op jit(solution)/shard_map/all_to_all | solution.py:496
  97.2 4.2 %all-to-all-start.3 = ((bf16[4,512,128]{2,1,0:T(8,128)(2,1)}), bf16[4,512,128]{2,1,0:T(8,128)(2,1)S(1)}, u32[]{:S(2)}, u32[]{:S(2)}) async-start(bf16[4,512,128]{2,1,0:T(8,128)(2,1)} %get-tuple-element.42), calls=%async_computation.3 | async-start | bytes 1048576 | tf_op jit(solution)/shard_map/all_to_all | solution.py:500
  101.4 0.1 copy.21.start
  101.5 0.7 shard_map.165
  102.2 14.7 %all_gather.21.runs = bf16[4,96,128]{2,1,0:T(8,128)(2,1)S(1)} all-gather(bf16[1,96,128]{2,1,0:T(8,128)(2,1)} %get-tuple-element.45), channel_id=1, replica_groups={{0,128,256,384},{32,160,288,416},{64,192,320,448},{96,224,352,480},{1,1..., dimensions={0}, use_global_device_ids=true | all-gather | bytes 122880 | tf_op jit(solution)/shard_map/all_gather | solution.py:515
  116.9 1.2 shard_map.166
  118.2 10.9 %all_to_all.27.z = bf16[4,256,256]{2,1,0:T(8,128)(2,1)S(1)} all-to-all(bf16[4,256,256]{2,1,0:T(8,128)(2,1)S(1)} %shard_map.166), channel_id=1, replica_groups={{0,2,4,6},{1,3,5,7},{8,10,12,14},{9,11,13,15},{16,18,20,22},{17,19,21,2..., dimensions={0} | all-to-all | bytes 1048576 | tf_op jit(solution)/shard_map/all_to_all | solution.py:542
  129.1 8.8 %all-gather.7.cloned.1.call-done = bf16[4096,256]{1,0:T(8,128)(2,1)} async-done(((bf16[1024,256]{1,0:T(8,128)(2,1)}), bf16[4096,256]{1,0:T(8,128)(2,1)}) %all-gather.7.cloned.1.call-update) | async-done | bytes 2097168 | tf_op jit(solution)/shard_map/all_gather | solution.py:499
  137.9 9.5 %collective-permute-start = (bf16[4,256,256]{2,1,0:T(8,128)(2,1)S(1)}, bf16[4,256,256]{2,1,0:T(8,128)(2,1)S(1)}, u32[]{:S(2)}, u32[]{:S(2)}) collective-permute-start(bf16[4,256,256]{2,1,0:T(8,128)(2,1)S(1)} %all_to_all.27.z), channel_id=1, source_target_pairs={{0,1},{1,0},{2,3},{3,2},{4,5},{5,4},{6,7},{7,6},{8,9},{9,8},{10,11... | collective-permute-start | bytes 1572872 | tf_op jit(solution)/shard_map/ppermute | solution.py:544
  147.4 1.6 %shard_map.167.rest_0_ = f32[256,512]{1,0:T(8,128)S(1)} custom-call(s32[1]{0:T(128)} %bitcast.core, bf16[4,256,256]{2,1,0:T(8,128)(2,1)S(1)} %all_to_all.27.z, bf16[4,1024,256]{2,1,0:T(8,128)(2,1)} %bitcast.21), custom_call_target="tpu_custom_call" | custom-call | tf_op jit(solution)/shard_map/pallas_call | solution.py:410
  149.0 2.3 %shard_map.168 = bf16[256,512]{1,0:T(8,128)(2,1)} custom-call(s32[1]{0:T(128)S(6)} %sub.3.core, bf16[4,256,256]{2,1,0:T(8,128)(2,1)S(1)} %collective-permute-done.z, bf16[4,1024,256]{2,1,0:T(8,128)(2,1)} %bitcast.22, f32[256,512]{1,0:T(8,128)S(1)} %shard_map.167.rest_0_), custom_call_target="tpu_custom_call" | custom-call | tf_op jit(solution)/shard_map/pallas_call | solution.py:410
  (21 shorter events, 0.0 us)
Async XLA Ops:
  12.6 5.9 %copy-start.7 = (bf16[64,448]{1,0:T(8,128)(2,1)S(1)}, bf16[64,448]{1,0:T(8,128)(2,1)}, u32[]{:S(2)}) copy-start(bf16[64,448]{1,0:T(8,128)(2,1)} %get-tuple-element.35) | copy-start | bytes 172036
  12.6 43.1 %all-to-all-start = ((bf16[4,256,1024]{2,1,0:T(8,128)(2,1)}), bf16[4,256,1024]{2,1,0:T(8,128)(2,1)S(1)}, u32[]{:S(2)}, u32[]{:S(2)}) async-start(bf16[4,256,1024]{2,1,0:T(8,128)(2,1)} %get-tuple-element.34), calls=%async_computation | async-start | bytes 4194304 | tf_op jit(solution)/shard_map/all_to_all | solution.py:468
  17.7 69.0 %all-gather.5.cloned.1.call-start = ((), (), s32[]{:S(2)}) async-start(), calls=%async_computation.5 | async-start | bytes 1114112 | tf_op jit(solution)/shard_map/all_gather | solution.py:466
  18.5 119.5 %all-gather.7.cloned.1.call-start = ((), (), s32[]{:S(2)}) async-start(), calls=%async_computation.6 | async-start | bytes 2621440 | tf_op jit(solution)/shard_map/all_gather | solution.py:499
  55.6 17.0 %copy-start = (f32[256,128]{1,0:T(8,128)S(1)}, f32[256,128]{1,0:T(8,128)}, u32[]{:S(2)}) copy-start(f32[256,128]{1,0:T(8,128)} %get-tuple-element.39.inverse) | copy-start | bytes 393220
  55.6 17.0 %copy-start.2 = (bf16[64,128]{1,0:T(8,128)(2,1)S(1)}, bf16[64,128]{1,0:T(8,128)(2,1)}, u32[]{:S(2)}) copy-start(bf16[64,128]{1,0:T(8,128)(2,1)} %second.1) | copy-start | bytes 49156
  55.6 17.0 %copy-start.3 = (f32[2,256]{1,0:T(2,128)S(1)}, f32[2,256]{1,0:T(2,128)}, u32[]{:S(2)}) copy-start(f32[2,256]{1,0:T(2,128)} %extra.1) | copy-start | bytes 6148
  55.6 17.0 %copy-start.4 = (f32[128]{0:T(128)S(1)}, f32[128]{0:T(128)}, u32[]{:S(2)}) copy-start(f32[128]{0:T(128)} %param.26) | copy-start | bytes 1540
  86.7 14.7 %copy-start.8 = (f32[1,2,64,64]{3,2,1,0:T(8,128)S(1)}, f32[1,2,64,64]{3,2,1,0:T(8,128)}, u32[]{:S(2)}) copy-start(f32[1,2,64,64]{3,2,1,0:T(8,128)} %param.29) | copy-start | bytes 98308
  86.7 30.2 %copy-start.1 = (bf16[1,128,128]{2,1,0:T(8,128)(2,1)S(1)}, bf16[1,128,128]{2,1,0:T(8,128)(2,1)}, u32[]{:S(2)}) copy-start(bf16[1,128,128]{2,1,0:T(8,128)(2,1)} %param.30) | copy-start | bytes 98308
  86.7 30.2 %copy-start.5 = (f32[128]{0:T(128)S(1)}, f32[128]{0:T(128)}, u32[]{:S(2)}) copy-start(f32[128]{0:T(128)} %param.28) | copy-start | bytes 1540
  86.7 30.2 %copy-start.6 = (f32[128]{0:T(128)S(1)}, f32[128]{0:T(128)}, u32[]{:S(2)}) copy-start(f32[128]{0:T(128)} %param.31) | copy-start | bytes 1540
  97.2 19.7 %all-to-all-start.3 = ((bf16[4,512,128]{2,1,0:T(8,128)(2,1)}), bf16[4,512,128]{2,1,0:T(8,128)(2,1)S(1)}, u32[]{:S(2)}, u32[]{:S(2)}) async-start(bf16[4,512,128]{2,1,0:T(8,128)(2,1)} %get-tuple-element.42), calls=%async_computation.3 | async-start | bytes 1048576 | tf_op jit(solution)/shard_map/all_to_all | solution.py:500
  137.9 11.1 %collective-permute-start = (bf16[4,256,256]{2,1,0:T(8,128)(2,1)S(1)}, bf16[4,256,256]{2,1,0:T(8,128)(2,1)S(1)}, u32[]{:S(2)}, u32[]{:S(2)}) collective-permute-start(bf16[4,256,256]{2,1,0:T(8,128)(2,1)S(1)} %all_to_all.27.z), channel_id=1, source_target_pairs={{0,1},{1,0},{2,3},{3,2},{4,5},{5,4},{6,7},{7,6},{8,9},{9,8},{10,11... | collective-permute-start | bytes 1572872 | tf_op jit(solution)/shard_map/ppermute | solution.py:544
Sparse Core Ops, SparseCore 0:
  20.6 66.0 all-gather.4
  89.6 48.2 all-gather.6

commit v8 on v7

--- a/solution.py
+++ b/solution.py
@@ -40,18 +40,16 @@
     return jax.ShapeDtypeStruct(shape, dtype)
 
 
-def pack_kernel(own, key, value, pool, low, query, gate, pool_rows, state_rows, early, late):
-    at = 0
-    for r in (key, value, pool, low):
-        early[:, at : at + r.shape[1]] = r[...]
-        at += r.shape[1]
+def pack_late_kernel(own, query, gate, pool_rows, state_rows, late):
     mine = pl.ds(pl.multiple_of(own[0] * LANES, LANES), LANES)
     blocks = (query[...], gate[...], pool_rows[:, mine], state_rows[:, mine])
     for j, block in enumerate(blocks):
         late[:, j * LANES : (j + 1) * LANES] = block
 
 
-def prep_kernel(act, gain, x, inverse, held, arrived):
+def prep_kernel(
+    act, gain, key, value, pool, low, x, inverse, early, held, made, arrived, left
+):
     tokens, width = act.shape
     rows = tokens // 4
     copies = []
@@ -59,7 +57,12 @@
         at = pl.ds(c * rows, rows)
         copies.append(pltpu.make_async_copy(act.at[at], held.at[at], arrived.at[c]))
         copies[c].start()
+    at = 0
+    for r in (key, value, pool, low):
+        early[:, at : at + r.shape[1]] = r[...]
+        at += r.shape[1]
     half = lax.broadcasted_iota(jnp.int32, (rows, LANES), 1) < HEAD
+    out = []
     for c in range(4):
         copies[c].wait()
         block = pl.ds(c * rows, rows)
@@ -73,30 +76,42 @@
                 tiles.append(t * gain[:, at : at + LANES])
             to = slice(p * LANES, (p + 1) * LANES)
             for j, (a, b) in enumerate(((tiles[0], tiles[2]), (tiles[1], tiles[3]))):
-                x[2 * j, block, to] = jnp.where(half, a, pltpu.roll(b, HEAD, 1)).astype(bf16)
-                x[2 * j + 1, block, to] = jnp.where(half, pltpu.roll(a, HEAD, 1), b).astype(bf16)
+                made[2 * j, block, to] = jnp.where(half, a, pltpu.roll(b, HEAD, 1)).astype(bf16)
+                made[2 * j + 1, block, to] = jnp.where(half, pltpu.roll(a, HEAD, 1), b).astype(bf16)
+        for f in range(4):
+            out.append(
+                pltpu.make_async_copy(made.at[f, block], x.at[f, block], left.at[4 * c + f])
+            )
+            out[-1].start()
         total = jnp.sum(squares, axis=1, keepdims=True)
         inverse[block] = jnp.broadcast_to(lax.rsqrt(total / width + norm_eps), (rows, LANES))
-
-
-def prepare(act, gain):
+    for o in out:
+        o.wait()
+
+
+def prepare(act, gain, *weights):
     tokens, width = act.shape
     vmem = pl.BlockSpec(memory_space=pltpu.VMEM)
+    anywhere = pl.BlockSpec(memory_space=pl.ANY)
+    shape = (4, tokens, width // 4)
+    columns = sum(w.shape[1] for w in weights)
     return pl.pallas_call(
         prep_kernel,
-        in_specs=[pl.BlockSpec(memory_space=pl.ANY), vmem],
-        out_specs=[vmem, vmem],
-        out_shape=[struct((4, tokens, width // 4), bf16), struct((tokens, LANES), f32)],
-        scratch_shapes=[pltpu.VMEM((tokens, width), bf16), pltpu.SemaphoreType.DMA((4,))],
+        in_specs=[anywhere] + [vmem] * (1 + len(weights)),
+        out_specs=[anywhere, vmem, vmem],
+        out_shape=[
+            struct(shape, bf16),
+            struct((tokens, LANES), f32),
+            struct((weights[0].shape[0], columns), bf16),
+        ],
+        scratch_shapes=[
+            pltpu.VMEM((tokens, width), bf16),
+            pltpu.VMEM(shape, bf16),
+            pltpu.SemaphoreType.DMA((4,)),
+            pltpu.SemaphoreType.DMA((16,)),
+        ],
         name="prep",
-    )(act, gain)
-
-
-def thirds(x):
-    first = x.astype(bf16)
-    left = x - first.astype(f32)
-    second = left.astype(bf16)
-    return first, second, (left - second.astype(f32)).astype(bf16)
+    )(act, gain, *weights)
 
 
 def early_kernel(x, w, out, same_x, made, left):
@@ -121,15 +136,23 @@
 def late_kernel(x, w, out, quarter, held, made, arrived, left):
     tokens = x.shape[1]
     columns = 2 * LANES
-    into = pltpu.make_async_copy(w, held, arrived)
-    into.start()
-    into.wait()
+    depth = w.shape[0] // 4
+    into = []
+    for c in range(4):
+        at = pl.ds(c * depth, depth)
+        into.append(pltpu.make_async_copy(w.at[at], held.at[at], arrived.at[c]))
+        into[c].start()
+    first = jnp.zeros((tokens, columns), f32)
+    for c in range(4):
+        into[c].wait()
+        at = slice(c * depth, (c + 1) * depth)
+        first = first + jnp.dot(x[0, :, at], held[at, :columns], preferred_element_type=f32)
     across = pltpu.make_async_copy(held.at[:, columns:], quarter, left.at[4])
     across.start()
     weight = held[:, :columns]
     copies = [across]
     for f in range(4):
-        p = jnp.dot(x[f], weight, preferred_element_type=f32)
+        p = first if f == 0 else jnp.dot(x[f], weight, preferred_element_type=f32)
         made[f, :tokens] = p[:, :LANES].astype(bf16)
         made[f, tokens:] = p[:, LANES:].astype(bf16)
         copies.append(pltpu.make_async_copy(made.at[f], out.at[f], left.at[f]))
@@ -168,7 +191,7 @@
         scratch_shapes=[
             pltpu.VMEM(w.shape, bf16),
             pltpu.VMEM(shape, bf16),
-            pltpu.SemaphoreType.DMA,
+            pltpu.SemaphoreType.DMA((4,)),
             pltpu.SemaphoreType.DMA((5,)),
         ],
         compiler_params=limit,
@@ -448,23 +471,26 @@
     columns = pooling_output_rows.shape[1]
     own = lax.axis_index("fs").astype(jnp.int32).reshape(1)
     tp = lax.axis_index("tp").astype(jnp.int32)
-    early, late = call(
-        pack_kernel,
-        [struct((rows, 3 * LANES + HEAD), bf16), struct((rows, 4 * LANES), bf16)],
-        "pack",
+    (late,) = call(
+        pack_late_kernel,
+        [struct((rows, 4 * LANES), bf16)],
+        "pack_late",
         own,
+        query_projection_weight,
+        output_gate_weight,
+        pooling_output_rows,
+        attention_output_rows,
+    )
+    late, activations = lax.optimization_barrier((late, activations))
+    late = lax.all_gather(late, "sp", axis=0, tiled=True)
+    x, inverse, early = prepare(
+        activations.reshape(tokens, width),
+        input_norm_gain.reshape(1, width),
         key_projection_weight,
         value_projection_weight,
         pooling_channel_weight,
         decay_first_factor,
-        query_projection_weight,
-        output_gate_weight,
-        pooling_output_rows,
-        attention_output_rows,
-    )
-    late, early, activations = lax.optimization_barrier((late, early, activations))
-    late = lax.all_gather(late, "sp", axis=0, tiled=True)
-    x, inverse = prepare(activations.reshape(tokens, width), input_norm_gain.reshape(1, width))
+    )
     x = lax.all_to_all(x, "fs", 0, 0)
     early = lax.all_gather(early, "sp").reshape(-1, early.shape[1])
     inverse = near(inverse)

time: 159 us -> 159 us (level)
  no operation moved by 1% of the time
where the time goes in v8:
time: 159 us; the launch traced here: 158 us
  blocking collectives  84.3 us (53%)
  waiting for transfers between devices  22.2 us (14%)
  Pallas kernels  19.5 us (12%)
  starting transfers between devices  18.9 us (12%)
  between operations  13.6 us (9%)
    all_gather x1, blocking collectives, body(): early = lax.all_gather(early, 'sp').reshape(-1, early.shape[1])  37.1 us
    all_gather x1, blocking collectives, body(): runs = lax.all_gather(total[0], 'sp', axis_index_groups=strided)  14.7 us
    all_to_all x1, blocking collectives, body(): parts = lax.all_to_all(parts, 'fs', 0, 0)  13.8 us
    all_gather x1, waiting for transfers between devices, body(): late = lax.all_gather(late, 'sp', axis=0, tiled=True)  12.6 us
    all_to_all x1, blocking collectives, body(): same = lax.all_to_all(mine, 'tp', 0, 0, axis_index_groups=groups)  10.9 us
    ppermute x1, starting transfers between devices, body(): other = lax.ppermute(same, 'tp', [(i, i ^ 1) for i in range(peers)])  9.5 us
    all_gather x1, waiting for transfers between devices, body(): out_rows = lax.all_gather(quarter, 'fs')  8.81 us
    all_to_all x1, blocking collectives, body(): quad = lax.all_to_all(spread, 'sp', 0, 0, axis_index_groups=quads)  7.74 us
  transfers between devices with their start and end apart: 5, of which 2 were waited for; matrix products, arithmetic and copies ran while one was open for 0% of the time, Pallas kernels for 5%

profile of v8, /device:TPU:1, one launch (start us, length us, event | category | flops | bytes accessed | tf_op | source)
XLA Modules:
  0.0 158.5 jit_solution(5711921298379568680)
XLA Ops:
  6.5 1.5 shard_map.163
  8.1 4.7 %prep.1 = (bf16[4,256,1024]{2,1,0:T(8,128)(2,1)}, f32[256,128]{1,0:T(8,128)}, bf16[64,448]{1,0:T(8,128)(2,1)}) custom-call(bf16[256,4096]{1,0:T(8,128)(2,1)} %bitcast.23, f32[1,4096]{1,0:T(1,128)} %bitcast.25, bf16[64,128]{1,0:T(8,128)(2,1)} %key.1, bf16[64,128]{1,0:T(8,128)(2,1)} %value.1, bf16[64,128]{1,0:T(8,128)(2,1)} %pool.1, bf16[64,64]{1,0:T(8,128)(2,1)} %low.1), custom_call_target="tpu_custom_call" | custom-call | tf_op jit(solution)/shard_map/prep/pallas_call | solution.py:98
  12.8 5.1 %all-to-all-start = ((bf16[4,256,1024]{2,1,0:T(8,128)(2,1)}), bf16[4,256,1024]{2,1,0:T(8,128)(2,1)S(1)}, u32[]{:S(2)}, u32[]{:S(2)}) async-start(bf16[4,256,1024]{2,1,0:T(8,128)(2,1)} %get-tuple-element.30), calls=%async_computation | async-start | bytes 4194304 | tf_op jit(solution)/shard_map/all_to_all | solution.py:494
  18.0 0.7 all-gather.5.cloned.1.call-update
  18.7 0.0 all-gather.7.cloned.1.call-start
  18.8 37.1 %all-gather.w = bf16[1024,448]{1,0:T(8,128)(2,1)S(1)} all-gather(bf16[64,448]{1,0:T(8,128)(2,1)S(1)} %copy-done.7), channel_id=2, replica_groups=mesh['sp'=16,'fs'=4,'tp'=8] {'sp'}, dimensions={0}, use_global_device_ids=true | all-gather | bytes 974848 | tf_op jit(solution)/shard_map/all_gather | solution.py:495
  55.9 0.0 all-to-all-done.x
  55.9 3.2 %early_parts.1 = (bf16[4,896,128]{2,1,0:T(8,128)(2,1)S(1)}, bf16[4,256,1024]{2,1,0:T(8,128)(2,1)S(1)}) custom-call(bf16[4,256,1024]{2,1,0:T(8,128)(2,1)S(1)} %all-to-all-done.x, bf16[1024,448]{1,0:T(8,128)(2,1)S(1)} %all-gather.w), custom_call_target="tpu_custom_call", output_to_operand_aliasing={{1}: (0, {})} | custom-call | tf_op jit(solution)/shard_map/early_parts/pallas_call | solution.py:169
  59.1 13.8 %all_to_all.25.parts = bf16[4,896,128]{2,1,0:T(8,128)(2,1)S(1)} all-to-all(bf16[4,896,128]{2,1,0:T(8,128)(2,1)S(1)} %get-tuple-element.34), channel_id=1, replica_groups=mesh['sp'=16,'fs'=4,'tp'=8] {'fs'}, dimensions={0} | all-to-all | bytes 1835008 | tf_op jit(solution)/shard_map/all_to_all | solution.py:498
  72.9 1.4 shard_map.164
  74.3 12.6 %all-gather.5.cloned.1.call-done.w = bf16[1024,512]{1,0:T(8,128)(2,1)} async-done(((bf16[64,512]{1,0:T(8,128)(2,1)}), bf16[1024,512]{1,0:T(8,128)(2,1)}) %all-gather.5.cloned.1.call-update) | async-done | bytes 1048592 | tf_op jit(solution)/shard_map/all_gather | solution.py:485
  87.0 2.8 %late_parts.1 = (bf16[4,512,128]{2,1,0:T(8,128)(2,1)}, bf16[1024,256]{1,0:T(8,128)(2,1)}) custom-call(bf16[4,256,1024]{2,1,0:T(8,128)(2,1)S(1)} %get-tuple-element.32.x, bf16[1024,512]{1,0:T(8,128)(2,1)} %all-gather.5.cloned.1.call-done.w), custom_call_target="tpu_custom_call" | custom-call | tf_op jit(solution)/shard_map/late_parts/pallas_call | solution.py:186
  89.8 0.0 all-gather.7.cloned.1.call-update
  89.8 7.7 %all_to_all.26.quad = bf16[4,96,128]{2,1,0:T(8,128)(2,1)S(1)} all-to-all(bf16[4,96,128]{2,1,0:T(8,128)(2,1)S(1)} %get-tuple-element.36), channel_id=1, replica_groups={{0,32,64,96},{128,160,192,224},{256,288,320,352},{384,416,448,480},{1,3..., dimensions={0} | all-to-all | bytes 196608 | tf_op jit(solution)/shard_map/all_to_all | solution.py:522
  97.5 4.2 %all-to-all-start.3 = ((bf16[4,512,128]{2,1,0:T(8,128)(2,1)}), bf16[4,512,128]{2,1,0:T(8,128)(2,1)S(1)}, u32[]{:S(2)}, u32[]{:S(2)}) async-start(bf16[4,512,128]{2,1,0:T(8,128)(2,1)} %get-tuple-element.38), calls=%async_computation.3 | async-start | bytes 1048576 | tf_op jit(solution)/shard_map/all_to_all | solution.py:526
  101.7 0.1 copy.21.start
  101.8 0.7 shard_map.165
  102.5 14.7 %all_gather.21.runs = bf16[4,96,128]{2,1,0:T(8,128)(2,1)S(1)} all-gather(bf16[1,96,128]{2,1,0:T(8,128)(2,1)} %get-tuple-element.41), channel_id=1, replica_groups={{0,128,256,384},{32,160,288,416},{64,192,320,448},{96,224,352,480},{1,1..., dimensions={0}, use_global_device_ids=true | all-gather | bytes 122880 | tf_op jit(solution)/shard_map/all_gather | solution.py:541
  117.3 1.2 shard_map.166
  118.5 10.9 %all_to_all.27.z = bf16[4,256,256]{2,1,0:T(8,128)(2,1)S(1)} all-to-all(bf16[4,256,256]{2,1,0:T(8,128)(2,1)S(1)} %shard_map.166), channel_id=1, replica_groups={{0,2,4,6},{1,3,5,7},{8,10,12,14},{9,11,13,15},{16,18,20,22},{17,19,21,2..., dimensions={0} | all-to-all | bytes 1048576 | tf_op jit(solution)/shard_map/all_to_all | solution.py:568
  129.4 8.8 %all-gather.7.cloned.1.call-done = bf16[4096,256]{1,0:T(8,128)(2,1)} async-done(((bf16[1024,256]{1,0:T(8,128)(2,1)}), bf16[4096,256]{1,0:T(8,128)(2,1)}) %all-gather.7.cloned.1.call-update) | async-done | bytes 2097168 | tf_op jit(solution)/shard_map/all_gather | solution.py:525
  138.2 9.5 %collective-permute-start = (bf16[4,256,256]{2,1,0:T(8,128)(2,1)S(1)}, bf16[4,256,256]{2,1,0:T(8,128)(2,1)S(1)}, u32[]{:S(2)}, u32[]{:S(2)}) collective-permute-start(bf16[4,256,256]{2,1,0:T(8,128)(2,1)S(1)} %all_to_all.27.z), channel_id=1, source_target_pairs={{0,1},{1,0},{2,3},{3,2},{4,5},{5,4},{6,7},{7,6},{8,9},{9,8},{10,11... | collective-permute-start | bytes 1572872 | tf_op jit(solution)/shard_map/ppermute | solution.py:570
  147.7 1.6 %shard_map.167.rest_0_ = f32[256,512]{1,0:T(8,128)S(1)} custom-call(s32[1]{0:T(128)} %bitcast.core, bf16[4,256,256]{2,1,0:T(8,128)(2,1)S(1)} %all_to_all.27.z, bf16[4,1024,256]{2,1,0:T(8,128)(2,1)} %bitcast.21), custom_call_target="tpu_custom_call" | custom-call | tf_op jit(solution)/shard_map/pallas_call | solution.py:433
  149.4 2.3 %shard_map.168 = bf16[256,512]{1,0:T(8,128)(2,1)} custom-call(s32[1]{0:T(128)S(6)} %sub.3.core, bf16[4,256,256]{2,1,0:T(8,128)(2,1)S(1)} %collective-permute-done.z, bf16[4,1024,256]{2,1,0:T(8,128)(2,1)} %bitcast.22, f32[256,512]{1,0:T(8,128)S(1)} %shard_map.167.rest_0_), custom_call_target="tpu_custom_call" | custom-call | tf_op jit(solution)/shard_map/pallas_call | solution.py:433
  (21 shorter events, 0.0 us)
Async XLA Ops:
  12.8 5.9 %copy-start.7 = (bf16[64,448]{1,0:T(8,128)(2,1)S(1)}, bf16[64,448]{1,0:T(8,128)(2,1)}, u32[]{:S(2)}) copy-start(bf16[64,448]{1,0:T(8,128)(2,1)} %get-tuple-element.31) | copy-start | bytes 172036
  12.8 43.1 %all-to-all-start = ((bf16[4,256,1024]{2,1,0:T(8,128)(2,1)}), bf16[4,256,1024]{2,1,0:T(8,128)(2,1)S(1)}, u32[]{:S(2)}, u32[]{:S(2)}) async-start(bf16[4,256,1024]{2,1,0:T(8,128)(2,1)} %get-tuple-element.30), calls=%async_computation | async-start | bytes 4194304 | tf_op jit(solution)/shard_map/all_to_all | solution.py:494
  18.0 69.0 %all-gather.5.cloned.1.call-start = ((), (), s32[]{:S(2)}) async-start(), calls=%async_computation.5 | async-start | bytes 1114112 | tf_op jit(solution)/shard_map/all_gather | solution.py:485
  18.7 119.5 %all-gather.7.cloned.1.call-start = ((), (), s32[]{:S(2)}) async-start(), calls=%async_computation.6 | async-start | bytes 2621440 | tf_op jit(solution)/shard_map/all_gather | solution.py:525
  55.9 17.0 %copy-start = (f32[256,128]{1,0:T(8,128)S(1)}, f32[256,128]{1,0:T(8,128)}, u32[]{:S(2)}) copy-start(f32[256,128]{1,0:T(8,128)} %get-tuple-element.35.inverse) | copy-start | bytes 393220
  55.9 17.0 %copy-start.2 = (bf16[64,128]{1,0:T(8,128)(2,1)S(1)}, bf16[64,128]{1,0:T(8,128)(2,1)}, u32[]{:S(2)}) copy-start(bf16[64,128]{1,0:T(8,128)(2,1)} %second.1) | copy-start | bytes 49156
  55.9 17.0 %copy-start.3 = (f32[2,256]{1,0:T(2,128)S(1)}, f32[2,256]{1,0:T(2,128)}, u32[]{:S(2)}) copy-start(f32[2,256]{1,0:T(2,128)} %extra.1) | copy-start | bytes 6148
  55.9 17.0 %copy-start.4 = (f32[128]{0:T(128)S(1)}, f32[128]{0:T(128)}, u32[]{:S(2)}) copy-start(f32[128]{0:T(128)} %param.26) | copy-start | bytes 1540
  87.0 14.8 %copy-start.8 = (f32[1,2,64,64]{3,2,1,0:T(8,128)S(1)}, f32[1,2,64,64]{3,2,1,0:T(8,128)}, u32[]{:S(2)}) copy-start(f32[1,2,64,64]{3,2,1,0:T(8,128)} %param.29) | copy-start | bytes 98308
  87.0 30.3 %copy-start.1 = (bf16[1,128,128]{2,1,0:T(8,128)(2,1)S(1)}, bf16[1,128,128]{2,1,0:T(8,128)(2,1)}, u32[]{:S(2)}) copy-start(bf16[1,128,128]{2,1,0:T(8,128)(2,1)} %param.30) | copy-start | bytes 98308
  87.0 30.3 %copy-start.5 = (f32[128]{0:T(128)S(1)}, f32[128]{0:T(128)}, u32[]{:S(2)}) copy-start(f32[128]{0:T(128)} %param.28) | copy-start | bytes 1540
  87.0 30.3 %copy-start.6 = (f32[128]{0:T(128)S(1)}, f32[128]{0:T(128)}, u32[]{:S(2)}) copy-start(f32[128]{0:T(128)} %param.31) | copy-start | bytes 1540
  97.5 19.7 %all-to-all-start.3 = ((bf16[4,512,128]{2,1,0:T(8,128)(2,1)}), bf16[4,512,128]{2,1,0:T(8,128)(2,1)S(1)}, u32[]{:S(2)}, u32[]{:S(2)}) async-start(bf16[4,512,128]{2,1,0:T(8,128)(2,1)} %get-tuple-element.38), calls=%async_computation.3 | async-start | bytes 1048576 | tf_op jit(solution)/shard_map/all_to_all | solution.py:526
  138.2 11.1 %collective-permute-start = (bf16[4,256,256]{2,1,0:T(8,128)(2,1)S(1)}, bf16[4,256,256]{2,1,0:T(8,128)(2,1)S(1)}, u32[]{:S(2)}, u32[]{:S(2)}) collective-permute-start(bf16[4,256,256]{2,1,0:T(8,128)(2,1)S(1)} %all_to_all.27.z), channel_id=1, source_target_pairs={{0,1},{1,0},{2,3},{3,2},{4,5},{5,4},{6,7},{7,6},{8,9},{9,8},{10,11... | collective-permute-start | bytes 1572872 | tf_op jit(solution)/shard_map/ppermute | solution.py:570
Sparse Core Ops, SparseCore 0:
  20.9 66.0 all-gather.4
  89.9 48.2 all-gather.6

commit v9 on v8

--- a/solution.py
+++ b/solution.py
@@ -10,7 +10,7 @@
 HEAD = 64
 LANES = 128
 HALO = 16
-RUN_ROWS = 96
+RUN_ROWS = 80
 norm_eps = 1e-06
 decay_temper = 16.0
 highest = lax.Precision.HIGHEST
@@ -40,15 +40,15 @@
     return jax.ShapeDtypeStruct(shape, dtype)
 
 
-def pack_late_kernel(own, query, gate, pool_rows, state_rows, late):
+def pack_late_kernel(own, query, gate, pool, pool_rows, state_rows, late):
     mine = pl.ds(pl.multiple_of(own[0] * LANES, LANES), LANES)
-    blocks = (query[...], gate[...], pool_rows[:, mine], state_rows[:, mine])
+    blocks = (query[...], gate[...], pool[...], pool_rows[:, mine], state_rows[:, mine])
     for j, block in enumerate(blocks):
         late[:, j * LANES : (j + 1) * LANES] = block
 
 
 def prep_kernel(
-    act, gain, key, value, pool, low, x, inverse, early, held, made, arrived, left
+    act, gain, key, value, low, x, inverse, early, held, made, arrived, left
 ):
     tokens, width = act.shape
     rows = tokens // 4
@@ -58,7 +58,7 @@
         copies.append(pltpu.make_async_copy(act.at[at], held.at[at], arrived.at[c]))
         copies[c].start()
     at = 0
-    for r in (key, value, pool, low):
+    for r in (key, value, low):
         early[:, at : at + r.shape[1]] = r[...]
         at += r.shape[1]
     half = lax.broadcasted_iota(jnp.int32, (rows, LANES), 1) < HEAD
@@ -114,28 +114,29 @@
     )(act, gain, *weights)
 
 
-def early_kernel(x, w, out, same_x, made, left):
+def early_kernel(x, w, out, same_x, ends, made, left):
     tokens = x.shape[1]
     half = lax.broadcasted_iota(jnp.int32, (tokens // 2, LANES), 1) < HEAD
     weight = w[...]
     copies = []
     for f in range(4):
         p = jnp.dot(x[f], weight, preferred_element_type=f32)
-        for j in range(3):
+        for j in range(2):
             at = slice(j * tokens, (j + 1) * tokens)
             made[f, at] = p[:, j * LANES : (j + 1) * LANES].astype(bf16)
-        d = jnp.concatenate([p[:, 3 * LANES :], p[:, 3 * LANES :]], axis=1)
+        d = jnp.concatenate([p[:, 2 * LANES :], p[:, 2 * LANES :]], axis=1)
         d = jnp.where(half, d[: tokens // 2], d[tokens // 2 :])
-        made[f, 3 * tokens :] = d.astype(bf16)
+        made[f, 2 * tokens :] = d.astype(bf16)
+        ends[f] = x[f, tokens - HALO :]
         copies.append(pltpu.make_async_copy(made.at[f], out.at[f], left.at[f]))
         copies[f].start()
     for c in copies:
         c.wait()
 
 
-def late_kernel(x, w, out, quarter, held, made, arrived, left):
+def late_kernel(x, w, ends, out, quarter, held, made, arrived, left):
     tokens = x.shape[1]
-    columns = 2 * LANES
+    columns = 3 * LANES
     depth = w.shape[0] // 4
     into = []
     for c in range(4):
@@ -153,8 +154,11 @@
     copies = [across]
     for f in range(4):
         p = first if f == 0 else jnp.dot(x[f], weight, preferred_element_type=f32)
-        made[f, :tokens] = p[:, :LANES].astype(bf16)
-        made[f, tokens:] = p[:, LANES:].astype(bf16)
+        for j in range(3):
+            at = slice(j * tokens, (j + 1) * tokens)
+            made[f, at] = p[:, j * LANES : (j + 1) * LANES].astype(bf16)
+        edge = jnp.dot(ends[f], weight[:, 2 * LANES :], preferred_element_type=f32)
+        made[f, 3 * tokens :] = edge.astype(bf16)
         copies.append(pltpu.make_async_copy(made.at[f], out.at[f], left.at[f]))
         copies[f + 1].start()
     for c in copies:
@@ -162,15 +166,19 @@
 
 
 def early_partials(x, w):
-    _, tokens, _ = x.shape
+    _, tokens, depth = x.shape
     vmem = pl.BlockSpec(memory_space=pltpu.VMEM)
     anywhere = pl.BlockSpec(memory_space=pl.ANY)
     shape = (4, tokens * w.shape[1] // LANES, LANES)
     return pl.pallas_call(
         early_kernel,
         in_specs=[vmem, vmem],
-        out_specs=[anywhere, vmem],
-        out_shape=[struct(shape, bf16), pltpu.VMEM(x.shape, bf16)],
+        out_specs=[anywhere, vmem, vmem],
+        out_shape=[
+            struct(shape, bf16),
+            pltpu.VMEM(x.shape, bf16),
+            struct((4, HALO, depth), bf16),
+        ],
         scratch_shapes=[pltpu.VMEM(shape, bf16), pltpu.SemaphoreType.DMA((4,))],
         input_output_aliases={0: 1},
         compiler_params=limit,
@@ -178,16 +186,16 @@
     )(x, w)
 
 
-def late_partials(x, w):
+def late_partials(x, w, ends):
     _, tokens, depth = x.shape
     vmem = pl.BlockSpec(memory_space=pltpu.VMEM)
     anywhere = pl.BlockSpec(memory_space=pl.ANY)
-    shape = (4, 2 * tokens, LANES)
+    shape = (4, 3 * tokens + HALO, LANES)
     return pl.pallas_call(
         late_kernel,
-        in_specs=[vmem, pl.BlockSpec(memory_space=pltpu.HBM)],
+        in_specs=[vmem, pl.BlockSpec(memory_space=pltpu.HBM), vmem],
         out_specs=[anywhere, anywhere],
-        out_shape=[struct(shape, bf16), struct((depth, w.shape[1] - 2 * LANES), bf16)],
+        out_shape=[struct(shape, bf16), struct((depth, w.shape[1] - 3 * LANES), bf16)],
         scratch_shapes=[
             pltpu.VMEM(w.shape, bf16),
             pltpu.VMEM(shape, bf16),
@@ -196,7 +204,7 @@
         ],
         compiler_params=limit,
         name="late_parts",
-    )(x, pltpu.with_memory_space_constraint(w, pltpu.HBM))
+    )(x, pltpu.with_memory_space_constraint(w, pltpu.HBM), ends)
 
 
 def total_of(parts, at, rows):
@@ -223,15 +231,13 @@
 
 
 def local_kernel(
-    parts, inverse, second, bias, extra, keys, values, pool, sums, prior, opening, spread
+    parts, inverse, second, bias, extra, keys, values, sums, prior, opening, spread
 ):
     inv = inverse[...]
     tokens = inv.shape[0]
     keys[...] = projected(parts, inv, 0).astype(f32)
     values[...] = projected(parts, inv, 1).astype(f32)
-    pooled = projected(parts, inv, 2)
-    pool[...] = pooled
-    both = total_of(parts, 3 * tokens, tokens // 2)
+    both = total_of(parts, 2 * tokens, tokens // 2)
     low = jnp.concatenate([both[:, :HEAD], both[:, HEAD:]], axis=0)
     low = (low * inv[:, :HEAD]).astype(bf16)
     x = jnp.dot(low, second[...], preferred_element_type=f32) + bias[...]
@@ -263,42 +269,46 @@
         opening[n : n + 1] = before
         state = jnp.exp(final) * state + heads_of(pairs, half)
         before = before + final
+    row = lax.broadcasted_iota(jnp.int32, (HALO, LANES), 0)
+    lane = lax.broadcasted_iota(jnp.int32, (HALO, LANES), 1)
+    last = jnp.sum(jnp.where(row == lane, inv[tokens - HALO :], 0.0), axis=0, keepdims=True)
+    mine = run_of(state, before, last)
     for to in range(spread.shape[0]):
-        write_run(spread, to, state, before, pooled[tokens - HALO :])
-
-
-def write_run(out, to, state, log, tail):
+        spread[to] = mine
+
+
+def run_of(state, log, inverse):
     row = lax.broadcasted_iota(jnp.int32, (HALO, LANES), 0)
-    logs = jnp.zeros((HALO, LANES), f32)
-    for j, part in enumerate(thirds(log)):
-        logs = jnp.where(row == j, part.astype(f32), logs)
-    out[to, :HEAD] = state.astype(bf16)
-    out[to, HEAD : HEAD + HALO] = logs.astype(bf16)
-    out[to, HEAD + HALO :] = tail
+    extra = jnp.zeros((HALO, LANES), f32)
+    for j, part in enumerate(thirds(log) + thirds(inverse)):
+        extra = jnp.where(row == j, part.astype(f32), extra)
+    return jnp.concatenate([state, extra], axis=0).astype(bf16)
 
 
 def read_run(came):
     came = came.astype(f32)
     log = came[HEAD : HEAD + 1] + came[HEAD + 1 : HEAD + 2] + came[HEAD + 2 : HEAD + 3]
-    return came[:HEAD], log
-
-
-def quad_kernel(sp, quad, total, within, log_within, previous):
+    inverse = came[HEAD + 3 : HEAD + 4] + came[HEAD + 4 : HEAD + 5] + came[HEAD + 5 : HEAD + 6]
+    return came[:HEAD], log, inverse
+
+
+def quad_kernel(sp, quad, total, within, log_within, inverse_within):
     place = sp[0] % 4
     state = jnp.zeros((HEAD, LANES), f32)
     log = jnp.zeros((1, LANES), f32)
+    inverse = jnp.zeros((1, LANES), f32)
     for j in range(4):
 
         @pl.when(place == j)
-        def _(state=state, log=log):
+        def _(state=state, log=log, inverse=inverse):
             within[...] = state
             log_within[...] = jnp.broadcast_to(log, log_within.shape)
-
-        s, decay = read_run(quad[j])
+            inverse_within[...] = jnp.broadcast_to(inverse, inverse_within.shape)
+
+        s, decay, inverse = read_run(quad[j])
         state = jnp.exp(decay) * state + s
         log = log + decay
-    write_run(total, 0, state, log, quad[3, HEAD + HALO :])
-    previous[...] = quad[jnp.maximum(place - 1, 0), HEAD + HALO :]
+    total[0] = run_of(state, log, inverse)
 
 
 def finish_kernel(
@@ -307,11 +317,10 @@
     runs,
     within_quad,
     log_within,
-    previous,
+    inverse_within,
     start,
     parts,
     inverse,
-    pool,
     keys,
     values,
     sums,
@@ -326,9 +335,11 @@
     tokens = inv.shape[0]
     place = sp[0]
     state = start[...]
+    edge = jnp.zeros((1, LANES), f32)
     for j in range(runs.shape[0]):
-        came, log = read_run(runs[j])
+        came, log, outside = read_run(runs[j])
         state = jnp.where(j < place // 4, jnp.exp(log) * state + came, state)
+        edge = jnp.where(j < place // 4, outside, edge)
     state = jnp.exp(log_within[:1]) * state + within_quad[...]
     queries = projected(parts, inv, 0).astype(f32) * HEAD ** (-0.5)
     outgate = projected(parts, inv, 1).astype(f32)
@@ -374,10 +385,12 @@
         for to in range(mine.shape[0]):
             mine[to, at, LANES:] = done
 
-    current = pool[...].astype(f32)
-    outside = runs[jnp.maximum(place // 4 - 1, 0), HEAD + HALO :].astype(f32)
-    outside = jnp.where(place >= 4, outside, 0.0)
-    before = jnp.where(place % 4 > 0, previous[...].astype(f32), outside)
+    current = projected(parts, inv, 2).astype(f32)
+    edge = jnp.where(place % 4 > 0, inverse_within[:1], edge)
+    row = lax.broadcasted_iota(jnp.int32, (HALO, LANES), 0)
+    lane = lax.broadcasted_iota(jnp.int32, (HALO, LANES), 1)
+    scale = jnp.sum(jnp.where(row == lane, edge, 0.0), axis=1, keepdims=True)
+    before = (total_of(parts, 3 * tokens, HALO) * scale).astype(bf16).astype(f32)
     extended = jnp.concatenate([before, current], axis=0)
 
     def back(x, by):
@@ -473,11 +486,12 @@
     tp = lax.axis_index("tp").astype(jnp.int32)
     (late,) = call(
         pack_late_kernel,
-        [struct((rows, 4 * LANES), bf16)],
+        [struct((rows, 5 * LANES), bf16)],
         "pack_late",
         own,
         query_projection_weight,
         output_gate_weight,
+        pooling_channel_weight,
         pooling_output_rows,
         attention_output_rows,
     )
@@ -488,21 +502,21 @@
         input_norm_gain.reshape(1, width),
         key_projection_weight,
         value_projection_weight,
-        pooling_channel_weight,
         decay_first_factor,
     )
     x = lax.all_to_all(x, "fs", 0, 0)
     early = lax.all_gather(early, "sp").reshape(-1, early.shape[1])
     inverse = near(inverse)
-    parts, x = early_partials(near(x), near(early))
+    parts, x, ends = early_partials(near(x), near(early))
+    count = lax.axis_size("sp")
+    ends = lax.ppermute(ends, "sp", [(i, i + 1) for i in range(count - 1)])
     parts = lax.all_to_all(parts, "fs", 0, 0)
     wide = pltpu.VMEM((tokens, LANES), f32)
-    keys, values, pool, sums, prior, opening, spread = call(
+    keys, values, sums, prior, opening, spread = call(
         local_kernel,
         [
             wide,
             wide,
-            pltpu.VMEM((tokens, LANES), bf16),
             wide,
             wide,
             pltpu.VMEM((tokens // BLOCK, LANES), f32),
@@ -520,18 +534,18 @@
     quads = [[4 * a + b for b in range(4)] for a in range(lax.axis_size("sp") // 4)]
     late, _ = lax.optimization_barrier((late, spread))
     quad = lax.all_to_all(spread, "sp", 0, 0, axis_index_groups=quads)
-    late, quarter = late_partials(near(x), late)
+    late, quarter = late_partials(near(x), late, near(ends))
     _, _, quad = lax.optimization_barrier((late, quarter, quad))
     out_rows = lax.all_gather(quarter, "fs")
     late = lax.all_to_all(late, "fs", 0, 0)
     sp = lax.axis_index("sp").astype(jnp.int32).reshape(1)
-    total, within, log_within, previous = call(
+    total, within, log_within, inverse_within = call(
         quad_kernel,
         [
             struct((1, RUN_ROWS, LANES), bf16),
             pltpu.VMEM((HEAD, LANES), f32),
             pltpu.VMEM((8, LANES), f32),
-            pltpu.VMEM((HALO, LANES), bf16),
+            pltpu.VMEM((8, LANES), f32),
         ],
         "quad_total",
         sp,
@@ -549,11 +563,10 @@
         near(runs),
         near(within),
         near(log_within),
-        near(previous),
+        near(inverse_within),
         near(start),
         near(late),
         inverse,
-        near(pool),
         near(keys),
         near(values),
         near(sums),

time: 159 us -> 149 us (0.937)
  blocking collectives: 84.3 us -> 72.2 us
  waiting for transfers between devices: 22.2 us -> 17.4 us
  starting transfers between devices: 18.9 us -> 23.1 us
  local copies, waits for them, and re-layouts: 0.1 us -> 2.65 us
    all_to_all x1 -> x0, blocking collectives: 13.8 us -> none  [body(): parts = lax.all_to_all(parts, 'fs', 0, 0)]
    all_gather x1, waiting for transfers between devices: 12.6 us -> 3.04 us  [body(): late = lax.all_gather(late, 'sp', axis=0, tiled=True)]
    all_to_all x0 -> x1, waiting for transfers between devices: none -> 5.39 us  [body(): parts = lax.all_to_all(parts, 'fs', 0, 0)]
    all_to_all x0 -> x1, starting transfers between devices: none -> 3.87 us  [body(): parts = lax.all_to_all(parts, 'fs', 0, 0)]
    unnamed x18 -> x26, local copies, waits for them, and re-layouts: 0.03 us -> 2.59 us
    ppermute x0 -> x1, starting transfers between devices: none -> 2.29 us  [body(): ends = lax.ppermute(ends, 'sp', [(i, i + 1) for i in range(count - 1)])]
  transfers between devices with their start and end apart: 5 -> 7, of which waited for: 2 -> 3; matrix products, arithmetic and copies ran while one was open for 0% -> 0% of each run, Pallas kernels for 5% -> 8%
where the time goes in v9:
time: 149 us
  blocking collectives  72.2 us (48%)
  starting transfers between devices  23.1 us (16%)
  Pallas kernels  19.8 us (13%)
  waiting for transfers between devices  17.4 us (12%)
  between operations  13.6 us (9%)
  local copies, waits for them, and re-layouts  2.65 us (2%)
    all_gather x1, blocking collectives, body(): early = lax.all_gather(early, 'sp').reshape(-1, early.shape[1])  37.5 us
    all_gather x1, blocking collectives, body(): runs = lax.all_gather(total[0], 'sp', axis_index_groups=strided)  14.7 us
    all_to_all x1, blocking collectives, body(): same = lax.all_to_all(mine, 'tp', 0, 0, axis_index_groups=groups)  11.3 us
    all_gather x1, waiting for transfers between devices, body(): out_rows = lax.all_gather(quarter, 'fs')  8.92 us
    all_to_all x1, blocking collectives, body(): quad = lax.all_to_all(spread, 'sp', 0, 0, axis_index_groups=quads)  8.72 us
    ppermute x1, starting transfers between devices, body(): other = lax.ppermute(same, 'tp', [(i, i ^ 1) for i in range(peers)])  8.26 us
    all_to_all x1, waiting for transfers between devices, body(): parts = lax.all_to_all(parts, 'fs', 0, 0)  5.39 us
    all_to_all x1, starting transfers between devices, body(): x = lax.all_to_all(x, 'fs', 0, 0)  5.14 us
  transfers between devices with their start and end apart: 7, of which 3 were waited for; matrix products, arithmetic and copies ran while one was open for 0% of the time, Pallas kernels for 8%

profile of v9, /device:TPU:1, one launch (start us, length us, event | category | flops | bytes accessed | tf_op | source)
XLA Modules:
  0.0 148.7 jit_solution(17965819136096947683)
XLA Ops:
  6.5 1.6 %shard_map.163 = bf16[64,640]{1,0:T(8,128)(2,1)} custom-call(s32[1]{0:T(128)} %bitcast.3.own, bf16[64,128]{1,0:T(8,128)(2,1)} %query.1, bf16[64,128]{1,0:T(8,128)(2,1)} %gate.1, bf16[64,128]{1,0:T(8,128)(2,1)} %pool.1, bf16[64,512]{1,0:T(8,128)(2,1)} %pool_rows.1, bf16[64,512]{1,0:T(8,128)(2,1)} %state_rows.1), custom_call_target="tpu_custom_call" | custom-call | tf_op jit(solution)/shard_map/pallas_call | solution.py:25
  8.1 4.8 %prep.1 = (bf16[4,256,1024]{2,1,0:T(8,128)(2,1)}, f32[256,128]{1,0:T(8,128)}, bf16[64,320]{1,0:T(8,128)(2,1)}) custom-call(bf16[256,4096]{1,0:T(8,128)(2,1)} %bitcast.23, f32[1,4096]{1,0:T(1,128)} %bitcast.25, bf16[64,128]{1,0:T(8,128)(2,1)} %key.1, bf16[64,128]{1,0:T(8,128)(2,1)} %value.1, bf16[64,64]{1,0:T(8,128)(2,1)} %low.1), custom_call_target="tpu_custom_call" | custom-call | tf_op jit(solution)/shard_map/prep/pallas_call | solution.py:98
  12.9 5.1 %all-to-all-start = ((bf16[4,256,1024]{2,1,0:T(8,128)(2,1)}), bf16[4,256,1024]{2,1,0:T(8,128)(2,1)S(1)}, u32[]{:S(2)}, u32[]{:S(2)}) async-start(bf16[4,256,1024]{2,1,0:T(8,128)(2,1)} %get-tuple-element.30), calls=%async_computation | async-start | bytes 4194304 | tf_op jit(solution)/shard_map/all_to_all | solution.py:507
  18.1 37.5 %all-gather.w = bf16[1024,320]{1,0:T(8,128)(2,1)S(1)} all-gather(bf16[64,320]{1,0:T(8,128)(2,1)S(1)} %copy-done.12), channel_id=2, replica_groups=mesh['sp'=16,'fs'=4,'tp'=8] {'sp'}, dimensions={0}, use_global_device_ids=true | all-gather | bytes 696320 | tf_op jit(solution)/shard_map/all_gather | solution.py:508
  55.6 2.7 %early_parts.1 = (bf16[4,640,128]{2,1,0:T(8,128)(2,1)}, bf16[4,256,1024]{2,1,0:T(8,128)(2,1)S(1)}, bf16[4,16,1024]{2,1,0:T(8,128)(2,1)}) custom-call(bf16[4,256,1024]{2,1,0:T(8,128)(2,1)S(1)} %all-to-all-done.x, bf16[1024,320]{1,0:T(8,128)(2,1)S(1)} %all-gather.w), custom_call_target="tpu_custom_call", output_to_operand_aliasing={{1}: (0, {})} | custom-call | tf_op jit(solution)/shard_map/early_parts/pallas_call | solution.py:173
  58.3 3.9 %all-to-all-start.1 = ((bf16[4,640,128]{2,1,0:T(8,128)(2,1)}), bf16[4,640,128]{2,1,0:T(8,128)(2,1)S(1)}, u32[]{:S(2)}, u32[]{:S(2)}) async-start(bf16[4,640,128]{2,1,0:T(8,128)(2,1)} %get-tuple-element.34), calls=%async_computation.1 | async-start | bytes 1310720 | tf_op jit(solution)/shard_map/all_to_all | solution.py:513
  62.1 2.3 %collective-permute-start = (bf16[4,16,1024]{2,1,0:T(8,128)(2,1)}, bf16[4,16,1024]{2,1,0:T(8,128)(2,1)S(1)}, u32[]{:S(2)}, u32[]{:S(2)}) collective-permute-start(bf16[4,16,1024]{2,1,0:T(8,128)(2,1)} %get-tuple-element.38), channel_id=1, source_target_pairs={{0,32},{32,64},{64,96},{96,128},{128,160},{160,192},{192,224},{224... | collective-permute-start | bytes 393224 | tf_op jit(solution)/shard_map/ppermute | solution.py:512
  64.4 5.4 %all-to-all-done.1.parts = bf16[4,640,128]{2,1,0:T(8,128)(2,1)S(1)} async-done(((bf16[4,640,128]{2,1,0:T(8,128)(2,1)}), bf16[4,640,128]{2,1,0:T(8,128)(2,1)S(1)}, u32[]{:S(2)}, u32[]{:S(2)}) %all-to-all-start.1) | async-done | bytes 655392 | tf_op jit(solution)/shard_map/all_to_all | solution.py:513
  69.8 0.7 copy-done.5
  70.5 0.7 copy-done.10
  71.2 1.4 shard_map.164
  72.6 0.6 copy-done.1
  73.8 3.0 %all-gather.5.cloned.1.call-done.w = bf16[1024,640]{1,0:T(8,128)(2,1)} async-done(((bf16[64,640]{1,0:T(8,128)(2,1)}), bf16[1024,640]{1,0:T(8,128)(2,1)}) %all-gather.5.cloned.1.call-update) | async-done | bytes 1310736 | tf_op jit(solution)/shard_map/all_gather | solution.py:499
  76.8 3.6 %late_parts.1 = (bf16[4,784,128]{2,1,0:T(8,128)(2,1)}, bf16[1024,256]{1,0:T(8,128)(2,1)}) custom-call(bf16[4,256,1024]{2,1,0:T(8,128)(2,1)S(1)} %get-tuple-element.32.x, bf16[1024,640]{1,0:T(8,128)(2,1)} %all-gather.5.cloned.1.call-done.w, bf16[4,16,1024]{2,1,0:T(8,128)(2,1)S(1)} %collective-permute-done.ends), custom_call_target="tpu_custom_call" | custom-call | tf_op jit(solution)/shard_map/late_parts/pallas_call | solution.py:194
  80.5 8.7 %all_to_all.25.quad = bf16[4,80,128]{2,1,0:T(8,128)(2,1)S(1)} all-to-all(bf16[4,80,128]{2,1,0:T(8,128)(2,1)S(1)} %copy-done.2), channel_id=1, replica_groups={{0,32,64,96},{128,160,192,224},{256,288,320,352},{384,416,448,480},{1,3..., dimensions={0} | all-to-all | bytes 163840 | tf_op jit(solution)/shard_map/all_to_all | solution.py:536
  89.2 3.5 %all-to-all-start.3 = ((bf16[4,784,128]{2,1,0:T(8,128)(2,1)}), bf16[4,784,128]{2,1,0:T(8,128)(2,1)S(1)}, u32[]{:S(2)}, u32[]{:S(2)}) async-start(bf16[4,784,128]{2,1,0:T(8,128)(2,1)} %get-tuple-element.39), calls=%async_computation.3 | async-start | bytes 1605632 | tf_op jit(solution)/shard_map/all_to_all | solution.py:540
  92.8 0.7 shard_map.165
  93.5 14.7 %all_gather.21.runs = bf16[4,80,128]{2,1,0:T(8,128)(2,1)S(1)} all-gather(bf16[1,80,128]{2,1,0:T(8,128)(2,1)} %get-tuple-element.42), channel_id=1, replica_groups={{0,128,256,384},{32,160,288,416},{64,192,320,448},{96,224,352,480},{1,1..., dimensions={0}, use_global_device_ids=true | all-gather | bytes 102400 | tf_op jit(solution)/shard_map/all_gather | solution.py:555
  108.2 1.2 shard_map.166
  109.5 11.3 %all_to_all.26.z = bf16[4,256,256]{2,1,0:T(8,128)(2,1)S(1)} all-to-all(bf16[4,256,256]{2,1,0:T(8,128)(2,1)S(1)} %shard_map.166), channel_id=1, replica_groups={{0,2,4,6},{1,3,5,7},{8,10,12,14},{9,11,13,15},{16,18,20,22},{17,19,21,2..., dimensions={0} | all-to-all | bytes 1048576 | tf_op jit(solution)/shard_map/all_to_all | solution.py:581
  120.7 8.9 %all-gather.7.cloned.1.call-done = bf16[4096,256]{1,0:T(8,128)(2,1)} async-done(((bf16[1024,256]{1,0:T(8,128)(2,1)}), bf16[4096,256]{1,0:T(8,128)(2,1)}) %all-gather.7.cloned.1.call-update) | async-done | bytes 2097168 | tf_op jit(solution)/shard_map/all_gather | solution.py:539
  129.7 8.3 %collective-permute-start.1 = (bf16[4,256,256]{2,1,0:T(8,128)(2,1)S(1)}, bf16[4,256,256]{2,1,0:T(8,128)(2,1)S(1)}, u32[]{:S(2)}, u32[]{:S(2)}) collective-permute-start(bf16[4,256,256]{2,1,0:T(8,128)(2,1)S(1)} %all_to_all.26.z), channel_id=1, source_target_pairs={{0,1},{1,0},{2,3},{3,2},{4,5},{5,4},{6,7},{7,6},{8,9},{9,8},{10,11... | collective-permute-start | bytes 1572872 | tf_op jit(solution)/shard_map/ppermute | solution.py:583
  137.9 1.6 %shard_map.167.rest_0_ = f32[256,512]{1,0:T(8,128)S(1)} custom-call(s32[1]{0:T(128)} %bitcast.core, bf16[4,256,256]{2,1,0:T(8,128)(2,1)S(1)} %all_to_all.26.z, bf16[4,1024,256]{2,1,0:T(8,128)(2,1)} %bitcast.21), custom_call_target="tpu_custom_call" | custom-call | tf_op jit(solution)/shard_map/pallas_call | solution.py:446
  139.5 2.3 %shard_map.168 = bf16[256,512]{1,0:T(8,128)(2,1)} custom-call(s32[1]{0:T(128)S(6)} %sub.3.core, bf16[4,256,256]{2,1,0:T(8,128)(2,1)S(1)} %collective-permute-done.1.z, bf16[4,1024,256]{2,1,0:T(8,128)(2,1)} %bitcast.22, f32[256,512]{1,0:T(8,128)S(1)} %shard_map.167.rest_0_), custom_call_target="tpu_custom_call" | custom-call | tf_op jit(solution)/shard_map/pallas_call | solution.py:446
  (32 shorter events, 0.7 us)
Async XLA Ops:
  6.5 70.3 %all-gather.5.cloned.1.call-start = ((), (), s32[]{:S(2)}) async-start(), calls=%async_computation.5 | async-start | bytes 1392640 | tf_op jit(solution)/shard_map/all_gather | solution.py:499
  12.9 5.2 %copy-start.12 = (bf16[64,320]{1,0:T(8,128)(2,1)S(1)}, bf16[64,320]{1,0:T(8,128)(2,1)}, u32[]{:S(2)}) copy-start(bf16[64,320]{1,0:T(8,128)(2,1)} %get-tuple-element.31) | copy-start | bytes 122884
  12.9 42.7 %all-to-all-start = ((bf16[4,256,1024]{2,1,0:T(8,128)(2,1)}), bf16[4,256,1024]{2,1,0:T(8,128)(2,1)S(1)}, u32[]{:S(2)}, u32[]{:S(2)}) async-start(bf16[4,256,1024]{2,1,0:T(8,128)(2,1)} %get-tuple-element.30), calls=%async_computation | async-start | bytes 4194304 | tf_op jit(solution)/shard_map/all_to_all | solution.py:507
  55.6 14.2 %copy-start = (f32[256,128]{1,0:T(8,128)S(1)}, f32[256,128]{1,0:T(8,128)}, u32[]{:S(2)}) copy-start(f32[256,128]{1,0:T(8,128)} %get-tuple-element.35.inverse) | copy-start | bytes 393220
  55.6 14.2 %copy-start.4 = (bf16[64,128]{1,0:T(8,128)(2,1)S(1)}, bf16[64,128]{1,0:T(8,128)(2,1)}, u32[]{:S(2)}) copy-start(bf16[64,128]{1,0:T(8,128)(2,1)} %second.1) | copy-start | bytes 49156
  58.3 11.6 %all-to-all-start.1 = ((bf16[4,640,128]{2,1,0:T(8,128)(2,1)}), bf16[4,640,128]{2,1,0:T(8,128)(2,1)S(1)}, u32[]{:S(2)}, u32[]{:S(2)}) async-start(bf16[4,640,128]{2,1,0:T(8,128)(2,1)} %get-tuple-element.34), calls=%async_computation.1 | async-start | bytes 1310720 | tf_op jit(solution)/shard_map/all_to_all | solution.py:513
  62.1 67.5 %all-gather.7.cloned.1.call-start = ((), (), s32[]{:S(2)}) async-start(), calls=%async_computation.6 | async-start | bytes 2621440 | tf_op jit(solution)/shard_map/all_gather | solution.py:539
  62.1 14.7 %collective-permute-start = (bf16[4,16,1024]{2,1,0:T(8,128)(2,1)}, bf16[4,16,1024]{2,1,0:T(8,128)(2,1)S(1)}, u32[]{:S(2)}, u32[]{:S(2)}) collective-permute-start(bf16[4,16,1024]{2,1,0:T(8,128)(2,1)} %get-tuple-element.38), channel_id=1, source_target_pairs={{0,32},{32,64},{64,96},{96,128},{128,160},{160,192},{192,224},{224... | collective-permute-start | bytes 393224 | tf_op jit(solution)/shard_map/ppermute | solution.py:512
  69.8 0.7 copy-start.5
  70.5 0.7 copy-start.10
  72.6 0.6 copy-start.1
  73.2 0.6 copy-start.6
  76.8 3.7 %copy-start.2 = (bf16[4,80,128]{2,1,0:T(8,128)(2,1)S(1)}, bf16[4,80,128]{2,1,0:T(8,128)(2,1)}, u32[]{:S(2)}) copy-start(bf16[4,80,128]{2,1,0:T(8,128)(2,1)} %copy-done.1) | copy-start | bytes 245764
  76.8 15.9 %copy-start.11 = (f32[1,2,64,64]{3,2,1,0:T(8,128)S(1)}, f32[1,2,64,64]{3,2,1,0:T(8,128)}, u32[]{:S(2)}) copy-start(f32[1,2,64,64]{3,2,1,0:T(8,128)} %param.29) | copy-start | bytes 98308
  80.4 27.8 %copy-start.3 = (bf16[1,128,128]{2,1,0:T(8,128)(2,1)S(1)}, bf16[1,128,128]{2,1,0:T(8,128)(2,1)}, u32[]{:S(2)}) copy-start(bf16[1,128,128]{2,1,0:T(8,128)(2,1)} %param.30) | copy-start | bytes 98308
  80.4 27.8 %copy-start.7 = (f32[4,128]{1,0:T(4,128)S(1)}, f32[4,128]{1,0:T(4,128)}, u32[]{:S(2)}) copy-start(f32[4,128]{1,0:T(4,128)} %copy-done.6) | copy-start | bytes 6148
  80.4 27.8 %copy-start.8 = (f32[128]{0:T(128)S(1)}, f32[128]{0:T(128)}, u32[]{:S(2)}) copy-start(f32[128]{0:T(128)} %param.28) | copy-start | bytes 1540
  80.4 27.8 %copy-start.9 = (f32[128]{0:T(128)S(1)}, f32[128]{0:T(128)}, u32[]{:S(2)}) copy-start(f32[128]{0:T(128)} %param.31) | copy-start | bytes 1540
  89.2 19.0 %all-to-all-start.3 = ((bf16[4,784,128]{2,1,0:T(8,128)(2,1)}), bf16[4,784,128]{2,1,0:T(8,128)(2,1)S(1)}, u32[]{:S(2)}, u32[]{:S(2)}) async-start(bf16[4,784,128]{2,1,0:T(8,128)(2,1)} %get-tuple-element.39), calls=%async_computation.3 | async-start | bytes 1605632 | tf_op jit(solution)/shard_map/all_to_all | solution.py:540
  129.7 9.9 %collective-permute-start.1 = (bf16[4,256,256]{2,1,0:T(8,128)(2,1)S(1)}, bf16[4,256,256]{2,1,0:T(8,128)(2,1)S(1)}, u32[]{:S(2)}, u32[]{:S(2)}) collective-permute-start(bf16[4,256,256]{2,1,0:T(8,128)(2,1)S(1)} %all_to_all.26.z), channel_id=1, source_target_pairs={{0,1},{1,0},{2,3},{3,2},{4,5},{5,4},{6,7},{7,6},{8,9},{9,8},{10,11... | collective-permute-start | bytes 1572872 | tf_op jit(solution)/shard_map/ppermute | solution.py:583
Sparse Core Ops, SparseCore 0:
  9.4 67.3 all-gather.4
  80.6 49.0 all-gather.6

commit v10 on v9

--- a/solution.py
+++ b/solution.py
@@ -28,7 +28,7 @@
         out_specs=[vmem] * len(outs),
         out_shape=outs,
         input_output_aliases=aliases,
-        compiler_params=limit if name in ("local", "finish") else None,
+        compiler_params=limit if name in ("local", "finish", "output") else None,
     )(*args)
 
 
@@ -151,14 +151,18 @@
     across = pltpu.make_async_copy(held.at[:, columns:], quarter, left.at[4])
     across.start()
     weight = held[:, :columns]
+    edges = jnp.dot(
+        ends[...].reshape(4 * HALO, x.shape[2]),
+        weight[:, 2 * LANES :],
+        preferred_element_type=f32,
+    ).astype(bf16)
     copies = [across]
     for f in range(4):
         p = first if f == 0 else jnp.dot(x[f], weight, preferred_element_type=f32)
         for j in range(3):
             at = slice(j * tokens, (j + 1) * tokens)
             made[f, at] = p[:, j * LANES : (j + 1) * LANES].astype(bf16)
-        edge = jnp.dot(ends[f], weight[:, 2 * LANES :], preferred_element_type=f32)
-        made[f, 3 * tokens :] = edge.astype(bf16)
+        made[f, 3 * tokens :] = edges[f * HALO : (f + 1) * HALO]
         copies.append(pltpu.make_async_copy(made.at[f], out.at[f], left.at[f]))
         copies[f + 1].start()
     for c in copies:
@@ -416,48 +420,59 @@
         mine[to, :, :LANES] = done
 
 
-def output_kernel(core, z, rows, *rest):
-    *before, out, held, arrived = rest
+def block_of(held, x):
+    return jnp.concatenate(
+        [
+            jnp.concatenate([held[x, f, :, :LANES], held[x, f, :, LANES:]], axis=0)
+            for f in range(held.shape[1])
+        ],
+        axis=1,
+    )
+
+
+def half_kernel(core, z, rows, out, staged, held, arrived):
+    steps = z.shape[0]
     copies = []
+    for j, (to, c) in enumerate(((held, core[0]), (staged, 1 - core[0]))):
+        for x in range(steps):
+            at = pl.ds(pl.multiple_of((2 * x + c) * LANES, LANES), LANES)
+            k = j * steps + x
+            copies.append(pltpu.make_async_copy(rows.at[:, at], to.at[x], arrived.at[k]))
+            copies[k].start()
+    total = jnp.zeros(out.shape, f32)
+    for x in range(steps):
+        copies[x].wait()
+        total = total + jnp.dot(z[x], block_of(held, x), preferred_element_type=f32)
+    out[...] = total
+    for x in range(steps):
+        copies[steps + x].wait()
+
+
+def output_kernel(z, staged, half, out):
+    total = half[...]
     for x in range(z.shape[0]):
-        at = pl.ds(pl.multiple_of((2 * x + core[0]) * LANES, LANES), LANES)
-        copies.append(pltpu.make_async_copy(rows.at[:, at], held.at[x], arrived.at[x]))
-        copies[x].start()
-    total = jnp.zeros(out.shape, f32)
-    for b in before:
-        total = b[...]
-    for x in range(z.shape[0]):
-        copies[x].wait()
-        w = jnp.concatenate(
-            [
-                jnp.concatenate([held[x, f, :, :LANES], held[x, f, :, LANES:]], axis=0)
-                for f in range(rows.shape[0])
-            ],
-            axis=1,
-        )
-        total = total + jnp.dot(z[x], w, preferred_element_type=f32)
+        total = total + jnp.dot(z[x], block_of(staged, x), preferred_element_type=f32)
     out[...] = total.astype(out.dtype)
 
 
-def output(core, z, rows, before, out):
+def first_half(core, z, rows):
     vmem = pl.BlockSpec(memory_space=pltpu.VMEM)
-    steps = z.shape[0]
-    parts, _, width = rows.shape
+    steps, tokens, width = z.shape
+    parts = rows.shape[0]
+    shape = (steps, parts, LANES, width)
     return pl.pallas_call(
-        output_kernel,
+        half_kernel,
         in_specs=[
             pl.BlockSpec(memory_space=pltpu.SMEM),
             vmem,
-            pl.BlockSpec(memory_space=pl.ANY),
-        ]
-        + [vmem] * len(before),
-        out_specs=vmem,
-        out_shape=out,
-        scratch_shapes=[
-            pltpu.VMEM((steps, parts, LANES, width), bf16),
-            pltpu.SemaphoreType.DMA((steps,)),
-        ],
-    )(core, near(z), rows, *before)
+            pl.BlockSpec(memory_space=pltpu.HBM),
+        ],
+        out_specs=[vmem, vmem],
+        compiler_params=limit,
+        out_shape=[pltpu.VMEM((tokens, parts * LANES), f32), pltpu.VMEM(shape, bf16)],
+        scratch_shapes=[pltpu.VMEM(shape, bf16), pltpu.SemaphoreType.DMA((2 * steps,))],
+        name="half",
+    )(core, near(z), pltpu.with_memory_space_constraint(rows, pltpu.HBM))
 
 
 def body(
@@ -534,10 +549,10 @@
     quads = [[4 * a + b for b in range(4)] for a in range(lax.axis_size("sp") // 4)]
     late, _ = lax.optimization_barrier((late, spread))
     quad = lax.all_to_all(spread, "sp", 0, 0, axis_index_groups=quads)
-    late, quarter = late_partials(near(x), late, near(ends))
-    _, _, quad = lax.optimization_barrier((late, quarter, quad))
+    late_parts, quarter = late_partials(near(x), late, near(ends))
+    _, _, quad = lax.optimization_barrier((late_parts, quarter, quad))
     out_rows = lax.all_gather(quarter, "fs")
-    late = lax.all_to_all(late, "fs", 0, 0)
+    late = lax.all_to_all(late_parts, "fs", 0, 0)
     sp = lax.axis_index("sp").astype(jnp.int32).reshape(1)
     total, within, log_within, inverse_within = call(
         quad_kernel,
@@ -582,8 +597,16 @@
     same, out_rows = lax.optimization_barrier((same, out_rows))
     other = lax.ppermute(same, "tp", [(i, i ^ 1) for i in range(peers)])
     core = (tp & 1).reshape(1)
-    half = output(core, same, out_rows, (), pltpu.VMEM((tokens, columns), f32))
-    result = output(1 - core, other, out_rows, (near(half),), struct((tokens, columns), bf16))
+    half, staged = first_half(core, same, out_rows)
+    (result,) = call(
+        output_kernel,
+        [struct((tokens, columns), bf16)],
+        "output",
+        near(other),
+        near(staged),
+        near(half),
+        scalars=0,
+    )
     return result[None]
 
 
@@ -609,4 +632,6 @@
     )
     out_specs = P("fs", "sp", "tp")
 
-    return jax.shard_map(body, mesh=mesh, in_specs=in_specs, out_specs=out_specs, check_vma=False)
+    return jax.shard_map(
+        body, mesh=mesh, in_specs=in_specs, out_specs=out_specs, check_vma=False
+    )

time: 149 us -> 148 us (level)
    pallas_call x2 -> x1, Pallas kernels: 3.87 us -> 1.63 us  [first_half(): pl.pallas_call(half_kernel, in_specs=[pl.BlockSpec(memory_space=pltpu.SME...]
    pallas_call x4 -> x5, Pallas kernels: 4.88 us -> 6.01 us  [call(): pl.pallas_call(kernel, in_specs=[smem] * scalars + [vmem] * (len(args) -...]
where the time goes in v10:
time: 148 us
  blocking collectives  72.8 us (49%)
  starting transfers between devices  22.8 us (15%)
  Pallas kernels  18.5 us (12%)
  waiting for transfers between devices  17.1 us (12%)
  between operations  13.6 us (9%)
  local copies, waits for them, and re-layouts  2.66 us (2%)
    all_gather x1, blocking collectives, body(): early = lax.all_gather(early, 'sp').reshape(-1, early.shape[1])  37.9 us
    all_gather x1, blocking collectives, body(): runs = lax.all_gather(total[0], 'sp', axis_index_groups=strided)  15.1 us
    all_to_all x1, blocking collectives, body(): same = lax.all_to_all(mine, 'tp', 0, 0, axis_index_groups=groups)  11 us
    all_to_all x1, blocking collectives, body(): quad = lax.all_to_all(spread, 'sp', 0, 0, axis_index_groups=quads)  8.86 us
    all_gather x1, waiting for transfers between devices, body(): out_rows = lax.all_gather(quarter, 'fs')  8.77 us
    ppermute x1, starting transfers between devices, body(): other = lax.ppermute(same, 'tp', [(i, i ^ 1) for i in range(peers)])  8.45 us
    pallas_call x5, Pallas kernels, call(): pl.pallas_call(kernel, in_specs=[smem] * scalars + [vmem] * (len(args) -...  6.01 us
    all_to_all x1, waiting for transfers between devices, body(): parts = lax.all_to_all(parts, 'fs', 0, 0)  5.51 us
  transfers between devices with their start and end apart: 7, of which 3 were waited for; matrix products, arithmetic and copies ran while one was open for 0% of the time, Pallas kernels for 8%

profile of v10, /device:TPU:1, one launch (start us, length us, event | category | flops | bytes accessed | tf_op | source)
XLA Modules:
  0.0 147.5 jit_solution(13668429442011755177)
XLA Ops:
  6.5 1.6 %shard_map.163 = bf16[64,640]{1,0:T(8,128)(2,1)} custom-call(s32[1]{0:T(128)} %bitcast.2.own, bf16[64,128]{1,0:T(8,128)(2,1)} %query.1, bf16[64,128]{1,0:T(8,128)(2,1)} %gate.1, bf16[64,128]{1,0:T(8,128)(2,1)} %pool.1, bf16[64,512]{1,0:T(8,128)(2,1)} %pool_rows.1, bf16[64,512]{1,0:T(8,128)(2,1)} %state_rows.1), custom_call_target="tpu_custom_call" | custom-call | tf_op jit(solution)/shard_map/pallas_call | solution.py:25
  8.1 4.7 %prep.1 = (bf16[4,256,1024]{2,1,0:T(8,128)(2,1)}, f32[256,128]{1,0:T(8,128)}, bf16[64,320]{1,0:T(8,128)(2,1)}) custom-call(bf16[256,4096]{1,0:T(8,128)(2,1)} %bitcast.21, f32[1,4096]{1,0:T(1,128)} %bitcast.24, bf16[64,128]{1,0:T(8,128)(2,1)} %key.1, bf16[64,128]{1,0:T(8,128)(2,1)} %value.1, bf16[64,64]{1,0:T(8,128)(2,1)} %low.1), custom_call_target="tpu_custom_call" | custom-call | tf_op jit(solution)/shard_map/prep/pallas_call | solution.py:98
  12.9 5.1 %all-to-all-start = ((bf16[4,256,1024]{2,1,0:T(8,128)(2,1)}), bf16[4,256,1024]{2,1,0:T(8,128)(2,1)S(1)}, u32[]{:S(2)}, u32[]{:S(2)}) async-start(bf16[4,256,1024]{2,1,0:T(8,128)(2,1)} %get-tuple-element.32), calls=%async_computation | async-start | bytes 4194304 | tf_op jit(solution)/shard_map/all_to_all | solution.py:522
  18.0 37.9 %all-gather.w = bf16[1024,320]{1,0:T(8,128)(2,1)S(1)} all-gather(bf16[64,320]{1,0:T(8,128)(2,1)S(1)} %copy-done.12), channel_id=2, replica_groups=mesh['sp'=16,'fs'=4,'tp'=8] {'sp'}, dimensions={0}, use_global_device_ids=true | all-gather | bytes 696320 | tf_op jit(solution)/shard_map/all_gather | solution.py:523
  56.0 2.7 %early_parts.1 = (bf16[4,640,128]{2,1,0:T(8,128)(2,1)}, bf16[4,256,1024]{2,1,0:T(8,128)(2,1)S(1)}, bf16[4,16,1024]{2,1,0:T(8,128)(2,1)}) custom-call(bf16[4,256,1024]{2,1,0:T(8,128)(2,1)S(1)} %all-to-all-done.x, bf16[1024,320]{1,0:T(8,128)(2,1)S(1)} %all-gather.w), custom_call_target="tpu_custom_call", output_to_operand_aliasing={{1}: (0, {})} | custom-call | tf_op jit(solution)/shard_map/early_parts/pallas_call | solution.py:177
  58.7 3.6 %all-to-all-start.1 = ((bf16[4,640,128]{2,1,0:T(8,128)(2,1)}), bf16[4,640,128]{2,1,0:T(8,128)(2,1)S(1)}, u32[]{:S(2)}, u32[]{:S(2)}) async-start(bf16[4,640,128]{2,1,0:T(8,128)(2,1)} %get-tuple-element.36), calls=%async_computation.1 | async-start | bytes 1310720 | tf_op jit(solution)/shard_map/all_to_all | solution.py:528
  62.3 2.1 %collective-permute-start = (bf16[4,16,1024]{2,1,0:T(8,128)(2,1)}, bf16[4,16,1024]{2,1,0:T(8,128)(2,1)S(1)}, u32[]{:S(2)}, u32[]{:S(2)}) collective-permute-start(bf16[4,16,1024]{2,1,0:T(8,128)(2,1)} %get-tuple-element.40), channel_id=1, source_target_pairs={{0,32},{32,64},{64,96},{96,128},{128,160},{160,192},{192,224},{224... | collective-permute-start | bytes 393224 | tf_op jit(solution)/shard_map/ppermute | solution.py:527
  64.4 5.5 %all-to-all-done.1.parts = bf16[4,640,128]{2,1,0:T(8,128)(2,1)S(1)} async-done(((bf16[4,640,128]{2,1,0:T(8,128)(2,1)}), bf16[4,640,128]{2,1,0:T(8,128)(2,1)S(1)}, u32[]{:S(2)}, u32[]{:S(2)}) %all-to-all-start.1) | async-done | bytes 655392 | tf_op jit(solution)/shard_map/all_to_all | solution.py:528
  69.9 0.7 copy-done.5
  70.6 0.7 copy-done.10
  71.3 1.4 shard_map.164
  72.7 0.6 copy-done.1
  73.9 2.8 %all-gather.5.cloned.1.call-done.w = bf16[1024,640]{1,0:T(8,128)(2,1)} async-done(((bf16[64,640]{1,0:T(8,128)(2,1)}), bf16[1024,640]{1,0:T(8,128)(2,1)}) %all-gather.5.cloned.1.call-update) | async-done | bytes 1310736 | tf_op jit(solution)/shard_map/all_gather | solution.py:514
  76.7 3.4 %late_parts.1 = (bf16[4,784,128]{2,1,0:T(8,128)(2,1)}, bf16[1024,256]{1,0:T(8,128)(2,1)}) custom-call(bf16[4,256,1024]{2,1,0:T(8,128)(2,1)S(1)} %get-tuple-element.34.x, bf16[1024,640]{1,0:T(8,128)(2,1)} %all-gather.5.cloned.1.call-done.w, bf16[4,16,1024]{2,1,0:T(8,128)(2,1)S(1)} %collective-permute-done.ends), custom_call_target="tpu_custom_call" | custom-call | tf_op jit(solution)/shard_map/late_parts/pallas_call | solution.py:198
  80.2 8.9 %all_to_all.25.quad = bf16[4,80,128]{2,1,0:T(8,128)(2,1)S(1)} all-to-all(bf16[4,80,128]{2,1,0:T(8,128)(2,1)S(1)} %copy-done.2), channel_id=1, replica_groups={{0,32,64,96},{128,160,192,224},{256,288,320,352},{384,416,448,480},{1,3..., dimensions={0} | all-to-all | bytes 163840 | tf_op jit(solution)/shard_map/all_to_all | solution.py:551
  89.1 3.5 %all-to-all-start.3 = ((bf16[4,784,128]{2,1,0:T(8,128)(2,1)}), bf16[4,784,128]{2,1,0:T(8,128)(2,1)S(1)}, u32[]{:S(2)}, u32[]{:S(2)}) async-start(bf16[4,784,128]{2,1,0:T(8,128)(2,1)} %get-tuple-element.41), calls=%async_computation.3 | async-start | bytes 1605632 | tf_op jit(solution)/shard_map/all_to_all | solution.py:555
  92.7 0.7 shard_map.165
  93.4 15.1 %all_gather.21.runs = bf16[4,80,128]{2,1,0:T(8,128)(2,1)S(1)} all-gather(bf16[1,80,128]{2,1,0:T(8,128)(2,1)} %get-tuple-element.44), channel_id=1, replica_groups={{0,128,256,384},{32,160,288,416},{64,192,320,448},{96,224,352,480},{1,1..., dimensions={0}, use_global_device_ids=true | all-gather | bytes 102400 | tf_op jit(solution)/shard_map/all_gather | solution.py:570
  108.4 1.2 shard_map.166
  109.7 11.0 %all_to_all.26.z = bf16[4,256,256]{2,1,0:T(8,128)(2,1)S(1)} all-to-all(bf16[4,256,256]{2,1,0:T(8,128)(2,1)S(1)} %shard_map.166), channel_id=1, replica_groups={{0,2,4,6},{1,3,5,7},{8,10,12,14},{9,11,13,15},{16,18,20,22},{17,19,21,2..., dimensions={0} | all-to-all | bytes 1048576 | tf_op jit(solution)/shard_map/all_to_all | solution.py:596
  120.7 8.8 %all-gather.7.cloned.1.call-done = bf16[4096,256]{1,0:T(8,128)(2,1)} async-done(((bf16[1024,256]{1,0:T(8,128)(2,1)}), bf16[4096,256]{1,0:T(8,128)(2,1)}) %all-gather.7.cloned.1.call-update) | async-done | bytes 2097168 | tf_op jit(solution)/shard_map/all_gather | solution.py:554
  129.4 8.5 %collective-permute-start.1 = (bf16[4,256,256]{2,1,0:T(8,128)(2,1)S(1)}, bf16[4,256,256]{2,1,0:T(8,128)(2,1)S(1)}, u32[]{:S(2)}, u32[]{:S(2)}) collective-permute-start(bf16[4,256,256]{2,1,0:T(8,128)(2,1)S(1)} %all_to_all.26.z), channel_id=1, source_target_pairs={{0,1},{1,0},{2,3},{3,2},{4,5},{5,4},{6,7},{7,6},{8,9},{9,8},{10,11... | collective-permute-start | bytes 1572872 | tf_op jit(solution)/shard_map/ppermute | solution.py:598
  137.9 1.6 %half.1 = (f32[256,512]{1,0:T(8,128)S(1)}, bf16[4,4,128,256]{3,2,1,0:T(8,128)(2,1)S(1)}) custom-call(s32[1]{0:T(128)} %bitcast.13.core, bf16[4,256,256]{2,1,0:T(8,128)(2,1)S(1)} %all_to_all.26.z, bf16[4,1024,256]{2,1,0:T(8,128)(2,1)} %bitcast.22), custom_call_target="tpu_custom_call" | custom-call | tf_op jit(solution)/shard_map/half/pallas_call | solution.py:463
  139.6 1.1 shard_map.167
  (32 shorter events, 0.7 us)
Async XLA Ops:
  6.5 70.2 %all-gather.5.cloned.1.call-start = ((), (), s32[]{:S(2)}) async-start(), calls=%async_computation.5 | async-start | bytes 1392640 | tf_op jit(solution)/shard_map/all_gather | solution.py:514
  12.9 5.2 %copy-start.12 = (bf16[64,320]{1,0:T(8,128)(2,1)S(1)}, bf16[64,320]{1,0:T(8,128)(2,1)}, u32[]{:S(2)}) copy-start(bf16[64,320]{1,0:T(8,128)(2,1)} %get-tuple-element.33) | copy-start | bytes 122884
  12.9 43.1 %all-to-all-start = ((bf16[4,256,1024]{2,1,0:T(8,128)(2,1)}), bf16[4,256,1024]{2,1,0:T(8,128)(2,1)S(1)}, u32[]{:S(2)}, u32[]{:S(2)}) async-start(bf16[4,256,1024]{2,1,0:T(8,128)(2,1)} %get-tuple-element.32), calls=%async_computation | async-start | bytes 4194304 | tf_op jit(solution)/shard_map/all_to_all | solution.py:522
  56.0 14.0 %copy-start = (f32[256,128]{1,0:T(8,128)S(1)}, f32[256,128]{1,0:T(8,128)}, u32[]{:S(2)}) copy-start(f32[256,128]{1,0:T(8,128)} %get-tuple-element.37.inverse) | copy-start | bytes 393220
  56.0 14.0 %copy-start.4 = (bf16[64,128]{1,0:T(8,128)(2,1)S(1)}, bf16[64,128]{1,0:T(8,128)(2,1)}, u32[]{:S(2)}) copy-start(bf16[64,128]{1,0:T(8,128)(2,1)} %second.1) | copy-start | bytes 49156
  58.7 11.3 %all-to-all-start.1 = ((bf16[4,640,128]{2,1,0:T(8,128)(2,1)}), bf16[4,640,128]{2,1,0:T(8,128)(2,1)S(1)}, u32[]{:S(2)}, u32[]{:S(2)}) async-start(bf16[4,640,128]{2,1,0:T(8,128)(2,1)} %get-tuple-element.36), calls=%async_computation.1 | async-start | bytes 1310720 | tf_op jit(solution)/shard_map/all_to_all | solution.py:528
  62.3 67.1 %all-gather.7.cloned.1.call-start = ((), (), s32[]{:S(2)}) async-start(), calls=%async_computation.6 | async-start | bytes 2621440 | tf_op jit(solution)/shard_map/all_gather | solution.py:554
  62.3 14.4 %collective-permute-start = (bf16[4,16,1024]{2,1,0:T(8,128)(2,1)}, bf16[4,16,1024]{2,1,0:T(8,128)(2,1)S(1)}, u32[]{:S(2)}, u32[]{:S(2)}) collective-permute-start(bf16[4,16,1024]{2,1,0:T(8,128)(2,1)} %get-tuple-element.40), channel_id=1, source_target_pairs={{0,32},{32,64},{64,96},{96,128},{128,160},{160,192},{192,224},{224... | collective-permute-start | bytes 393224 | tf_op jit(solution)/shard_map/ppermute | solution.py:527
  69.9 0.7 copy-start.5
  70.6 0.7 copy-start.10
  72.7 0.6 copy-start.1
  73.3 0.6 copy-start.6
  76.7 3.5 %copy-start.2 = (bf16[4,80,128]{2,1,0:T(8,128)(2,1)S(1)}, bf16[4,80,128]{2,1,0:T(8,128)(2,1)}, u32[]{:S(2)}) copy-start(bf16[4,80,128]{2,1,0:T(8,128)(2,1)} %copy-done.1) | copy-start | bytes 245764
  76.7 15.9 %copy-start.11 = (f32[1,2,64,64]{3,2,1,0:T(8,128)S(1)}, f32[1,2,64,64]{3,2,1,0:T(8,128)}, u32[]{:S(2)}) copy-start(f32[1,2,64,64]{3,2,1,0:T(8,128)} %param.29) | copy-start | bytes 98308
  80.1 28.3 %copy-start.3 = (bf16[1,128,128]{2,1,0:T(8,128)(2,1)S(1)}, bf16[1,128,128]{2,1,0:T(8,128)(2,1)}, u32[]{:S(2)}) copy-start(bf16[1,128,128]{2,1,0:T(8,128)(2,1)} %param.30) | copy-start | bytes 98308
  80.2 28.3 %copy-start.7 = (f32[4,128]{1,0:T(4,128)S(1)}, f32[4,128]{1,0:T(4,128)}, u32[]{:S(2)}) copy-start(f32[4,128]{1,0:T(4,128)} %copy-done.6) | copy-start | bytes 6148
  80.2 28.3 %copy-start.8 = (f32[128]{0:T(128)S(1)}, f32[128]{0:T(128)}, u32[]{:S(2)}) copy-start(f32[128]{0:T(128)} %param.28) | copy-start | bytes 1540
  80.2 28.3 %copy-start.9 = (f32[128]{0:T(128)S(1)}, f32[128]{0:T(128)}, u32[]{:S(2)}) copy-start(f32[128]{0:T(128)} %param.31) | copy-start | bytes 1540
  89.1 19.3 %all-to-all-start.3 = ((bf16[4,784,128]{2,1,0:T(8,128)(2,1)}), bf16[4,784,128]{2,1,0:T(8,128)(2,1)S(1)}, u32[]{:S(2)}, u32[]{:S(2)}) async-start(bf16[4,784,128]{2,1,0:T(8,128)(2,1)} %get-tuple-element.41), calls=%async_computation.3 | async-start | bytes 1605632 | tf_op jit(solution)/shard_map/all_to_all | solution.py:555
  129.4 10.1 %collective-permute-start.1 = (bf16[4,256,256]{2,1,0:T(8,128)(2,1)S(1)}, bf16[4,256,256]{2,1,0:T(8,128)(2,1)S(1)}, u32[]{:S(2)}, u32[]{:S(2)}) collective-permute-start(bf16[4,256,256]{2,1,0:T(8,128)(2,1)S(1)} %all_to_all.26.z), channel_id=1, source_target_pairs={{0,1},{1,0},{2,3},{3,2},{4,5},{5,4},{6,7},{7,6},{8,9},{9,8},{10,11... | collective-permute-start | bytes 1572872 | tf_op jit(solution)/shard_map/ppermute | solution.py:598
Sparse Core Ops, SparseCore 0:
  9.4 67.2 all-gather.4
  80.3 49.0 all-gather.6

commit v11 on v10

--- a/solution.py
+++ b/solution.py
@@ -41,10 +41,25 @@
 
 
 def pack_late_kernel(own, query, gate, pool, pool_rows, state_rows, late):
-    mine = pl.ds(pl.multiple_of(own[0] * LANES, LANES), LANES)
-    blocks = (query[...], gate[...], pool[...], pool_rows[:, mine], state_rows[:, mine])
-    for j, block in enumerate(blocks):
-        late[:, j * LANES : (j + 1) * LANES] = block
+    for j, block in enumerate((query, gate, pool, pool_rows, state_rows)):
+        late[:, j * LANES : (j + 1) * LANES] = block[...]
+
+
+def pack_late(own, query, gate, pool, pool_rows, state_rows):
+    rows = query.shape[0]
+    whole = pl.BlockSpec((rows, LANES), lambda i, own: (0, 0))
+    mine = pl.BlockSpec((rows, LANES), lambda i, own: (0, own[0]))
+    return pl.pallas_call(
+        pack_late_kernel,
+        grid_spec=pltpu.PrefetchScalarGridSpec(
+            num_scalar_prefetch=1,
+            grid=(1,),
+            in_specs=[whole, whole, whole, mine, mine],
+            out_specs=pl.BlockSpec((rows, 5 * LANES), lambda i, own: (0, 0)),
+        ),
+        out_shape=struct((rows, 5 * LANES), bf16),
+        name="pack_late",
+    )(own, query, gate, pool, pool_rows, state_rows)
 
 
 def prep_kernel(
@@ -495,14 +510,10 @@
     attention_output_rows,
 ):
     _, tokens, width = activations.shape
-    rows = key_projection_weight.shape[0]
     columns = pooling_output_rows.shape[1]
     own = lax.axis_index("fs").astype(jnp.int32).reshape(1)
     tp = lax.axis_index("tp").astype(jnp.int32)
-    (late,) = call(
-        pack_late_kernel,
-        [struct((rows, 5 * LANES), bf16)],
-        "pack_late",
+    late = pack_late(
         own,
         query_projection_weight,
         output_gate_weight,

time: 148 us -> 148 us (level)
    pallas_call x5 -> x4, Pallas kernels: 6.01 us -> 4.45 us  [call(): pl.pallas_call(kernel, in_specs=[smem] * scalars + [vmem] * (len(args) -...]
where the time goes in v11:
time: 148 us; the launch traced here: 147 us
  blocking collectives  72.1 us (49%)
  starting transfers between devices  23.1 us (16%)
  Pallas kernels  18.4 us (12%)
  waiting for transfers between devices  17.5 us (12%)
  between operations  13.6 us (9%)
  local copies, waits for them, and re-layouts  2.66 us (2%)
    all_gather x1, blocking collectives, body(): early = lax.all_gather(early, 'sp').reshape(-1, early.shape[1])  37.7 us
    all_gather x1, blocking collectives, body(): runs = lax.all_gather(total[0], 'sp', axis_index_groups=strided)  15.2 us
    all_to_all x1, blocking collectives, body(): same = lax.all_to_all(mine, 'tp', 0, 0, axis_index_groups=groups)  11 us
    ppermute x1, starting transfers between devices, body(): other = lax.ppermute(same, 'tp', [(i, i ^ 1) for i in range(peers)])  8.65 us
    all_gather x1, waiting for transfers between devices, body(): out_rows = lax.all_gather(quarter, 'fs')  8.39 us
    all_to_all x1, blocking collectives, body(): quad = lax.all_to_all(spread, 'sp', 0, 0, axis_index_groups=quads)  8.21 us
    all_to_all x1, waiting for transfers between devices, body(): parts = lax.all_to_all(parts, 'fs', 0, 0)  5.75 us
    all_to_all x1, starting transfers between devices, body(): x = lax.all_to_all(x, 'fs', 0, 0)  5.14 us
  transfers between devices with their start and end apart: 7, of which 3 were waited for; matrix products, arithmetic and copies ran while one was open for 0% of the time, Pallas kernels for 8%

profile of v11, /device:TPU:1, one launch (start us, length us, event | category | flops | bytes accessed | tf_op | source)
XLA Modules:
  0.0 147.4 jit_solution(5181933381143535443)
XLA Ops:
  6.5 1.4 pack_late.1
  8.0 4.7 %prep.1 = (bf16[4,256,1024]{2,1,0:T(8,128)(2,1)}, f32[256,128]{1,0:T(8,128)}, bf16[64,320]{1,0:T(8,128)(2,1)}) custom-call(bf16[256,4096]{1,0:T(8,128)(2,1)} %bitcast.21, f32[1,4096]{1,0:T(1,128)} %bitcast.24, bf16[64,128]{1,0:T(8,128)(2,1)} %key.1, bf16[64,128]{1,0:T(8,128)(2,1)} %value.1, bf16[64,64]{1,0:T(8,128)(2,1)} %low.1), custom_call_target="tpu_custom_call" | custom-call | tf_op jit(solution)/shard_map/prep/pallas_call | solution.py:113
  12.8 5.1 %all-to-all-start = ((bf16[4,256,1024]{2,1,0:T(8,128)(2,1)}), bf16[4,256,1024]{2,1,0:T(8,128)(2,1)S(1)}, u32[]{:S(2)}, u32[]{:S(2)}) async-start(bf16[4,256,1024]{2,1,0:T(8,128)(2,1)} %get-tuple-element.32), calls=%async_computation | async-start | bytes 4194304 | tf_op jit(solution)/shard_map/all_to_all | solution.py:533
  17.9 37.7 %all-gather.w = bf16[1024,320]{1,0:T(8,128)(2,1)S(1)} all-gather(bf16[64,320]{1,0:T(8,128)(2,1)S(1)} %copy-done.12), channel_id=2, replica_groups=mesh['sp'=16,'fs'=4,'tp'=8] {'sp'}, dimensions={0}, use_global_device_ids=true | all-gather | bytes 696320 | tf_op jit(solution)/shard_map/all_gather | solution.py:534
  55.6 2.7 %early_parts.1 = (bf16[4,640,128]{2,1,0:T(8,128)(2,1)}, bf16[4,256,1024]{2,1,0:T(8,128)(2,1)S(1)}, bf16[4,16,1024]{2,1,0:T(8,128)(2,1)}) custom-call(bf16[4,256,1024]{2,1,0:T(8,128)(2,1)S(1)} %all-to-all-done.x, bf16[1024,320]{1,0:T(8,128)(2,1)S(1)} %all-gather.w), custom_call_target="tpu_custom_call", output_to_operand_aliasing={{1}: (0, {})} | custom-call | tf_op jit(solution)/shard_map/early_parts/pallas_call | solution.py:192
  58.3 4.0 %all-to-all-start.1 = ((bf16[4,640,128]{2,1,0:T(8,128)(2,1)}), bf16[4,640,128]{2,1,0:T(8,128)(2,1)S(1)}, u32[]{:S(2)}, u32[]{:S(2)}) async-start(bf16[4,640,128]{2,1,0:T(8,128)(2,1)} %get-tuple-element.36), calls=%async_computation.1 | async-start | bytes 1310720 | tf_op jit(solution)/shard_map/all_to_all | solution.py:539
  62.3 1.9 %collective-permute-start = (bf16[4,16,1024]{2,1,0:T(8,128)(2,1)}, bf16[4,16,1024]{2,1,0:T(8,128)(2,1)S(1)}, u32[]{:S(2)}, u32[]{:S(2)}) collective-permute-start(bf16[4,16,1024]{2,1,0:T(8,128)(2,1)} %get-tuple-element.40), channel_id=1, source_target_pairs={{0,32},{32,64},{64,96},{96,128},{128,160},{160,192},{192,224},{224... | collective-permute-start | bytes 393224 | tf_op jit(solution)/shard_map/ppermute | solution.py:538
  64.2 5.8 %all-to-all-done.1.parts = bf16[4,640,128]{2,1,0:T(8,128)(2,1)S(1)} async-done(((bf16[4,640,128]{2,1,0:T(8,128)(2,1)}), bf16[4,640,128]{2,1,0:T(8,128)(2,1)S(1)}, u32[]{:S(2)}, u32[]{:S(2)}) %all-to-all-start.1) | async-done | bytes 655392 | tf_op jit(solution)/shard_map/all_to_all | solution.py:539
  69.9 0.7 copy-done.5
  70.6 0.7 copy-done.10
  71.3 1.4 shard_map.163
  72.7 0.6 copy-done.1
  73.9 3.3 %all-gather.5.cloned.1.call-done.w = bf16[1024,640]{1,0:T(8,128)(2,1)} async-done(((bf16[64,640]{1,0:T(8,128)(2,1)}), bf16[1024,640]{1,0:T(8,128)(2,1)}) %all-gather.5.cloned.1.call-update) | async-done | bytes 1310736 | tf_op jit(solution)/shard_map/all_gather | solution.py:525
  77.2 3.4 %late_parts.1 = (bf16[4,784,128]{2,1,0:T(8,128)(2,1)}, bf16[1024,256]{1,0:T(8,128)(2,1)}) custom-call(bf16[4,256,1024]{2,1,0:T(8,128)(2,1)S(1)} %get-tuple-element.34.x, bf16[1024,640]{1,0:T(8,128)(2,1)} %all-gather.5.cloned.1.call-done.w, bf16[4,16,1024]{2,1,0:T(8,128)(2,1)S(1)} %collective-permute-done.ends), custom_call_target="tpu_custom_call" | custom-call | tf_op jit(solution)/shard_map/late_parts/pallas_call | solution.py:213
  80.7 8.2 %all_to_all.25.quad = bf16[4,80,128]{2,1,0:T(8,128)(2,1)S(1)} all-to-all(bf16[4,80,128]{2,1,0:T(8,128)(2,1)S(1)} %copy-done.2), channel_id=1, replica_groups={{0,32,64,96},{128,160,192,224},{256,288,320,352},{384,416,448,480},{1,3..., dimensions={0} | all-to-all | bytes 163840 | tf_op jit(solution)/shard_map/all_to_all | solution.py:562
  88.9 3.5 %all-to-all-start.3 = ((bf16[4,784,128]{2,1,0:T(8,128)(2,1)}), bf16[4,784,128]{2,1,0:T(8,128)(2,1)S(1)}, u32[]{:S(2)}, u32[]{:S(2)}) async-start(bf16[4,784,128]{2,1,0:T(8,128)(2,1)} %get-tuple-element.41), calls=%async_computation.3 | async-start | bytes 1605632 | tf_op jit(solution)/shard_map/all_to_all | solution.py:566
  92.5 0.7 shard_map.164
  93.2 15.2 %all_gather.21.runs = bf16[4,80,128]{2,1,0:T(8,128)(2,1)S(1)} all-gather(bf16[1,80,128]{2,1,0:T(8,128)(2,1)} %get-tuple-element.44), channel_id=1, replica_groups={{0,128,256,384},{32,160,288,416},{64,192,320,448},{96,224,352,480},{1,1..., dimensions={0}, use_global_device_ids=true | all-gather | bytes 102400 | tf_op jit(solution)/shard_map/all_gather | solution.py:581
  108.4 1.2 shard_map.165
  109.7 11.0 %all_to_all.26.z = bf16[4,256,256]{2,1,0:T(8,128)(2,1)S(1)} all-to-all(bf16[4,256,256]{2,1,0:T(8,128)(2,1)S(1)} %shard_map.165), channel_id=1, replica_groups={{0,2,4,6},{1,3,5,7},{8,10,12,14},{9,11,13,15},{16,18,20,22},{17,19,21,2..., dimensions={0} | all-to-all | bytes 1048576 | tf_op jit(solution)/shard_map/all_to_all | solution.py:607
  120.7 8.4 %all-gather.7.cloned.1.call-done = bf16[4096,256]{1,0:T(8,128)(2,1)} async-done(((bf16[1024,256]{1,0:T(8,128)(2,1)}), bf16[4096,256]{1,0:T(8,128)(2,1)}) %all-gather.7.cloned.1.call-update) | async-done | bytes 2097168 | tf_op jit(solution)/shard_map/all_gather | solution.py:565
  129.1 8.6 %collective-permute-start.1 = (bf16[4,256,256]{2,1,0:T(8,128)(2,1)S(1)}, bf16[4,256,256]{2,1,0:T(8,128)(2,1)S(1)}, u32[]{:S(2)}, u32[]{:S(2)}) collective-permute-start(bf16[4,256,256]{2,1,0:T(8,128)(2,1)S(1)} %all_to_all.26.z), channel_id=1, source_target_pairs={{0,1},{1,0},{2,3},{3,2},{4,5},{5,4},{6,7},{7,6},{8,9},{9,8},{10,11... | collective-permute-start | bytes 1572872 | tf_op jit(solution)/shard_map/ppermute | solution.py:609
  137.7 1.6 %half.1 = (f32[256,512]{1,0:T(8,128)S(1)}, bf16[4,4,128,256]{3,2,1,0:T(8,128)(2,1)S(1)}) custom-call(s32[1]{0:T(128)} %bitcast.13.core, bf16[4,256,256]{2,1,0:T(8,128)(2,1)S(1)} %all_to_all.26.z, bf16[4,1024,256]{2,1,0:T(8,128)(2,1)} %bitcast.22), custom_call_target="tpu_custom_call" | custom-call | tf_op jit(solution)/shard_map/half/pallas_call | solution.py:478
  139.4 1.1 shard_map.166
  (32 shorter events, 0.7 us)
Async XLA Ops:
  6.5 70.7 %all-gather.5.cloned.1.call-start = ((), (), s32[]{:S(2)}) async-start(), calls=%async_computation.5 | async-start | bytes 1392640 | tf_op jit(solution)/shard_map/all_gather | solution.py:525
  12.7 5.2 %copy-start.12 = (bf16[64,320]{1,0:T(8,128)(2,1)S(1)}, bf16[64,320]{1,0:T(8,128)(2,1)}, u32[]{:S(2)}) copy-start(bf16[64,320]{1,0:T(8,128)(2,1)} %get-tuple-element.33) | copy-start | bytes 122884
  12.8 42.9 %all-to-all-start = ((bf16[4,256,1024]{2,1,0:T(8,128)(2,1)}), bf16[4,256,1024]{2,1,0:T(8,128)(2,1)S(1)}, u32[]{:S(2)}, u32[]{:S(2)}) async-start(bf16[4,256,1024]{2,1,0:T(8,128)(2,1)} %get-tuple-element.32), calls=%async_computation | async-start | bytes 4194304 | tf_op jit(solution)/shard_map/all_to_all | solution.py:533
  55.6 14.3 %copy-start = (f32[256,128]{1,0:T(8,128)S(1)}, f32[256,128]{1,0:T(8,128)}, u32[]{:S(2)}) copy-start(f32[256,128]{1,0:T(8,128)} %get-tuple-element.37.inverse) | copy-start | bytes 393220
  55.6 14.3 %copy-start.4 = (bf16[64,128]{1,0:T(8,128)(2,1)S(1)}, bf16[64,128]{1,0:T(8,128)(2,1)}, u32[]{:S(2)}) copy-start(bf16[64,128]{1,0:T(8,128)(2,1)} %second.1) | copy-start | bytes 49156
  58.3 11.6 %all-to-all-start.1 = ((bf16[4,640,128]{2,1,0:T(8,128)(2,1)}), bf16[4,640,128]{2,1,0:T(8,128)(2,1)S(1)}, u32[]{:S(2)}, u32[]{:S(2)}) async-start(bf16[4,640,128]{2,1,0:T(8,128)(2,1)} %get-tuple-element.36), calls=%async_computation.1 | async-start | bytes 1310720 | tf_op jit(solution)/shard_map/all_to_all | solution.py:539
  62.3 66.8 %all-gather.7.cloned.1.call-start = ((), (), s32[]{:S(2)}) async-start(), calls=%async_computation.6 | async-start | bytes 2621440 | tf_op jit(solution)/shard_map/all_gather | solution.py:565
  62.3 14.9 %collective-permute-start = (bf16[4,16,1024]{2,1,0:T(8,128)(2,1)}, bf16[4,16,1024]{2,1,0:T(8,128)(2,1)S(1)}, u32[]{:S(2)}, u32[]{:S(2)}) collective-permute-start(bf16[4,16,1024]{2,1,0:T(8,128)(2,1)} %get-tuple-element.40), channel_id=1, source_target_pairs={{0,32},{32,64},{64,96},{96,128},{128,160},{160,192},{192,224},{224... | collective-permute-start | bytes 393224 | tf_op jit(solution)/shard_map/ppermute | solution.py:538
  69.9 0.7 copy-start.5
  70.6 0.7 copy-start.10
  72.7 0.6 copy-start.1
  73.3 0.6 copy-start.6
  77.2 3.5 %copy-start.2 = (bf16[4,80,128]{2,1,0:T(8,128)(2,1)S(1)}, bf16[4,80,128]{2,1,0:T(8,128)(2,1)}, u32[]{:S(2)}) copy-start(bf16[4,80,128]{2,1,0:T(8,128)(2,1)} %copy-done.1) | copy-start | bytes 245764
  77.2 15.2 %copy-start.11 = (f32[1,2,64,64]{3,2,1,0:T(8,128)S(1)}, f32[1,2,64,64]{3,2,1,0:T(8,128)}, u32[]{:S(2)}) copy-start(f32[1,2,64,64]{3,2,1,0:T(8,128)} %param.29) | copy-start | bytes 98308
  80.6 27.8 %copy-start.3 = (bf16[1,128,128]{2,1,0:T(8,128)(2,1)S(1)}, bf16[1,128,128]{2,1,0:T(8,128)(2,1)}, u32[]{:S(2)}) copy-start(bf16[1,128,128]{2,1,0:T(8,128)(2,1)} %param.30) | copy-start | bytes 98308
  80.7 27.8 %copy-start.7 = (f32[4,128]{1,0:T(4,128)S(1)}, f32[4,128]{1,0:T(4,128)}, u32[]{:S(2)}) copy-start(f32[4,128]{1,0:T(4,128)} %copy-done.6) | copy-start | bytes 6148
  80.7 27.8 %copy-start.8 = (f32[128]{0:T(128)S(1)}, f32[128]{0:T(128)}, u32[]{:S(2)}) copy-start(f32[128]{0:T(128)} %param.28) | copy-start | bytes 1540
  80.7 27.8 %copy-start.9 = (f32[128]{0:T(128)S(1)}, f32[128]{0:T(128)}, u32[]{:S(2)}) copy-start(f32[128]{0:T(128)} %param.31) | copy-start | bytes 1540
  88.9 19.5 %all-to-all-start.3 = ((bf16[4,784,128]{2,1,0:T(8,128)(2,1)}), bf16[4,784,128]{2,1,0:T(8,128)(2,1)S(1)}, u32[]{:S(2)}, u32[]{:S(2)}) async-start(bf16[4,784,128]{2,1,0:T(8,128)(2,1)} %get-tuple-element.41), calls=%async_computation.3 | async-start | bytes 1605632 | tf_op jit(solution)/shard_map/all_to_all | solution.py:566
  129.1 10.3 %collective-permute-start.1 = (bf16[4,256,256]{2,1,0:T(8,128)(2,1)S(1)}, bf16[4,256,256]{2,1,0:T(8,128)(2,1)S(1)}, u32[]{:S(2)}, u32[]{:S(2)}) collective-permute-start(bf16[4,256,256]{2,1,0:T(8,128)(2,1)S(1)} %all_to_all.26.z), channel_id=1, source_target_pairs={{0,1},{1,0},{2,3},{3,2},{4,5},{5,4},{6,7},{7,6},{8,9},{9,8},{10,11... | collective-permute-start | bytes 1572872 | tf_op jit(solution)/shard_map/ppermute | solution.py:609
Sparse Core Ops, SparseCore 0:
  9.4 67.7 all-gather.4
  80.8 48.1 all-gather.6
